TPU v7x, 32 devices: a whole 2x2x4 slice. The times are simulated.
32 devices in a mesh: grp: 2 (over y), fs: 4 (over z), tp: 4 (over x, core).
Axes of the slice: x: 2, y: 2, z: 4, core: 2. Of those that a mesh axis runs over, the one named last changes fastest.
Arguments:
- tokens: bfloat16 [2560, 2048], P(('grp', 'fs', 'tp')), parts along dimension 0, may hold values from -6 to 6
- mix_gain: bfloat16 [2048], replicated, may hold values from 0.099609375 to 1.8984375
- val_weight: bfloat16 [2048, 1024], P('fs', 'tp'), may hold values from -4 to 4
- gate_weight: bfloat16 [2048, 1024], P('fs', 'tp'), may hold values from -0.125 to 0.125
- conv_taps: bfloat16 [31, 1024], replicated, may hold values from -1 to 1
- chan_gain: bfloat16 [1024], replicated, may hold values from 0.099609375 to 1.8984375
- out_weight: bfloat16 [1024, 2048], P('tp', 'fs'), may hold values from -0.1875 to 0.1875
- mix_post_gain: bfloat16 [2048], replicated, may hold values from 0.099609375 to 1.8984375
- ffn_gain: bfloat16 [2048], replicated, may hold values from 0.099609375 to 1.8984375
- up_gate_weight: bfloat16 [2048, 5120], P('fs', 'tp'), may hold values from -0.125 to 0.125
- up_val_weight: bfloat16 [2048, 5120], P('fs', 'tp'), may hold values from -0.125 to 0.125
- ffn_taps: bfloat16 [2, 3, 5120], replicated, may hold values from -3.5 to 3.5
- down_weight: bfloat16 [5120, 2048], P('tp', 'fs'), may hold values from -0.078125 to 0.078125
- ffn_post_gain: bfloat16 [2048], replicated, may hold values from 0.099609375 to 1.8984375
Outputs:
- layer_out: bfloat16 [2560, 2048], P(('grp', 'fs', 'tp')), parts along dimension 0
There are 2 independent parts, one for each index of `grp`. A program takes and returns all parts, laid end to end along the dimension named above; an argument that names none is the same for every part. Nothing has to cross between parts.
All inputs are finite; a program needn't handle non-finite values.
Results may differ from a plain program's by a relative error of at most 0.019.
Values may be sent and summed in bfloat16 or wider, within the bound.
No kernel may reach another device: no remote copies, remote signals or barrier semaphores. Data moves between devices by JAX's collectives and lax.ppermute only.
A program may use at most 64 MiB of HBM per device.

v0:
```python
import jax
import jax.numpy as jnp
from jax import lax
from jax.experimental import pallas as pl
from jax.experimental.pallas import tpu as pltpu
from jax.sharding import PartitionSpec as P

LEN = 64
LANES = 128
BF16 = jnp.bfloat16
F32 = jnp.float32
MEBI = 2**20

norm_epsilon = 1e-06
chan_epsilon = 1e-05


def rms_scale(values, gain):
    inverse = lax.rsqrt(jnp.mean(values * values, axis=-1, keepdims=True) + norm_epsilon)
    return values * inverse * gain.astype(jnp.float32)


def depthwise(signal, tap_table):
    taps_count = tap_table.shape[0]
    channels = signal.shape[1]
    shaped = signal.astype(jnp.float32).reshape(signal.shape[0] // LEN, LEN, channels)
    padded = jnp.pad(shaped, ((0, 0), (taps_count - 1, 0), (0, 0)))
    tap_values = tap_table.astype(jnp.float32)
    result = jnp.zeros(shaped.shape, jnp.float32)
    for offset in range(taps_count):
        result = result + padded[:, offset : offset + LEN, :] * tap_values[offset]
    return result.reshape(signal.shape[0], channels)


def product(left, weight):
    return jnp.dot(left, weight, preferred_element_type=jnp.float32)


def swap(array, axis, size, bits):
    return lax.ppermute(array, axis, [(i, i ^ bits) for i in range(size)])


def pick(array, *indices):
    for index in indices:
        array = lax.dynamic_index_in_dim(array, index, 0, keepdims=False)
    return array


def halvings(size):
    return [1 << b for b in reversed(range(size.bit_length() - 1))]


def gather_blocks(block, axis, size):
    blocks = {0: block}
    for bits in halvings(size):
        for d in list(blocks):
            blocks[d | bits] = swap(blocks[d], axis, size, bits)
    return blocks


def scatter_blocks(blocks, axis, size):
    terms = {d: [b] for d, b in blocks.items()}
    for bits in reversed(halvings(size)):
        kept = {}
        for d in terms:
            if not d & bits:
                sent = add_terms(terms[d | bits])
                other = swap(sent, axis, size, bits)
                kept[d] = [*terms[d], other]
        terms = kept
    return terms[0]


def add_terms(terms):
    if len(terms) == 1:
        return terms[0]
    return sum(t.astype(F32) for t in terms).astype(BF16)


VMEM = pl.BlockSpec(memory_space=pltpu.VMEM)
SMEM = pl.BlockSpec(memory_space=pltpu.SMEM)
HBM = pl.BlockSpec(memory_space=pl.ANY)


def aligned(index, size):
    return pl.ds(pl.multiple_of(index * size, 16), size)


def start_copies(pairs, sems, first=0):
    copies = []
    for i, (source, target) in enumerate(pairs):
        copies.append(pltpu.make_async_copy(source, target, sems.at[first + i]))
        copies[-1].start()
    return copies


def row_kernel(body, arrays, outs):
    count = len(arrays)

    def run(*refs):
        results = body(*[ref[...].astype(F32) for ref in refs[:count]])
        for ref, result in zip(refs[count:], results):
            ref[...] = result.astype(ref.dtype)

    return pl.pallas_call(
        run,
        in_specs=[VMEM] * count,
        out_specs=[VMEM] * outs,
        out_shape=[jax.ShapeDtypeStruct(arrays[0].shape, BF16)] * outs,
        cost_estimate=pl.CostEstimate(
            flops=8 * arrays[0].size, transcendentals=0, bytes_accessed=4 * arrays[0].size
        ),
        compiler_params=pltpu.CompilerParams(vmem_limit_bytes=12 * MEBI),
    )(*arrays)


def glu_conv(spot, sizes, blocks, own, pieces, taps):
    ng, nf, nt = sizes
    rows, width = blocks[0].shape
    total = nt * rows
    depth, packed = own.shape
    share = depth // ng
    channels = packed // 2
    count = taps.shape[0]
    lead = -(-(count - 1) // 8) * 8
    segments = total // LEN
    keys = list(pieces)

    def run(spot_ref, taps_ref, *refs):
        block_refs, refs = refs[:nt], refs[nt:]
        own_ref, refs = refs[0], refs[1:]
        piece_refs, refs = refs[: len(keys)], refs[len(keys) :]
        conv_ref, sums_ref, gathered, weight, padded, sems = refs
        group, slab, member = spot_ref[0], spot_ref[1], spot_ref[2]
        pairs = [(block_refs[d], gathered.at[aligned(member ^ d, rows)]) for d in range(nt)]
        pairs.append((own_ref, weight.at[aligned(slab, depth)]))
        for (d, e), ref in zip(keys, piece_refs):
            place = (slab ^ d) * ng + (group ^ e)
            pairs.append((ref, weight.at[aligned(place, share)]))
        copies = start_copies(pairs, sems)
        padded[:, :lead, :] = jnp.zeros((segments, lead, channels), F32)
        for copy in copies:
            copy.wait()
        both = product(gathered[...], weight[...])
        glu = both[:, :channels] * jax.nn.sigmoid(both[:, channels:])
        glu = glu.astype(BF16).astype(F32)
        padded[:, lead:, :] = glu.reshape(segments, LEN, channels)

        def segment(s, carry):
            result = jnp.zeros((LEN, channels), F32)
            for k in range(count):
                begin = lead - (count - 1) + k
                result = result + padded[s, begin : begin + LEN, :] * taps_ref[k : k + 1, :]
            conv_ref[aligned(s, LEN), :] = result
            return carry

        lax.fori_loop(0, segments, segment, 0)
        conv = conv_ref[...]
        ones = jnp.ones((8, channels), F32)
        over = (((1,), (1,)), ((), ()))
        for i, term in enumerate((conv, conv * conv)):
            sums_ref[8 * i : 8 * i + 8, :] = lax.dot_general(
                ones, term, over, precision=lax.Precision.HIGHEST, preferred_element_type=F32
            )

    return pl.pallas_call(
        run,
        in_specs=[SMEM, VMEM] + [HBM] * (nt + 1 + len(keys)),
        out_specs=[VMEM, VMEM],
        out_shape=[
            jax.ShapeDtypeStruct((total, channels), F32),
            jax.ShapeDtypeStruct((16, total), F32),
        ],
        scratch_shapes=[
            pltpu.VMEM((total, width), BF16),
            pltpu.VMEM((nf * depth, packed), BF16),
            pltpu.VMEM((segments, lead + LEN, channels), F32),
            pltpu.SemaphoreType.DMA((nt + 1 + len(keys),)),
        ],
        cost_estimate=pl.CostEstimate(
            flops=2 * total * width * packed,
            transcendentals=total * channels,
            bytes_accessed=2 * width * packed,
        ),
        compiler_params=pltpu.CompilerParams(vmem_limit_bytes=24 * MEBI),
        name="glu_conv",
    )(spot, taps, *[blocks[d] for d in range(nt)], own, *pieces.values())


def out_product(spot, sizes, conv, sums, gain, all_channels, own, pieces):
    ng, nf, nt = sizes
    total, channels = conv.shape
    rows = total // nt
    depth, cols = own.shape
    share = depth // ng
    keys = list(pieces)

    def run(spot_ref, conv_ref, gain_ref, *refs):
        sum_refs, refs = refs[: len(sums)], refs[len(sums) :]
        own_ref, refs = refs[0], refs[1:]
        piece_refs, refs = refs[: len(keys)], refs[len(keys) :]
        out_refs, refs = refs[:nt], refs[nt:]
        weight, mixed, sems = refs
        group, slab, member = spot_ref[0], spot_ref[1], spot_ref[2]
        pairs = [(own_ref, weight.at[slab])]
        for (d, e), ref in zip(keys, piece_refs):
            pairs.append((ref, weight.at[slab ^ d, aligned(group ^ e, share)]))
        copies = start_copies(pairs, sems)
        sums_all = sum(ref[...] for ref in sum_refs) * (1.0 / all_channels)
        row = lax.broadcasted_iota(jnp.int32, (total, total), 0)
        column = lax.broadcasted_iota(jnp.int32, (total, total), 1)

        def upright(line):
            return jnp.sum(jnp.where(row == column, line, 0.0), axis=1, keepdims=True)

        chan_mean = upright(sums_all[0:1, :])
        chan_var = upright(sums_all[8:9, :]) - chan_mean * chan_mean
        scaled = (conv_ref[...] - chan_mean) * lax.rsqrt(chan_var + chan_epsilon) * gain_ref[...]
        activated = (scaled * jax.nn.sigmoid(scaled)).astype(BF16)
        for copy in copies:
            copy.wait()
        for s in range(nf):
            mixed[:, s * cols : (s + 1) * cols] = product(activated, weight[s]).astype(BF16)
        targets = [(mixed.at[aligned(member ^ d, rows)], out_refs[d]) for d in range(nt)]
        for copy in start_copies(targets, sems):
            copy.wait()

    return pl.pallas_call(
        run,
        in_specs=[SMEM, VMEM, VMEM] + [VMEM] * len(sums) + [HBM] * (1 + len(keys)),
        out_specs=[HBM] * nt,
        out_shape=[jax.ShapeDtypeStruct((rows, nf * cols), BF16)] * nt,
        scratch_shapes=[
            pltpu.VMEM((nf, depth, cols), BF16),
            pltpu.VMEM((total, nf * cols), BF16),
            pltpu.SemaphoreType.DMA((max(nt, 1 + len(keys)),)),
        ],
        cost_estimate=pl.CostEstimate(
            flops=2 * total * channels * nf * cols,
            transcendentals=total * channels,
            bytes_accessed=2 * channels * nf * cols,
        ),
        compiler_params=pltpu.CompilerParams(vmem_limit_bytes=24 * MEBI),
        name="out_product",
    )(spot, conv, gain, *sums, own, *pieces.values())


def ffn_chunk(spot, sizes, blocks, up_own, up_pieces, taps, down_own, down_pieces):
    ng, nf, nt = sizes
    rows, width = blocks[0].shape
    total = nt * rows
    depth, packed = up_own.shape
    units, cols = down_own.shape
    up_share, down_share = depth // ng, units // ng
    whole = units // LANES * LANES
    rest = units - whole
    keys = list(up_pieces)
    wide = 2 * LANES

    def run(spot_ref, taps_ref, *refs):
        block_refs, refs = refs[:nt], refs[nt:]
        up_own_ref, down_own_ref, refs = refs[0], refs[1], refs[2:]
        up_refs, refs = refs[: len(keys)], refs[len(keys) :]
        down_refs, refs = refs[: len(keys)], refs[len(keys) :]
        out_refs, refs = refs[:nt], refs[nt:]
        gathered, up, down, hidden, mixed, sems = refs
        group, slab, member = spot_ref[0], spot_ref[1], spot_ref[2]
        pairs = [(block_refs[d], gathered.at[aligned(member ^ d, rows)]) for d in range(nt)]
        pairs.append((up_own_ref, up.at[aligned(slab, depth)]))
        for (d, e), ref in zip(keys, up_refs):
            place = (slab ^ d) * ng + (group ^ e)
            pairs.append((ref, up.at[aligned(place, up_share)]))
        copies = start_copies(pairs, sems)
        late = [(down_own_ref, down.at[slab])]
        for (d, e), ref in zip(keys, down_refs):
            late.append((ref, down.at[slab ^ d, aligned(group ^ e, down_share)]))
        late = start_copies(late, sems, len(pairs))
        for copy in copies:
            copy.wait()

        def conv(column, size):
            raw = product(gathered[...], up[:, column : column + size])
            raw = raw.astype(BF16).astype(F32)
            place = lax.broadcasted_iota(jnp.int32, raw.shape, 0) % LEN
            span = taps_ref.shape[0]
            result = raw * taps_ref[span - 1 : span, column : column + size]
            for back in range(1, span):
                moved = jnp.where(place >= back, pltpu.roll(raw, back, 0), 0.0)
                tap = taps_ref[span - 1 - back : span - back, column : column + size]
                result = result + moved * tap
            return result

        def gelu(v):
            return 0.5 * v * (1.0 + jnp.tanh((2.0 / jnp.pi) ** 0.5 * (v + 0.044715 * v * v * v)))

        for column in range(0, whole, wide):
            size = min(wide, whole - column)
            gate, val = conv(column, size), conv(whole + column, size)
            hidden[:, column : column + size] = (gelu(gate) * val).astype(BF16)
        if rest:
            both = conv(2 * whole, LANES)
            lane = lax.broadcasted_iota(jnp.int32, both.shape, 1)
            gated = gelu(both) * pltpu.roll(both, LANES - rest, 1)
            hidden[:, whole:] = jnp.where(lane < rest, gated, 0.0).astype(BF16)
        for copy in late:
            copy.wait()
        for s in range(nf):
            columns = slice(s * cols, (s + 1) * cols)
            mixed[:, columns] = product(hidden[:, :units], down[s]).astype(BF16)
        targets = [(mixed.at[aligned(member ^ d, rows)], out_refs[d]) for d in range(nt)]
        for copy in start_copies(targets, sems):
            copy.wait()

    flops = 2 * total * width * packed + 2 * total * units * nf * cols
    return pl.pallas_call(
        run,
        in_specs=[SMEM, VMEM] + [HBM] * (nt + 2 + 2 * len(keys)),
        out_specs=[HBM] * nt,
        out_shape=[jax.ShapeDtypeStruct((rows, nf * cols), BF16)] * nt,
        scratch_shapes=[
            pltpu.VMEM((total, width), BF16),
            pltpu.VMEM((nf * depth, packed), BF16),
            pltpu.VMEM((nf, units, cols), BF16),
            pltpu.VMEM((total, whole + (LANES if rest else 0)), BF16),
            pltpu.VMEM((total, nf * cols), BF16),
            pltpu.SemaphoreType.DMA((nt + 2 + 2 * len(keys),)),
        ],
        cost_estimate=pl.CostEstimate(
            flops=flops, transcendentals=total * units, bytes_accessed=2 * width * packed
        ),
        compiler_params=pltpu.CompilerParams(vmem_limit_bytes=24 * MEBI),
        name="ffn_chunk",
    )(
        spot,
        taps,
        *[blocks[d] for d in range(nt)],
        up_own,
        down_own,
        *up_pieces.values(),
        *down_pieces.values(),
    )


def pair_order(nf):
    return sorted(range(1, nf), key=lambda d: (d != 1, -d))


def exchange_shards(sizes):
    ng, nf, nt = sizes
    far = pair_order(nf)

    def shards(
        tokens,
        mix_gain,
        val_weight,
        gate_weight,
        conv_taps,
        chan_gain,
        out_weight,
        mix_post_gain,
        ffn_gain,
        up_gate_weight,
        up_val_weight,
        ffn_taps,
        down_weight,
        ffn_post_gain,
    ):
        group, slab, member = (lax.axis_index(a) for a in ("grp", "fs", "tp"))
        spot = jnp.stack([group, slab, member]).astype(jnp.int32)

        def fetch(piece_for):
            pieces = {}
            for d in far:
                pieces[d, 0] = swap(piece_for(d), "fs", nf, d)
            for d in far:
                for e in range(1, ng):
                    pieces[d, e] = swap(pieces[d, 0], "grp", ng, e)
            return pieces

        def share(array):
            return pick(array.reshape(ng, array.shape[0] // ng, array.shape[1]), group)

        local_ch = val_weight.shape[1]
        glu_own = jnp.concatenate([val_weight, gate_weight], axis=1)
        glu_share = jnp.concatenate([share(val_weight), share(gate_weight)], axis=1)
        glu_pieces = fetch(lambda d: glu_share)
        out_share = share(out_weight)
        out_pieces = fetch(lambda d: out_share)

        local_ff = up_gate_weight.shape[1]
        units = local_ff // nf
        whole = units // LANES * LANES

        def pack(gate, val):
            def block(s):
                a, b, c = s * units, s * units + whole, (s + 1) * units
                cut = [gate[..., a:b], val[..., a:b], gate[..., b:c], val[..., b:c]]
                return jnp.concatenate(cut, axis=-1)

            return jnp.stack([block(s) for s in range(nf)])

        up_blocks = pack(up_gate_weight, up_val_weight)
        up_own = pick(up_blocks, slab)
        up_halves = up_blocks.reshape(nf, ng, up_blocks.shape[1] // ng, 2 * units)
        up_pieces = fetch(lambda d: pick(up_halves, slab ^ d, group))
        down_own = pick(down_weight.reshape(nf, units, down_weight.shape[1]), slab)
        down_halves = down_weight.reshape(nf, ng, units // ng, down_weight.shape[1])
        down_pieces = fetch(lambda d: pick(down_halves, slab ^ d, group))
        own_taps = lax.dynamic_slice_in_dim(ffn_taps, member * local_ff, local_ff, 2)
        own_taps = pick(pack(own_taps[0], own_taps[1]), slab).astype(F32)

        def scaled(values, gain):
            mean = jnp.mean(values * values, axis=-1, keepdims=True)
            return values * lax.rsqrt(mean + norm_epsilon) * gain

        mix_taps = lax.dynamic_slice_in_dim(conv_taps, member * local_ch, local_ch, 1)
        own_gain = lax.dynamic_slice_in_dim(chan_gain[None], member * local_ch, local_ch, 1)
        (normed,) = row_kernel(lambda t, g: (scaled(t, g),), [tokens, mix_gain[None]], 1)
        row_blocks = gather_blocks(normed, "tp", nt)
        conv, sums = glu_conv(spot, sizes, row_blocks, glu_own, glu_pieces, mix_taps.astype(F32))
        all_sums = [sums] + [swap(sums, "tp", nt, d) for d in range(1, nt)]
        mixed = out_product(
            spot,
            sizes,
            conv,
            all_sums,
            own_gain.astype(F32),
            chan_gain.shape[0],
            out_weight,
            out_pieces,
        )
        terms = scatter_blocks(dict(enumerate(mixed)), "tp", nt)

        def residual_rows(t, post, gain, *parts):
            result = (t + scaled(sum(parts), post)).astype(BF16).astype(F32)
            return result, scaled(result, gain)

        residual, acted = row_kernel(
            residual_rows, [tokens, mix_post_gain[None], ffn_gain[None], *terms], 2
        )

        last = []
        for d in [0, *far]:
            block = swap(acted, "fs", nf, d) if d else acted
            blocks = gather_blocks(block, "tp", nt)
            parts = ffn_chunk(
                spot, sizes, blocks, up_own, up_pieces, own_taps, down_own, down_pieces
            )
            terms = scatter_blocks(dict(enumerate(parts)), "tp", nt)
            if d:
                terms = [swap(add_terms(terms), "fs", nf, d)]
            last += terms
        (result,) = row_kernel(
            lambda r, gain, *parts: (r + scaled(sum(parts), gain),),
            [residual, ffn_post_gain[None], *last],
            1,
        )
        return result

    return shards


def gather_shards(
    tokens,
    mix_gain,
    val_weight,
    gate_weight,
    conv_taps,
    chan_gain,
    out_weight,
    mix_post_gain,
    ffn_gain,
    up_gate_weight,
    up_val_weight,
    ffn_taps,
    down_weight,
    ffn_post_gain,
):
    member = lax.axis_index("tp")
    normed_own = rms_scale(tokens.astype(jnp.float32), mix_gain).astype(jnp.bfloat16)
    normed = lax.all_gather(normed_own, "tp", axis=0, tiled=True)
    local_ch = val_weight.shape[1]
    values = product(normed, lax.all_gather(val_weight, "fs", axis=0, tiled=True))
    gate_sums = product(normed, lax.all_gather(gate_weight, "fs", axis=0, tiled=True))
    glu_out = (values * jax.nn.sigmoid(gate_sums)).astype(jnp.bfloat16)
    own_taps = lax.dynamic_slice_in_dim(conv_taps, member * local_ch, local_ch, 1)
    conv_out = depthwise(glu_out, own_taps)
    totals, squares = lax.psum(
        (jnp.sum(conv_out, axis=1), jnp.sum(conv_out * conv_out, axis=1)), "tp"
    )
    all_channels = chan_gain.shape[0]
    chan_mean = totals[:, None] / all_channels
    chan_var = squares[:, None] / all_channels - chan_mean * chan_mean
    own_gain = lax.dynamic_slice_in_dim(chan_gain, member * local_ch, local_ch, 0)
    scaled = (conv_out - chan_mean) * lax.rsqrt(chan_var + chan_epsilon)
    activated = jax.nn.silu(scaled * own_gain.astype(jnp.float32)).astype(jnp.bfloat16)
    out_full = lax.all_gather(out_weight, "fs", axis=1, tiled=True)
    mixed_sum = lax.psum_scatter(
        product(activated, out_full).astype(jnp.bfloat16), "tp", scatter_dimension=0, tiled=True
    ).astype(jnp.float32)
    residual = tokens.astype(jnp.float32) + rms_scale(mixed_sum, mix_post_gain)
    residual = residual.astype(jnp.bfloat16)
    normed_share = rms_scale(residual.astype(jnp.float32), ffn_gain).astype(jnp.bfloat16)
    normed_ffn = lax.all_gather(normed_share, "tp", axis=0, tiled=True)
    local_ff = up_gate_weight.shape[1]
    own_ffn_taps = lax.dynamic_slice_in_dim(ffn_taps, member * local_ff, local_ff, 2)
    gate_full = lax.all_gather(up_gate_weight, "fs", axis=0, tiled=True)
    val_full = lax.all_gather(up_val_weight, "fs", axis=0, tiled=True)
    up_gate = product(normed_ffn, gate_full).astype(jnp.bfloat16)
    up_val = product(normed_ffn, val_full).astype(jnp.bfloat16)
    gate_conv = depthwise(up_gate, own_ffn_taps[0])
    val_conv = depthwise(up_val, own_ffn_taps[1])
    hidden = (jax.nn.gelu(gate_conv, approximate=True) * val_conv).astype(jnp.bfloat16)
    down_full = lax.all_gather(down_weight, "fs", axis=1, tiled=True)
    ffn_sum = lax.psum_scatter(
        product(hidden, down_full).astype(jnp.bfloat16), "tp", scatter_dimension=0, tiled=True
    ).astype(jnp.float32)
    return (residual.astype(jnp.float32) + rms_scale(ffn_sum, ffn_post_gain)).astype(jnp.bfloat16)


def solution(mesh):
    sizes = tuple(mesh.shape[a] for a in ("grp", "fs", "tp"))
    specs = (
        P(("grp", "fs", "tp"), None),
        P(),
        P("fs", "tp"),
        P("fs", "tp"),
        P(),
        P(),
        P("tp", "fs"),
        P(),
        P(),
        P("fs", "tp"),
        P("fs", "tp"),
        P(),
        P("tp", "fs"),
        P(),
    )
    powers = all(size & (size - 1) == 0 for size in sizes)
    exchange = powers and sizes[1] * sizes[2] <= 16

    def run(*args):
        units = args[9].shape[1] // (sizes[1] * sizes[2])
        cuts = units % LANES in (0, LANES // 2) and units % (16 * sizes[0]) == 0
        shards = exchange_shards(sizes) if exchange and cuts else gather_shards
        return jax.shard_map(
            shards,
            mesh=mesh,
            in_specs=specs,
            out_specs=P(("grp", "fs", "tp"), None),
            check_vma=False,
        )(*args)

    return run
```

profile of v0, /device:TPU:0, one launch (start us, length us, event | category | flops | bytes accessed | tf_op | source)
XLA Modules:
  0.0 257.4 jit_solution(17581565311524891123)
XLA Ops:
  1.8 3.1 %collective-permute-start.3 = (bf16[256,512]{1,0:T(8,128)(2,1)}, bf16[256,512]{1,0:T(8,128)(2,1)S(1)}, u32[]{:S(2)}, u32[]{:S(2)}) collective-permute-start(bf16[256,512]{1,0:T(8,128)(2,1)} %pad_maximum_fusion.6), channel_id=1, source_target_pairs={{0,4},{4,0},{8,12},{12,8},{1,5},{5,1},{9,13},{13,9},{2,6},{6,2},{1... | collective-permute-start | bytes 786440 | tf_op jit(solution)/shard_map/ppermute | solution.py:40
  4.9 2.5 collective-permute-start.4
  10.8 2.5 collective-permute-start.13
  21.7 4.2 %collective-permute-done.12.refs_5_ = bf16[128,512]{1,0:T(8,128)(2,1)S(1)} collective-permute-done((bf16[128,512]{1,0:T(8,128)(2,1)}, bf16[128,512]{1,0:T(8,128)(2,1)S(1)}, u32[]{:S(2)}, u32[]{:S(2)}) %collective-permute-start.12) | collective-permute-done | bytes 131104 | tf_op jit(solution)/shard_map/ppermute | solution.py:40
  26.0 3.4 %collective-permute-start.14 = (bf16[128,512]{1,0:T(8,128)(2,1)}, bf16[128,512]{1,0:T(8,128)(2,1)S(1)}, u32[]{:S(2)}, u32[]{:S(2)}) collective-permute-start(bf16[128,512]{1,0:T(8,128)(2,1)} %dynamic-slice_bitcast_fusion.7), channel_id=1, source_target_pairs={{0,8},{4,12},{8,0},{12,4},{1,9},{5,13},{9,1},{13,5},{2,10},{6,14},... | collective-permute-start | bytes 393224 | tf_op jit(solution)/shard_map/ppermute | solution.py:40
  33.4 8.4 %collective-permute-done.14.refs_7_ = bf16[128,512]{1,0:T(8,128)(2,1)S(1)} collective-permute-done((bf16[128,512]{1,0:T(8,128)(2,1)}, bf16[128,512]{1,0:T(8,128)(2,1)S(1)}, u32[]{:S(2)}, u32[]{:S(2)}) %collective-permute-start.14) | collective-permute-done | bytes 131104 | tf_op jit(solution)/shard_map/ppermute | solution.py:40
  49.2 3.0 %collective-permute-done.6.refs_8_ = bf16[256,512]{1,0:T(8,128)(2,1)S(1)} collective-permute-done((bf16[256,512]{1,0:T(8,128)(2,1)S(1)}, bf16[256,512]{1,0:T(8,128)(2,1)S(1)}, u32[]{:S(2)}, u32[]{:S(2)}) %collective-permute-start.6) | collective-permute-done | bytes 262176 | tf_op jit(solution)/shard_map/ppermute | solution.py:40
  53.7 4.1 %collective-permute-done.7.refs_9_ = bf16[256,512]{1,0:T(8,128)(2,1)S(1)} collective-permute-done((bf16[256,512]{1,0:T(8,128)(2,1)S(1)}, bf16[256,512]{1,0:T(8,128)(2,1)S(1)}, u32[]{:S(2)}, u32[]{:S(2)}) %collective-permute-start.7) | collective-permute-done | bytes 262176 | tf_op jit(solution)/shard_map/ppermute | solution.py:40
  59.3 4.1 %collective-permute-done.8.refs_10_ = bf16[256,512]{1,0:T(8,128)(2,1)S(1)} collective-permute-done((bf16[256,512]{1,0:T(8,128)(2,1)S(1)}, bf16[256,512]{1,0:T(8,128)(2,1)S(1)}, u32[]{:S(2)}, u32[]{:S(2)}) %collective-permute-start.8) | collective-permute-done | bytes 262176 | tf_op jit(solution)/shard_map/ppermute | solution.py:40
  63.4 4.7 %glu_conv.1 = (f32[320,256]{1,0:T(8,128)S(1)}, f32[16,320]{1,0:T(8,128)S(1)}) custom-call(s32[3]{0:T(128)S(1)} %pad_add_fusion.spot_ref, f32[31,256]{1,0:T(8,128)S(1)} %dynamic-slice_convert_fusion.taps_ref, bf16[80,2048]{1,0:T(8,128)(2,1)S(1)} %shard_map.136.refs_0_, bf16[80,2048]{1,0:T(8,128)(2,1)S(1)} %collective-permute-done.refs_1_, ...), custom_call_target="tpu_custom_call" | custom-call | flops 671088640 | bytes 2097152 | tf_op jit(solution)/shard_map/glu_conv/pallas_call | solution.py:166
  73.1 2.6 %collective-permute-start.31 = (bf16[160,512]{1,0:T(8,128)(2,1)S(1)}, bf16[160,512]{1,0:T(8,128)(2,1)S(1)}, u32[]{:S(2)}, u32[]{:S(2)}) collective-permute-start(bf16[160,512]{1,0:T(8,128)(2,1)S(1)} %get-tuple-element.57), channel_id=1, source_target_pairs={{0,12},{4,8},{8,4},{12,0},{1,13},{5,9},{9,5},{13,1},{2,14},{6,10},... | collective-permute-start | bytes 491528 | tf_op jit(solution)/shard_map/ppermute | solution.py:40
  75.7 2.9 %out_product.1 = (bf16[80,2048]{1,0:T(8,128)(2,1)S(1)}, bf16[80,2048]{1,0:T(8,128)(2,1)S(1)}, bf16[80,2048]{1,0:T(8,128)(2,1)S(1)}, bf16[80,2048]{1,0:T(8,128)(2,1)S(1)}) custom-call(s32[3]{0:T(128)S(1)} %pad_add_fusion.spot_ref, f32[320,256]{1,0:T(8,128)S(1)} %get-tuple-element.29.conv_ref, f32[1,256]{1,0:T(1,128)S(1)} %bitcast.55, ...), custom_call_target="tpu_custom_call" | custom-call | flops 335544320 | bytes 1048576 | tf_op jit(solution)/shard_map/out_product/pallas_call | solution.py:228
  80.5 10.7 %collective-permute-done.30.refs_12_ = bf16[160,512]{1,0:T(8,128)(2,1)S(1)} collective-permute-done((bf16[160,512]{1,0:T(8,128)(2,1)S(1)}, bf16[160,512]{1,0:T(8,128)(2,1)S(1)}, u32[]{:S(2)}, u32[]{:S(2)}) %collective-permute-start.30) | collective-permute-done | bytes 163872 | tf_op jit(solution)/shard_map/ppermute | solution.py:40
  92.8 2.6 %collective-permute-start.25 = (bf16[256,640]{1,0:T(8,128)(2,1)S(1)}, bf16[256,640]{1,0:T(8,128)(2,1)S(1)}, u32[]{:S(2)}, u32[]{:S(2)}) collective-permute-start(bf16[256,640]{1,0:T(8,128)(2,1)S(1)} %get-tuple-element.54), channel_id=1, source_target_pairs={{0,12},{4,8},{8,4},{12,0},{1,13},{5,9},{9,5},{13,1},{2,14},{6,10},... | collective-permute-start | bytes 983048 | tf_op jit(solution)/shard_map/ppermute | solution.py:40
  106.8 14.6 %collective-permute-done.26.refs_8_ = bf16[256,640]{1,0:T(8,128)(2,1)S(1)} collective-permute-done((bf16[256,640]{1,0:T(8,128)(2,1)S(1)}, bf16[256,640]{1,0:T(8,128)(2,1)S(1)}, u32[]{:S(2)}, u32[]{:S(2)}) %collective-permute-start.26) | collective-permute-done | bytes 327712 | tf_op jit(solution)/shard_map/ppermute | solution.py:40
  123.5 2.6 %collective-permute-start.47 = (bf16[80,2048]{1,0:T(8,128)(2,1)S(1)}, bf16[80,2048]{1,0:T(8,128)(2,1)S(1)}, u32[]{:S(2)}, u32[]{:S(2)}) collective-permute-start(bf16[80,2048]{1,0:T(8,128)(2,1)S(1)} %get-tuple-element.36.refs_0_), channel_id=1, source_target_pairs={{0,12},{4,8},{8,4},{12,0},{1,13},{5,9},{9,5},{13,1},{2,14},{6,10},... | collective-permute-start | bytes 983048 | tf_op jit(solution)/shard_map/ppermute | solution.py:40
  128.6 3.4 %collective-permute-done.28.refs_10_ = bf16[256,640]{1,0:T(8,128)(2,1)S(1)} collective-permute-done((bf16[256,640]{1,0:T(8,128)(2,1)S(1)}, bf16[256,640]{1,0:T(8,128)(2,1)S(1)}, u32[]{:S(2)}, u32[]{:S(2)}) %collective-permute-start.28) | collective-permute-done | bytes 327712 | tf_op jit(solution)/shard_map/ppermute | solution.py:40
  132.4 3.6 %collective-permute-done.29.refs_11_ = bf16[256,640]{1,0:T(8,128)(2,1)S(1)} collective-permute-done((bf16[256,640]{1,0:T(8,128)(2,1)S(1)}, bf16[256,640]{1,0:T(8,128)(2,1)S(1)}, u32[]{:S(2)}, u32[]{:S(2)}) %collective-permute-start.29) | collective-permute-done | bytes 327712 | tf_op jit(solution)/shard_map/ppermute | solution.py:40
  137.0 8.6 %collective-permute-done.55.refs_0_ = bf16[80,2048]{1,0:T(8,128)(2,1)} collective-permute-done((bf16[80,2048]{1,0:T(8,128)(2,1)S(1)}, bf16[80,2048]{1,0:T(8,128)(2,1)}, u32[]{:S(2)}, u32[]{:S(2)}) %collective-permute-start.55) | collective-permute-done | bytes 327712 | tf_op jit(solution)/shard_map/ppermute | solution.py:40
  149.0 7.4 %collective-permute-done.57.refs_2_ = bf16[80,2048]{1,0:T(8,128)(2,1)S(1)} collective-permute-done((bf16[80,2048]{1,0:T(8,128)(2,1)}, bf16[80,2048]{1,0:T(8,128)(2,1)S(1)}, u32[]{:S(2)}, u32[]{:S(2)}) %collective-permute-start.57) | collective-permute-done | bytes 327712 | tf_op jit(solution)/shard_map/ppermute | solution.py:40
  157.0 6.4 %collective-permute-done.49.refs_2_ = bf16[80,2048]{1,0:T(8,128)(2,1)S(1)} collective-permute-done((bf16[80,2048]{1,0:T(8,128)(2,1)S(1)}, bf16[80,2048]{1,0:T(8,128)(2,1)S(1)}, u32[]{:S(2)}, u32[]{:S(2)}) %collective-permute-start.49) | collective-permute-done | bytes 327712 | tf_op jit(solution)/shard_map/ppermute | solution.py:40
  163.4 5.9 %collective-permute-done.41.refs_2_ = bf16[80,2048]{1,0:T(8,128)(2,1)S(1)} collective-permute-done((bf16[80,2048]{1,0:T(8,128)(2,1)S(1)}, bf16[80,2048]{1,0:T(8,128)(2,1)S(1)}, u32[]{:S(2)}, u32[]{:S(2)}) %collective-permute-start.41) | collective-permute-done | bytes 327712 | tf_op jit(solution)/shard_map/ppermute | solution.py:40
  169.9 7.3 %ffn_chunk.4 = (bf16[80,2048]{1,0:T(8,128)(2,1)S(1)}, bf16[80,2048]{1,0:T(8,128)(2,1)S(1)}, bf16[80,2048]{1,0:T(8,128)(2,1)S(1)}, bf16[80,2048]{1,0:T(8,128)(2,1)S(1)}) custom-call(s32[3]{0:T(128)S(1)} %pad_add_fusion.spot_ref, f32[3,640]{1,0:T(4,128)S(1)} %bitcast_convert_fusion.taps_ref, bf16[80,2048]{1,0:T(8,128)(2,1)S(1)} %get-tuple-element.36.refs_0_, ...), custom_call_target="tpu_custom_call" | custom-call | flops 1258291200 | bytes 2621440 | tf_op jit(solution)/shard_map/ffn_chunk/pallas_call | solution.py:315
  177.3 7.2 %ffn_chunk.7 = (bf16[80,2048]{1,0:T(8,128)(2,1)S(1)}, bf16[80,2048]{1,0:T(8,128)(2,1)S(1)}, bf16[80,2048]{1,0:T(8,128)(2,1)S(1)}, bf16[80,2048]{1,0:T(8,128)(2,1)S(1)}) custom-call(s32[3]{0:T(128)S(1)} %pad_add_fusion.spot_ref, f32[3,640]{1,0:T(4,128)S(1)} %bitcast_convert_fusion.taps_ref, bf16[80,2048]{1,0:T(8,128)(2,1)} %collective-permute-done.55.refs_0_, ...), custom_call_target="tpu_custom_call" | custom-call | flops 1258291200 | bytes 2621440 | tf_op jit(solution)/shard_map/ffn_chunk/pallas_call | solution.py:315
  185.1 7.5 %ffn_chunk.6 = (bf16[80,2048]{1,0:T(8,128)(2,1)S(1)}, bf16[80,2048]{1,0:T(8,128)(2,1)S(1)}, bf16[80,2048]{1,0:T(8,128)(2,1)S(1)}, bf16[80,2048]{1,0:T(8,128)(2,1)S(1)}) custom-call(s32[3]{0:T(128)S(1)} %pad_add_fusion.spot_ref, f32[3,640]{1,0:T(4,128)S(1)} %bitcast_convert_fusion.taps_ref, bf16[80,2048]{1,0:T(8,128)(2,1)S(1)} %collective-permute-done.47.refs_0_, ...), custom_call_target="tpu_custom_call" | custom-call | flops 1258291200 | bytes 2621440 | tf_op jit(solution)/shard_map/ffn_chunk/pallas_call | solution.py:315
  193.1 7.3 %ffn_chunk.5 = (bf16[80,2048]{1,0:T(8,128)(2,1)S(1)}, bf16[80,2048]{1,0:T(8,128)(2,1)S(1)}, bf16[80,2048]{1,0:T(8,128)(2,1)S(1)}, bf16[80,2048]{1,0:T(8,128)(2,1)S(1)}) custom-call(s32[3]{0:T(128)S(1)} %pad_add_fusion.spot_ref, f32[3,640]{1,0:T(4,128)S(1)} %bitcast_convert_fusion.taps_ref, bf16[80,2048]{1,0:T(8,128)(2,1)S(1)} %collective-permute-done.39.refs_0_, ...), custom_call_target="tpu_custom_call" | custom-call | flops 1258291200 | bytes 2621440 | tf_op jit(solution)/shard_map/ffn_chunk/pallas_call | solution.py:315
  204.9 8.4 %collective-permute-done.61 = bf16[80,2048]{1,0:T(8,128)(2,1)S(1)} collective-permute-done((bf16[80,2048]{1,0:T(8,128)(2,1)S(1)}, bf16[80,2048]{1,0:T(8,128)(2,1)S(1)}, u32[]{:S(2)}, u32[]{:S(2)}) %collective-permute-start.61) | collective-permute-done | bytes 327712 | tf_op jit(solution)/shard_map/ppermute | solution.py:40
  215.5 11.8 %collective-permute-done.53 = bf16[80,2048]{1,0:T(8,128)(2,1)S(1)} collective-permute-done((bf16[80,2048]{1,0:T(8,128)(2,1)S(1)}, bf16[80,2048]{1,0:T(8,128)(2,1)S(1)}, u32[]{:S(2)}, u32[]{:S(2)}) %collective-permute-start.53) | collective-permute-done | bytes 327712 | tf_op jit(solution)/shard_map/ppermute | solution.py:40
  228.0 2.7 %collective-permute-start.54 = (bf16[80,2048]{1,0:T(8,128)(2,1)S(1)}, bf16[80,2048]{1,0:T(8,128)(2,1)S(1)}, u32[]{:S(2)}, u32[]{:S(2)}) collective-permute-start(bf16[80,2048]{1,0:T(8,128)(2,1)S(1)} %add_convert_fusion.2), channel_id=1, source_target_pairs={{0,12},{4,8},{8,4},{12,0},{1,13},{5,9},{9,5},{13,1},{2,14},{6,10},... | collective-permute-start | bytes 983048 | tf_op jit(solution)/shard_map/ppermute | solution.py:40
  230.6 3.0 %collective-permute-done.45 = bf16[80,2048]{1,0:T(8,128)(2,1)S(1)} collective-permute-done((bf16[80,2048]{1,0:T(8,128)(2,1)S(1)}, bf16[80,2048]{1,0:T(8,128)(2,1)S(1)}, u32[]{:S(2)}, u32[]{:S(2)}) %collective-permute-start.45) | collective-permute-done | bytes 327712 | tf_op jit(solution)/shard_map/ppermute | solution.py:40
  234.7 16.3 %collective-permute-done.62.refs_7_ = bf16[80,2048]{1,0:T(8,128)(2,1)S(1)} collective-permute-done((bf16[80,2048]{1,0:T(8,128)(2,1)S(1)}, bf16[80,2048]{1,0:T(8,128)(2,1)S(1)}, u32[]{:S(2)}, u32[]{:S(2)}) %collective-permute-start.62) | collective-permute-done | bytes 327712 | tf_op jit(solution)/shard_map/ppermute | solution.py:40
  251.0 5.1 %collective-permute-done.46.refs_5_ = bf16[80,2048]{1,0:T(8,128)(2,1)S(1)} collective-permute-done((bf16[80,2048]{1,0:T(8,128)(2,1)S(1)}, bf16[80,2048]{1,0:T(8,128)(2,1)S(1)}, u32[]{:S(2)}, u32[]{:S(2)}) %collective-permute-start.46) | collective-permute-done | bytes 327712 | tf_op jit(solution)/shard_map/ppermute | solution.py:40
  (188 shorter events, 69.2 us)
Async XLA Ops:
  1.8 41.1 %collective-permute-start.3 = (bf16[256,512]{1,0:T(8,128)(2,1)}, bf16[256,512]{1,0:T(8,128)(2,1)S(1)}, u32[]{:S(2)}, u32[]{:S(2)}) collective-permute-start(bf16[256,512]{1,0:T(8,128)(2,1)} %pad_maximum_fusion.6), channel_id=1, source_target_pairs={{0,4},{4,0},{8,12},{12,8},{1,5},{5,1},{9,13},{13,9},{2,6},{6,2},{1... | collective-permute-start | bytes 786440 | tf_op jit(solution)/shard_map/ppermute | solution.py:40
  4.9 39.7 %collective-permute-start.4 = (bf16[256,512]{1,0:T(8,128)(2,1)}, bf16[256,512]{1,0:T(8,128)(2,1)S(1)}, u32[]{:S(2)}, u32[]{:S(2)}) collective-permute-start(bf16[256,512]{1,0:T(8,128)(2,1)} %pad_maximum_fusion.6), channel_id=1, source_target_pairs={{0,12},{4,8},{8,4},{12,0},{1,13},{5,9},{9,5},{13,1},{2,14},{6,10},... | collective-permute-start | bytes 786440 | tf_op jit(solution)/shard_map/ppermute | solution.py:40
  7.3 37.7 %collective-permute-start.5 = (bf16[256,512]{1,0:T(8,128)(2,1)}, bf16[256,512]{1,0:T(8,128)(2,1)S(1)}, u32[]{:S(2)}, u32[]{:S(2)}) collective-permute-start(bf16[256,512]{1,0:T(8,128)(2,1)} %pad_maximum_fusion.6), channel_id=1, source_target_pairs={{0,8},{4,12},{8,0},{12,4},{1,9},{5,13},{9,1},{13,5},{2,10},{6,14},... | collective-permute-start | bytes 786440 | tf_op jit(solution)/shard_map/ppermute | solution.py:40
  10.8 20.9 %collective-permute-start.13 = (bf16[128,512]{1,0:T(8,128)(2,1)}, bf16[128,512]{1,0:T(8,128)(2,1)S(1)}, u32[]{:S(2)}, u32[]{:S(2)}) collective-permute-start(bf16[128,512]{1,0:T(8,128)(2,1)} %dynamic-slice_bitcast_fusion.7), channel_id=1, source_target_pairs={{0,12},{4,8},{8,4},{12,0},{1,13},{5,9},{9,5},{13,1},{2,14},{6,10},... | collective-permute-start | bytes 393224 | tf_op jit(solution)/shard_map/ppermute | solution.py:40
  48.6 21.1 %collective-permute-start.15 = (bf16[128,512]{1,0:T(8,128)(2,1)S(1)}, bf16[128,512]{1,0:T(8,128)(2,1)S(1)}, u32[]{:S(2)}, u32[]{:S(2)}) collective-permute-start(bf16[128,512]{1,0:T(8,128)(2,1)S(1)} %collective-permute-done.12.refs_5_), channel_id=1, source_target_pairs={{0,16},{16,0},{1,17},{17,1},{2,18},{18,2},{3,19},{19,3},{4,20},{20... | collective-permute-start | bytes 393224 | tf_op jit(solution)/shard_map/ppermute | solution.py:40
  52.2 18.9 %collective-permute-start.16 = (bf16[128,512]{1,0:T(8,128)(2,1)S(1)}, bf16[128,512]{1,0:T(8,128)(2,1)S(1)}, u32[]{:S(2)}, u32[]{:S(2)}) collective-permute-start(bf16[128,512]{1,0:T(8,128)(2,1)S(1)} %collective-permute-done.13.refs_6_), channel_id=1, source_target_pairs={{0,16},{16,0},{1,17},{17,1},{2,18},{18,2},{3,19},{19,3},{4,20},{20... | collective-permute-start | bytes 393224 | tf_op jit(solution)/shard_map/ppermute | solution.py:40
  71.1 24.4 %collective-permute-start.24 = (bf16[256,640]{1,0:T(8,128)(2,1)S(1)}, bf16[256,640]{1,0:T(8,128)(2,1)S(1)}, u32[]{:S(2)}, u32[]{:S(2)}) collective-permute-start(bf16[256,640]{1,0:T(8,128)(2,1)S(1)} %get-tuple-element.55), channel_id=1, source_target_pairs={{0,4},{4,0},{8,12},{12,8},{1,5},{5,1},{9,13},{13,9},{2,6},{6,2},{1... | collective-permute-start | bytes 983048 | tf_op jit(solution)/shard_map/ppermute | solution.py:40
  71.7 19.5 %collective-permute-start.30 = (bf16[160,512]{1,0:T(8,128)(2,1)S(1)}, bf16[160,512]{1,0:T(8,128)(2,1)S(1)}, u32[]{:S(2)}, u32[]{:S(2)}) collective-permute-start(bf16[160,512]{1,0:T(8,128)(2,1)S(1)} %get-tuple-element.58), channel_id=1, source_target_pairs={{0,4},{4,0},{8,12},{12,8},{1,5},{5,1},{9,13},{13,9},{2,6},{6,2},{1... | collective-permute-start | bytes 491528 | tf_op jit(solution)/shard_map/ppermute | solution.py:40
  73.1 19.7 %collective-permute-start.31 = (bf16[160,512]{1,0:T(8,128)(2,1)S(1)}, bf16[160,512]{1,0:T(8,128)(2,1)S(1)}, u32[]{:S(2)}, u32[]{:S(2)}) collective-permute-start(bf16[160,512]{1,0:T(8,128)(2,1)S(1)} %get-tuple-element.57), channel_id=1, source_target_pairs={{0,12},{4,8},{8,4},{12,0},{1,13},{5,9},{9,5},{13,1},{2,14},{6,10},... | collective-permute-start | bytes 491528 | tf_op jit(solution)/shard_map/ppermute | solution.py:40
  75.7 19.7 %collective-permute-start.32 = (bf16[160,512]{1,0:T(8,128)(2,1)S(1)}, bf16[160,512]{1,0:T(8,128)(2,1)S(1)}, u32[]{:S(2)}, u32[]{:S(2)}) collective-permute-start(bf16[160,512]{1,0:T(8,128)(2,1)S(1)} %get-tuple-element.56), channel_id=1, source_target_pairs={{0,8},{4,12},{8,0},{12,4},{1,9},{5,13},{9,1},{13,5},{2,10},{6,14},... | collective-permute-start | bytes 491528 | tf_op jit(solution)/shard_map/ppermute | solution.py:40
  95.4 25.9 %collective-permute-start.26 = (bf16[256,640]{1,0:T(8,128)(2,1)S(1)}, bf16[256,640]{1,0:T(8,128)(2,1)S(1)}, u32[]{:S(2)}, u32[]{:S(2)}) collective-permute-start(bf16[256,640]{1,0:T(8,128)(2,1)S(1)} %get-tuple-element.53), channel_id=1, source_target_pairs={{0,8},{4,12},{8,0},{12,4},{1,9},{5,13},{9,1},{13,5},{2,10},{6,14},... | collective-permute-start | bytes 983048 | tf_op jit(solution)/shard_map/ppermute | solution.py:40
  95.5 27.4 %collective-permute-start.33 = (bf16[160,512]{1,0:T(8,128)(2,1)S(1)}, bf16[160,512]{1,0:T(8,128)(2,1)S(1)}, u32[]{:S(2)}, u32[]{:S(2)}) collective-permute-start(bf16[160,512]{1,0:T(8,128)(2,1)S(1)} %collective-permute-done.30.refs_12_), channel_id=1, source_target_pairs={{0,16},{16,0},{1,17},{17,1},{2,18},{18,2},{3,19},{19,3},{4,20},{20... | collective-permute-start | bytes 491528 | tf_op jit(solution)/shard_map/ppermute | solution.py:40
  97.0 26.3 %collective-permute-start.34 = (bf16[160,512]{1,0:T(8,128)(2,1)S(1)}, bf16[160,512]{1,0:T(8,128)(2,1)S(1)}, u32[]{:S(2)}, u32[]{:S(2)}) collective-permute-start(bf16[160,512]{1,0:T(8,128)(2,1)S(1)} %collective-permute-done.31.refs_13_), channel_id=1, source_target_pairs={{0,16},{16,0},{1,17},{17,1},{2,18},{18,2},{3,19},{19,3},{4,20},{20... | collective-permute-start | bytes 491528 | tf_op jit(solution)/shard_map/ppermute | solution.py:40
  100.0 26.1 %collective-permute-start.27 = (bf16[256,640]{1,0:T(8,128)(2,1)S(1)}, bf16[256,640]{1,0:T(8,128)(2,1)S(1)}, u32[]{:S(2)}, u32[]{:S(2)}) collective-permute-start(bf16[256,640]{1,0:T(8,128)(2,1)S(1)} %collective-permute-done.24.refs_6_), channel_id=1, source_target_pairs={{0,16},{16,0},{1,17},{17,1},{2,18},{18,2},{3,19},{19,3},{4,20},{20... | collective-permute-start | bytes 983048 | tf_op jit(solution)/shard_map/ppermute | solution.py:40
  123.4 22.2 %collective-permute-start.55 = (bf16[80,2048]{1,0:T(8,128)(2,1)S(1)}, bf16[80,2048]{1,0:T(8,128)(2,1)}, u32[]{:S(2)}, u32[]{:S(2)}) collective-permute-start(bf16[80,2048]{1,0:T(8,128)(2,1)S(1)} %get-tuple-element.36.refs_0_), channel_id=1, source_target_pairs={{0,8},{4,12},{8,0},{12,4},{1,9},{5,13},{9,1},{13,5},{2,10},{6,14},... | collective-permute-start | bytes 983048 | tf_op jit(solution)/shard_map/ppermute | solution.py:40
  123.5 22.8 %collective-permute-start.47 = (bf16[80,2048]{1,0:T(8,128)(2,1)S(1)}, bf16[80,2048]{1,0:T(8,128)(2,1)S(1)}, u32[]{:S(2)}, u32[]{:S(2)}) collective-permute-start(bf16[80,2048]{1,0:T(8,128)(2,1)S(1)} %get-tuple-element.36.refs_0_), channel_id=1, source_target_pairs={{0,12},{4,8},{8,4},{12,0},{1,13},{5,9},{9,5},{13,1},{2,14},{6,10},... | collective-permute-start | bytes 983048 | tf_op jit(solution)/shard_map/ppermute | solution.py:40
  126.1 20.7 %collective-permute-start.39 = (bf16[80,2048]{1,0:T(8,128)(2,1)S(1)}, bf16[80,2048]{1,0:T(8,128)(2,1)S(1)}, u32[]{:S(2)}, u32[]{:S(2)}) collective-permute-start(bf16[80,2048]{1,0:T(8,128)(2,1)S(1)} %get-tuple-element.36.refs_0_), channel_id=1, source_target_pairs={{0,4},{4,0},{8,12},{12,8},{1,5},{5,1},{9,13},{13,9},{2,6},{6,2},{1... | collective-permute-start | bytes 983048 | tf_op jit(solution)/shard_map/ppermute | solution.py:40
  147.9 21.5 %collective-permute-start.41 = (bf16[80,2048]{1,0:T(8,128)(2,1)S(1)}, bf16[80,2048]{1,0:T(8,128)(2,1)S(1)}, u32[]{:S(2)}, u32[]{:S(2)}) collective-permute-start(bf16[80,2048]{1,0:T(8,128)(2,1)S(1)} %collective-permute-done.39.refs_0_), channel_id=1, source_target_pairs={{0,2},{1,3},{2,0},{3,1},{4,6},{5,7},{6,4},{7,5},{8,10},{9,11},{10,... | collective-permute-start | bytes 983048 | tf_op jit(solution)/shard_map/ppermute | solution.py:40
  148.9 20.5 %collective-permute-start.23 = (bf16[80,2048]{1,0:T(8,128)(2,1)S(1)}, bf16[80,2048]{1,0:T(8,128)(2,1)S(1)}, u32[]{:S(2)}, u32[]{:S(2)}) collective-permute-start(bf16[80,2048]{1,0:T(8,128)(2,1)S(1)} %collective-permute-done.22.refs_2_), channel_id=1, source_target_pairs={{0,1},{1,0},{2,3},{3,2},{4,5},{5,4},{6,7},{7,6},{8,9},{9,8},{10,11... | collective-permute-start | bytes 983048 | tf_op jit(solution)/shard_map/ppermute | solution.py:40
  156.4 20.8 %collective-permute-start.58 = (bf16[80,2048]{1,0:T(8,128)(2,1)S(1)}, bf16[80,2048]{1,0:T(8,128)(2,1)S(1)}, u32[]{:S(2)}, u32[]{:S(2)}) collective-permute-start(bf16[80,2048]{1,0:T(8,128)(2,1)S(1)} %collective-permute-done.57.refs_2_), channel_id=1, source_target_pairs={{0,1},{1,0},{2,3},{3,2},{4,5},{5,4},{6,7},{7,6},{8,9},{9,8},{10,11... | collective-permute-start | bytes 983048 | tf_op jit(solution)/shard_map/ppermute | solution.py:40
  156.5 28.0 %collective-permute-start.48 = (bf16[80,2048]{1,0:T(8,128)(2,1)S(1)}, bf16[80,2048]{1,0:T(8,128)(2,1)S(1)}, u32[]{:S(2)}, u32[]{:S(2)}) collective-permute-start(bf16[80,2048]{1,0:T(8,128)(2,1)S(1)} %collective-permute-done.47.refs_0_), channel_id=1, source_target_pairs={{0,1},{1,0},{2,3},{3,2},{4,5},{5,4},{6,7},{7,6},{8,9},{9,8},{10,11... | collective-permute-start | bytes 983048 | tf_op jit(solution)/shard_map/ppermute | solution.py:40
  163.4 21.6 %collective-permute-start.50 = (bf16[80,2048]{1,0:T(8,128)(2,1)S(1)}, bf16[80,2048]{1,0:T(8,128)(2,1)S(1)}, u32[]{:S(2)}, u32[]{:S(2)}) collective-permute-start(bf16[80,2048]{1,0:T(8,128)(2,1)S(1)} %collective-permute-done.49.refs_2_), channel_id=1, source_target_pairs={{0,1},{1,0},{2,3},{3,2},{4,5},{5,4},{6,7},{7,6},{8,9},{9,8},{10,11... | collective-permute-start | bytes 983048 | tf_op jit(solution)/shard_map/ppermute | solution.py:40
  169.4 23.2 %collective-permute-start.40 = (bf16[80,2048]{1,0:T(8,128)(2,1)S(1)}, bf16[80,2048]{1,0:T(8,128)(2,1)S(1)}, u32[]{:S(2)}, u32[]{:S(2)}) collective-permute-start(bf16[80,2048]{1,0:T(8,128)(2,1)S(1)} %collective-permute-done.39.refs_0_), channel_id=1, source_target_pairs={{0,1},{1,0},{2,3},{3,2},{4,5},{5,4},{6,7},{7,6},{8,9},{9,8},{10,11... | collective-permute-start | bytes 983048 | tf_op jit(solution)/shard_map/ppermute | solution.py:40
  169.4 23.7 %collective-permute-start.42 = (bf16[80,2048]{1,0:T(8,128)(2,1)S(1)}, bf16[80,2048]{1,0:T(8,128)(2,1)S(1)}, u32[]{:S(2)}, u32[]{:S(2)}) collective-permute-start(bf16[80,2048]{1,0:T(8,128)(2,1)S(1)} %collective-permute-done.41.refs_2_), channel_id=1, source_target_pairs={{0,1},{1,0},{2,3},{3,2},{4,5},{5,4},{6,7},{7,6},{8,9},{9,8},{10,11... | collective-permute-start | bytes 983048 | tf_op jit(solution)/shard_map/ppermute | solution.py:40
  177.2 23.2 %collective-permute-start.37 = (bf16[80,2048]{1,0:T(8,128)(2,1)S(1)}, bf16[80,2048]{1,0:T(8,128)(2,1)S(1)}, u32[]{:S(2)}, u32[]{:S(2)}) collective-permute-start(bf16[80,2048]{1,0:T(8,128)(2,1)S(1)} %get-tuple-element.40), channel_id=1, source_target_pairs={{0,1},{1,0},{2,3},{3,2},{4,5},{5,4},{6,7},{7,6},{8,9},{9,8},{10,11... | collective-permute-start | bytes 983048 | tf_op jit(solution)/shard_map/ppermute | solution.py:40
  184.4 50.2 %collective-permute-start.36 = (bf16[80,2048]{1,0:T(8,128)(2,1)S(1)}, bf16[80,2048]{1,0:T(8,128)(2,1)S(1)}, u32[]{:S(2)}, u32[]{:S(2)}) collective-permute-start(bf16[80,2048]{1,0:T(8,128)(2,1)S(1)} %get-tuple-element.38), channel_id=1, source_target_pairs={{0,1},{1,0},{2,3},{3,2},{4,5},{5,4},{6,7},{7,6},{8,9},{9,8},{10,11... | collective-permute-start | bytes 983048 | tf_op jit(solution)/shard_map/ppermute | solution.py:40
  201.2 26.7 %collective-permute-start.43 = (bf16[80,2048]{1,0:T(8,128)(2,1)S(1)}, bf16[80,2048]{1,0:T(8,128)(2,1)S(1)}, u32[]{:S(2)}, u32[]{:S(2)}) collective-permute-start(bf16[80,2048]{1,0:T(8,128)(2,1)S(1)} %get-tuple-element.42), channel_id=1, source_target_pairs={{0,1},{1,0},{2,3},{3,2},{4,5},{5,4},{6,7},{7,6},{8,9},{9,8},{10,11... | collective-permute-start | bytes 983048 | tf_op jit(solution)/shard_map/ppermute | solution.py:40
  203.3 31.4 %collective-permute-start.38 = (bf16[80,2048]{1,0:T(8,128)(2,1)S(1)}, bf16[80,2048]{1,0:T(8,128)(2,1)S(1)}, u32[]{:S(2)}, u32[]{:S(2)}) collective-permute-start(bf16[80,2048]{1,0:T(8,128)(2,1)S(1)} %add_convert_fusion.6), channel_id=1, source_target_pairs={{0,2},{1,3},{2,0},{3,1},{4,6},{5,7},{6,4},{7,5},{8,10},{9,11},{10,... | collective-permute-start | bytes 983048 | tf_op jit(solution)/shard_map/ppermute | solution.py:40
  213.9 19.8 %collective-permute-start.45 = (bf16[80,2048]{1,0:T(8,128)(2,1)S(1)}, bf16[80,2048]{1,0:T(8,128)(2,1)S(1)}, u32[]{:S(2)}, u32[]{:S(2)}) collective-permute-start(bf16[80,2048]{1,0:T(8,128)(2,1)S(1)} %add_convert_fusion.5), channel_id=1, source_target_pairs={{0,2},{1,3},{2,0},{3,1},{4,6},{5,7},{6,4},{7,5},{8,10},{9,11},{10,... | collective-permute-start | bytes 983048 | tf_op jit(solution)/shard_map/ppermute | solution.py:40
  227.3 23.7 %collective-permute-start.62 = (bf16[80,2048]{1,0:T(8,128)(2,1)S(1)}, bf16[80,2048]{1,0:T(8,128)(2,1)S(1)}, u32[]{:S(2)}, u32[]{:S(2)}) collective-permute-start(bf16[80,2048]{1,0:T(8,128)(2,1)S(1)} %add_convert_fusion), channel_id=1, source_target_pairs={{0,8},{4,12},{8,0},{12,4},{1,9},{5,13},{9,1},{13,5},{2,10},{6,14},... | collective-permute-start | bytes 983048 | tf_op jit(solution)/shard_map/ppermute | solution.py:40
  228.0 23.0 %collective-permute-start.54 = (bf16[80,2048]{1,0:T(8,128)(2,1)S(1)}, bf16[80,2048]{1,0:T(8,128)(2,1)S(1)}, u32[]{:S(2)}, u32[]{:S(2)}) collective-permute-start(bf16[80,2048]{1,0:T(8,128)(2,1)S(1)} %add_convert_fusion.2), channel_id=1, source_target_pairs={{0,12},{4,8},{8,4},{12,0},{1,13},{5,9},{9,5},{13,1},{2,14},{6,10},... | collective-permute-start | bytes 983048 | tf_op jit(solution)/shard_map/ppermute | solution.py:40
  233.8 22.3 %collective-permute-start.46 = (bf16[80,2048]{1,0:T(8,128)(2,1)S(1)}, bf16[80,2048]{1,0:T(8,128)(2,1)S(1)}, u32[]{:S(2)}, u32[]{:S(2)}) collective-permute-start(bf16[80,2048]{1,0:T(8,128)(2,1)S(1)} %add_convert_fusion.4), channel_id=1, source_target_pairs={{0,4},{4,0},{8,12},{12,8},{1,5},{5,1},{9,13},{13,9},{2,6},{6,2},{1... | collective-permute-start | bytes 983048 | tf_op jit(solution)/shard_map/ppermute | solution.py:40
  (53 other events, 573.5 us)
where the time goes:
time: 258 us; the launch traced here: 257 us
  waiting for transfers between devices  139 us (54%)
  starting transfers between devices  58.5 us (23%)
  Pallas kernels  38.6 us (15%)
  local copies, waits for them, and re-layouts  11.8 us (5%)
  other arithmetic  8.58 us (3%)
    ppermute x63, waiting for transfers between devices, swap(): return lax.ppermute(array, axis, [(i, i ^ bits) for i in range(size)])  139 us
    ppermute x63, starting transfers between devices, swap(): return lax.ppermute(array, axis, [(i, i ^ bits) for i in range(size)])  58.5 us
    pallas_call x4, Pallas kernels, ffn_chunk(): pl.pallas_call(run, in_specs=[SMEM, VMEM] + [HBM] * (nt + 2 + 2 * len(key...  29.2 us
    squeeze x5, local copies, waits for them, and re-layouts, pick(): array = lax.dynamic_index_in_dim(array, index, 0, keepdims=False)  6 us
  transfers between devices with their start and end apart: 63, of which 24 were waited for; matrix products, arithmetic and copies ran while one was open for 7% of the time, Pallas kernels for 14%

commit v1 on v0

--- a/solution.py
+++ b/solution.py
@@ -38,12 +38,6 @@
 
 def swap(array, axis, size, bits):
     return lax.ppermute(array, axis, [(i, i ^ bits) for i in range(size)])
-
-
-def pick(array, *indices):
-    for index in indices:
-        array = lax.dynamic_index_in_dim(array, index, 0, keepdims=False)
-    return array
 
 
 def halvings(size):
@@ -79,7 +73,8 @@
 
 VMEM = pl.BlockSpec(memory_space=pltpu.VMEM)
 SMEM = pl.BlockSpec(memory_space=pltpu.SMEM)
-HBM = pl.BlockSpec(memory_space=pl.ANY)
+ANY = pl.BlockSpec(memory_space=pl.ANY)
+HBM = pl.BlockSpec(memory_space=pltpu.HBM)
 
 
 def aligned(index, size):
@@ -114,13 +109,13 @@
     )(*arrays)
 
 
-def glu_conv(spot, sizes, blocks, own, pieces, taps):
+def glu_conv(spot, sizes, blocks, val, gate, pieces, taps):
     ng, nf, nt = sizes
     rows, width = blocks[0].shape
     total = nt * rows
-    depth, packed = own.shape
+    depth, channels = val.shape
+    packed = 2 * channels
     share = depth // ng
-    channels = packed // 2
     count = taps.shape[0]
     lead = -(-(count - 1) // 8) * 8
     segments = total // LEN
@@ -128,12 +123,14 @@
 
     def run(spot_ref, taps_ref, *refs):
         block_refs, refs = refs[:nt], refs[nt:]
-        own_ref, refs = refs[0], refs[1:]
+        own_refs, refs = refs[:2], refs[2:]
         piece_refs, refs = refs[: len(keys)], refs[len(keys) :]
         conv_ref, sums_ref, gathered, weight, padded, sems = refs
         group, slab, member = spot_ref[0], spot_ref[1], spot_ref[2]
         pairs = [(block_refs[d], gathered.at[aligned(member ^ d, rows)]) for d in range(nt)]
-        pairs.append((own_ref, weight.at[aligned(slab, depth)]))
+        for i, ref in enumerate(own_refs):
+            columns = pl.ds(i * channels, channels)
+            pairs.append((ref, weight.at[aligned(slab, depth), columns]))
         for (d, e), ref in zip(keys, piece_refs):
             place = (slab ^ d) * ng + (group ^ e)
             pairs.append((ref, weight.at[aligned(place, share)]))
@@ -165,7 +162,7 @@
 
     return pl.pallas_call(
         run,
-        in_specs=[SMEM, VMEM] + [HBM] * (nt + 1 + len(keys)),
+        in_specs=[SMEM, VMEM] + [ANY] * nt + [HBM] * 2 + [ANY] * len(keys),
         out_specs=[VMEM, VMEM],
         out_shape=[
             jax.ShapeDtypeStruct((total, channels), F32),
@@ -175,7 +172,7 @@
             pltpu.VMEM((total, width), BF16),
             pltpu.VMEM((nf * depth, packed), BF16),
             pltpu.VMEM((segments, lead + LEN, channels), F32),
-            pltpu.SemaphoreType.DMA((nt + 1 + len(keys),)),
+            pltpu.SemaphoreType.DMA((nt + 2 + len(keys),)),
         ],
         cost_estimate=pl.CostEstimate(
             flops=2 * total * width * packed,
@@ -184,7 +181,7 @@
         ),
         compiler_params=pltpu.CompilerParams(vmem_limit_bytes=24 * MEBI),
         name="glu_conv",
-    )(spot, taps, *[blocks[d] for d in range(nt)], own, *pieces.values())
+    )(spot, taps, *[blocks[d] for d in range(nt)], val, gate, *pieces.values())
 
 
 def out_product(spot, sizes, conv, sums, gain, all_channels, own, pieces):
@@ -227,8 +224,8 @@
 
     return pl.pallas_call(
         run,
-        in_specs=[SMEM, VMEM, VMEM] + [VMEM] * len(sums) + [HBM] * (1 + len(keys)),
-        out_specs=[HBM] * nt,
+        in_specs=[SMEM, VMEM, VMEM] + [VMEM] * len(sums) + [HBM] + [ANY] * len(keys),
+        out_specs=[ANY] * nt,
         out_shape=[jax.ShapeDtypeStruct((rows, nf * cols), BF16)] * nt,
         scratch_shapes=[
             pltpu.VMEM((nf, depth, cols), BF16),
@@ -245,37 +242,203 @@
     )(spot, conv, gain, *sums, own, *pieces.values())
 
 
-def ffn_chunk(spot, sizes, blocks, up_own, up_pieces, taps, down_own, down_pieces):
-    ng, nf, nt = sizes
+def mix_shares(spot, sizes, val, gate, out):
+    ng = sizes[0]
+    depth, channels = val.shape
+    tall, cols = out.shape
+
+    def run(spot_ref, val_ref, gate_ref, out_ref, glu_share, out_share, glu_held, out_held, sems):
+        group = spot_ref[0]
+        rows = aligned(group, depth // ng)
+        pairs = [
+            (val_ref.at[rows], glu_held.at[:, pl.ds(0, channels)]),
+            (gate_ref.at[rows], glu_held.at[:, pl.ds(channels, channels)]),
+            (out_ref.at[aligned(group, tall // ng)], out_held),
+        ]
+        copies = start_copies(pairs, sems)
+        for copy in copies[:2]:
+            copy.wait()
+        outward = start_copies([(glu_held, glu_share)], sems, 3)
+        copies[2].wait()
+        outward += start_copies([(out_held, out_share)], sems, 4)
+        for copy in outward:
+            copy.wait()
+
+    return pl.pallas_call(
+        run,
+        in_specs=[SMEM, HBM, HBM, HBM],
+        out_specs=[ANY, ANY],
+        out_shape=[
+            jax.ShapeDtypeStruct((depth // ng, 2 * channels), BF16),
+            jax.ShapeDtypeStruct((tall // ng, cols), BF16),
+        ],
+        scratch_shapes=[
+            pltpu.VMEM((depth // ng, 2 * channels), BF16),
+            pltpu.VMEM((tall // ng, cols), BF16),
+            pltpu.SemaphoreType.DMA((5,)),
+        ],
+        compiler_params=pltpu.CompilerParams(vmem_limit_bytes=60 * MEBI),
+        name="mix_shares",
+    )(spot, val, gate, out)
+
+
+def ffn_shares(spot, sizes, gate, val, down):
+    ng, nf, _ = sizes
+    depth, local_ff = gate.shape
+    cols = down.shape[1]
+    units = local_ff // nf
+    whole = units // LANES * LANES
+    rest = units - whole
+    share = depth // ng
+    packed = 2 * units
+    count = nf - 1
+    tall = (whole // ng, rest // ng)
+
+    def run(spot_ref, *refs):
+        sources, refs = refs[:3], refs[3:]
+        up_refs, refs = refs[:count], refs[count:]
+        down_refs, refs = refs[:count], refs[count:]
+        up_own_ref, down_own_ref, gate_ref, val_ref, down_ref, halves, sems = refs
+        group, slab = spot_ref[0], spot_ref[1]
+        rows = aligned(group, share)
+        for copy in start_copies(zip(sources, (gate_ref, val_ref, down_ref)), sems):
+            copy.wait()
+        mine = pl.ds(pl.multiple_of(slab * whole, LANES), whole)
+        pairs = [
+            (gate_ref.at[:, mine], up_own_ref.at[:, pl.ds(0, whole)]),
+            (val_ref.at[:, mine], up_own_ref.at[:, pl.ds(whole, whole)]),
+            (down_ref.at[mine], down_own_ref.at[pl.ds(0, whole)]),
+        ]
+        if rest:
+            last = pl.ds(pl.multiple_of(nf * whole + slab * rest, 16), rest)
+            pairs.append((down_ref.at[last], down_own_ref.at[pl.ds(whole, rest)]))
+        for d in range(1, nf):
+            there = slab ^ d
+            columns = pl.ds(pl.multiple_of(there * whole, LANES), whole)
+            for i, ref in enumerate((gate_ref, val_ref)):
+                pairs.append((ref.at[rows, columns], up_refs[d - 1].at[:, pl.ds(i * whole, whole)]))
+            first = pl.multiple_of(there * whole + group * tall[0], 16)
+            pairs.append(
+                (down_ref.at[pl.ds(first, tall[0])], down_refs[d - 1].at[pl.ds(0, tall[0])])
+            )
+            if rest:
+                first = pl.multiple_of(nf * whole + there * rest + group * tall[1], 16)
+                part = down_refs[d - 1].at[pl.ds(tall[0], tall[1])]
+                pairs.append((down_ref.at[pl.ds(first, tall[1])], part))
+        copies = start_copies(pairs, sems, 3)
+        if rest:
+            lane = lax.broadcasted_iota(jnp.int32, (depth, LANES), 1)
+            for s in range(nf):
+                begin = nf * whole + s * rest // LANES * LANES
+                pair = [ref[:, begin : begin + LANES].astype(F32) for ref in (gate_ref, val_ref)]
+                moved = 1 if s * rest % LANES == 0 else 0
+                pair[moved] = pltpu.roll(pair[moved], rest, 1)
+                halves[s] = jnp.where(lane < rest, pair[0], pair[1]).astype(BF16)
+            pairs = [
+                (halves.at[slab ^ d, rows], up_refs[d - 1].at[:, pl.ds(2 * whole, LANES)])
+                for d in range(1, nf)
+            ]
+            pairs.append((halves.at[slab], up_own_ref.at[:, pl.ds(2 * whole, LANES)]))
+            copies += start_copies(pairs, sems, 3 + len(copies))
+        for copy in copies:
+            copy.wait()
+
+    outs = pl.pallas_call(
+        run,
+        in_specs=[SMEM, HBM, HBM, HBM],
+        out_specs=[ANY] * (2 * count + 2),
+        out_shape=[jax.ShapeDtypeStruct((share, packed), BF16)] * count
+        + [jax.ShapeDtypeStruct((units // ng, cols), BF16)] * count
+        + [jax.ShapeDtypeStruct((depth, packed), BF16)]
+        + [jax.ShapeDtypeStruct((units, cols), BF16)],
+        scratch_shapes=[
+            pltpu.VMEM(gate.shape, BF16),
+            pltpu.VMEM(val.shape, BF16),
+            pltpu.VMEM(down.shape, BF16),
+            pltpu.VMEM((nf, depth, LANES), BF16),
+            pltpu.SemaphoreType.DMA((8 + 5 * count,)),
+        ],
+        cost_estimate=pl.CostEstimate(
+            flops=depth * packed, transcendentals=0, bytes_accessed=8 * depth * packed
+        ),
+        compiler_params=pltpu.CompilerParams(vmem_limit_bytes=60 * MEBI),
+        name="ffn_shares",
+    )(spot, gate, val, down)
+    ups = {d: outs[d - 1] for d in range(1, nf)}
+    downs = {d: outs[count + d - 1] for d in range(1, nf)}
+    return ups, downs, outs[-2], outs[-1]
+
+
+def ffn_weights(spot, sizes, up_own, up_pieces, down_own, down_pieces):
+    ng, nf, _ = sizes
+    depth, packed = up_own.shape
+    units, cols = down_own.shape
+    whole = units // LANES * LANES
+    rest = units - whole
+    padded = -(-units // LANES) * LANES
+    share = depth // ng
+    tall = (whole // ng, rest // ng)
+    keys = list(up_pieces)
+
+    def run(spot_ref, up_own_ref, down_own_ref, *refs):
+        up_refs, refs = refs[: len(keys)], refs[len(keys) :]
+        down_refs, refs = refs[: len(keys)], refs[len(keys) :]
+        up, down, sems = refs
+        group, slab = spot_ref[0], spot_ref[1]
+        pairs = [
+            (up_own_ref, up.at[aligned(slab, depth)]),
+            (down_own_ref, down.at[slab, pl.ds(0, units)]),
+        ]
+        for (d, e), up_ref, down_ref in zip(keys, up_refs, down_refs):
+            place = (slab ^ d) * ng + (group ^ e)
+            pairs.append((up_ref, up.at[aligned(place, share)]))
+            target = down.at[slab ^ d, aligned(group ^ e, tall[0])]
+            pairs.append((down_ref.at[pl.ds(0, tall[0])], target))
+            if rest:
+                first = pl.multiple_of(whole + (group ^ e) * tall[1], 16)
+                target = down.at[slab ^ d, pl.ds(first, tall[1])]
+                pairs.append((down_ref.at[pl.ds(tall[0], tall[1])], target))
+        copies = start_copies(pairs, sems)
+        if padded > units:
+            down[:, units:, :] = jnp.zeros((nf, padded - units, cols), BF16)
+        for copy in copies:
+            copy.wait()
+
+    return pl.pallas_call(
+        run,
+        in_specs=[SMEM] + [ANY] * (2 + 2 * len(keys)),
+        out_specs=[VMEM, VMEM],
+        out_shape=[
+            jax.ShapeDtypeStruct((nf * depth, packed), BF16),
+            jax.ShapeDtypeStruct((nf, padded, cols), BF16),
+        ],
+        scratch_shapes=[pltpu.SemaphoreType.DMA((2 + 3 * len(keys),))],
+        cost_estimate=pl.CostEstimate(
+            flops=nf * depth * packed, transcendentals=0, bytes_accessed=4 * nf * depth * packed
+        ),
+        compiler_params=pltpu.CompilerParams(vmem_limit_bytes=12 * MEBI),
+        name="ffn_weights",
+    )(spot, up_own, down_own, *up_pieces.values(), *down_pieces.values())
+
+
+def ffn_chunk(spot, sizes, blocks, up, taps, down):
+    nt = sizes[2]
     rows, width = blocks[0].shape
     total = nt * rows
-    depth, packed = up_own.shape
-    units, cols = down_own.shape
-    up_share, down_share = depth // ng, units // ng
+    packed = up.shape[1]
+    parts, padded, cols = down.shape
+    units = packed // 2
     whole = units // LANES * LANES
     rest = units - whole
-    keys = list(up_pieces)
     wide = 2 * LANES
 
-    def run(spot_ref, taps_ref, *refs):
+    def run(spot_ref, taps_ref, up, down, *refs):
         block_refs, refs = refs[:nt], refs[nt:]
-        up_own_ref, down_own_ref, refs = refs[0], refs[1], refs[2:]
-        up_refs, refs = refs[: len(keys)], refs[len(keys) :]
-        down_refs, refs = refs[: len(keys)], refs[len(keys) :]
         out_refs, refs = refs[:nt], refs[nt:]
-        gathered, up, down, hidden, mixed, sems = refs
-        group, slab, member = spot_ref[0], spot_ref[1], spot_ref[2]
+        gathered, hidden, mixed, sems = refs
+        member = spot_ref[2]
         pairs = [(block_refs[d], gathered.at[aligned(member ^ d, rows)]) for d in range(nt)]
-        pairs.append((up_own_ref, up.at[aligned(slab, depth)]))
-        for (d, e), ref in zip(keys, up_refs):
-            place = (slab ^ d) * ng + (group ^ e)
-            pairs.append((ref, up.at[aligned(place, up_share)]))
-        copies = start_copies(pairs, sems)
-        late = [(down_own_ref, down.at[slab])]
-        for (d, e), ref in zip(keys, down_refs):
-            late.append((ref, down.at[slab ^ d, aligned(group ^ e, down_share)]))
-        late = start_copies(late, sems, len(pairs))
-        for copy in copies:
+        for copy in start_copies(pairs, sems):
             copy.wait()
 
         def conv(column, size):
@@ -302,52 +465,40 @@
             lane = lax.broadcasted_iota(jnp.int32, both.shape, 1)
             gated = gelu(both) * pltpu.roll(both, LANES - rest, 1)
             hidden[:, whole:] = jnp.where(lane < rest, gated, 0.0).astype(BF16)
-        for copy in late:
-            copy.wait()
-        for s in range(nf):
-            columns = slice(s * cols, (s + 1) * cols)
-            mixed[:, columns] = product(hidden[:, :units], down[s]).astype(BF16)
-        targets = [(mixed.at[aligned(member ^ d, rows)], out_refs[d]) for d in range(nt)]
-        for copy in start_copies(targets, sems):
-            copy.wait()
-
-    flops = 2 * total * width * packed + 2 * total * units * nf * cols
+        outward = []
+        for s in range(parts):
+            columns = pl.ds(s * cols, cols)
+            mixed[:, columns] = product(hidden[...], down[s]).astype(BF16)
+            targets = [
+                (mixed.at[aligned(member ^ d, rows), columns], out_refs[d].at[:, columns])
+                for d in range(nt)
+            ]
+            outward += start_copies(targets, sems, nt + len(outward))
+        for copy in outward:
+            copy.wait()
+
+    flops = 2 * total * width * packed + 2 * total * units * parts * cols
     return pl.pallas_call(
         run,
-        in_specs=[SMEM, VMEM] + [HBM] * (nt + 2 + 2 * len(keys)),
-        out_specs=[HBM] * nt,
-        out_shape=[jax.ShapeDtypeStruct((rows, nf * cols), BF16)] * nt,
+        in_specs=[SMEM, VMEM, VMEM, VMEM] + [ANY] * nt,
+        out_specs=[ANY] * nt,
+        out_shape=[jax.ShapeDtypeStruct((rows, parts * cols), BF16)] * nt,
         scratch_shapes=[
             pltpu.VMEM((total, width), BF16),
-            pltpu.VMEM((nf * depth, packed), BF16),
-            pltpu.VMEM((nf, units, cols), BF16),
-            pltpu.VMEM((total, whole + (LANES if rest else 0)), BF16),
-            pltpu.VMEM((total, nf * cols), BF16),
-            pltpu.SemaphoreType.DMA((nt + 2 + 2 * len(keys),)),
+            pltpu.VMEM((total, padded), BF16),
+            pltpu.VMEM((total, parts * cols), BF16),
+            pltpu.SemaphoreType.DMA((nt + nt * parts,)),
         ],
         cost_estimate=pl.CostEstimate(
             flops=flops, transcendentals=total * units, bytes_accessed=2 * width * packed
         ),
-        compiler_params=pltpu.CompilerParams(vmem_limit_bytes=24 * MEBI),
+        compiler_params=pltpu.CompilerParams(vmem_limit_bytes=20 * MEBI),
         name="ffn_chunk",
-    )(
-        spot,
-        taps,
-        *[blocks[d] for d in range(nt)],
-        up_own,
-        down_own,
-        *up_pieces.values(),
-        *down_pieces.values(),
-    )
-
-
-def pair_order(nf):
-    return sorted(range(1, nf), key=lambda d: (d != 1, -d))
+    )(spot, taps, up, down, *[blocks[d] for d in range(nt)])
 
 
 def exchange_shards(sizes):
     ng, nf, nt = sizes
-    far = pair_order(nf)
 
     def shards(
         tokens,
@@ -368,46 +519,42 @@
         group, slab, member = (lax.axis_index(a) for a in ("grp", "fs", "tp"))
         spot = jnp.stack([group, slab, member]).astype(jnp.int32)
 
-        def fetch(piece_for):
-            pieces = {}
-            for d in far:
-                pieces[d, 0] = swap(piece_for(d), "fs", nf, d)
-            for d in far:
+        def share_out(blocks):
+            pieces = {(d, 0): blocks[d] for d in range(1, nf)}
+            for d in range(1, nf):
                 for e in range(1, ng):
-                    pieces[d, e] = swap(pieces[d, 0], "grp", ng, e)
+                    pieces[d, e] = swap(blocks[d], "grp", ng, e)
             return pieces
 
-        def share(array):
-            return pick(array.reshape(ng, array.shape[0] // ng, array.shape[1]), group)
+        def fetch(shares):
+            sent = {d: swap(shares[d], "fs", nf, d) for d in shares}
+            return share_out(sent)
+
+        def fetch_all(mine):
+            return share_out(gather_blocks(mine, "fs", nf))
 
         local_ch = val_weight.shape[1]
-        glu_own = jnp.concatenate([val_weight, gate_weight], axis=1)
-        glu_share = jnp.concatenate([share(val_weight), share(gate_weight)], axis=1)
-        glu_pieces = fetch(lambda d: glu_share)
-        out_share = share(out_weight)
-        out_pieces = fetch(lambda d: out_share)
+        glu_share, out_share = mix_shares(spot, sizes, val_weight, gate_weight, out_weight)
+        glu_pieces = fetch_all(glu_share)
+        out_pieces = fetch_all(out_share)
 
         local_ff = up_gate_weight.shape[1]
         units = local_ff // nf
         whole = units // LANES * LANES
-
-        def pack(gate, val):
-            def block(s):
-                a, b, c = s * units, s * units + whole, (s + 1) * units
-                cut = [gate[..., a:b], val[..., a:b], gate[..., b:c], val[..., b:c]]
-                return jnp.concatenate(cut, axis=-1)
-
-            return jnp.stack([block(s) for s in range(nf)])
-
-        up_blocks = pack(up_gate_weight, up_val_weight)
-        up_own = pick(up_blocks, slab)
-        up_halves = up_blocks.reshape(nf, ng, up_blocks.shape[1] // ng, 2 * units)
-        up_pieces = fetch(lambda d: pick(up_halves, slab ^ d, group))
-        down_own = pick(down_weight.reshape(nf, units, down_weight.shape[1]), slab)
-        down_halves = down_weight.reshape(nf, ng, units // ng, down_weight.shape[1])
-        down_pieces = fetch(lambda d: pick(down_halves, slab ^ d, group))
-        own_taps = lax.dynamic_slice_in_dim(ffn_taps, member * local_ff, local_ff, 2)
-        own_taps = pick(pack(own_taps[0], own_taps[1]), slab).astype(F32)
+        rest = units - whole
+        up_shares, down_shares, up_own, down_own = ffn_shares(
+            spot, sizes, up_gate_weight, up_val_weight, down_weight
+        )
+        up_pieces, down_pieces = fetch(up_shares), fetch(down_shares)
+        up_full, down_full = ffn_weights(spot, sizes, up_own, up_pieces, down_own, down_pieces)
+        begin = member * local_ff
+        taps_whole = lax.dynamic_slice_in_dim(ffn_taps, begin + slab * whole, whole, 2)
+        own_taps = [taps_whole[0], taps_whole[1]]
+        if rest:
+            first = begin + nf * whole + slab * rest
+            taps_rest = lax.dynamic_slice_in_dim(ffn_taps, first, rest, 2)
+            own_taps += [taps_rest[0], taps_rest[1]]
+        own_taps = jnp.concatenate(own_taps, axis=1).astype(F32)
 
         def scaled(values, gain):
             mean = jnp.mean(values * values, axis=-1, keepdims=True)
@@ -417,7 +564,9 @@
         own_gain = lax.dynamic_slice_in_dim(chan_gain[None], member * local_ch, local_ch, 1)
         (normed,) = row_kernel(lambda t, g: (scaled(t, g),), [tokens, mix_gain[None]], 1)
         row_blocks = gather_blocks(normed, "tp", nt)
-        conv, sums = glu_conv(spot, sizes, row_blocks, glu_own, glu_pieces, mix_taps.astype(F32))
+        conv, sums = glu_conv(
+            spot, sizes, row_blocks, val_weight, gate_weight, glu_pieces, mix_taps.astype(F32)
+        )
         all_sums = [sums] + [swap(sums, "tp", nt, d) for d in range(1, nt)]
         mixed = out_product(
             spot,
@@ -440,12 +589,10 @@
         )
 
         last = []
-        for d in [0, *far]:
-            block = swap(acted, "fs", nf, d) if d else acted
-            blocks = gather_blocks(block, "tp", nt)
-            parts = ffn_chunk(
-                spot, sizes, blocks, up_own, up_pieces, own_taps, down_own, down_pieces
-            )
+        acts = gather_blocks(acted, "fs", nf)
+        for d in range(nf):
+            blocks = gather_blocks(acts[d], "tp", nt)
+            parts = ffn_chunk(spot, sizes, blocks, up_full, own_taps, down_full)
             terms = scatter_blocks(dict(enumerate(parts)), "tp", nt)
             if d:
                 terms = [swap(add_terms(terms), "fs", nf, d)]
@@ -541,7 +688,7 @@
 
     def run(*args):
         units = args[9].shape[1] // (sizes[1] * sizes[2])
-        cuts = units % LANES in (0, LANES // 2) and units % (16 * sizes[0]) == 0
+        cuts = units % LANES in (0, LANES // 2) and units % (32 * sizes[0]) == 0
         shards = exchange_shards(sizes) if exchange and cuts else gather_shards
         return jax.shard_map(
             shards,

time: 258 us -> 233 us (0.903); the launches traced: 257 us -> 230 us
  waiting for transfers between devices: 139 us -> 121 us
  local copies, waits for them, and re-layouts: 11.8 us -> 3.44 us
  other arithmetic: 8.58 us -> 2.92 us
  starting transfers between devices: 58.5 us -> 62.5 us
    ppermute x63, waiting for transfers between devices: 139 us -> 121 us  [swap(): return lax.ppermute(array, axis, [(i, i ^ bits) for i in range(size)])]
    squeeze x6 -> x2, local copies, waits for them, and re-layouts: 6.01 us -> 0.01 us  [the longest x1 0.01 us: shards(): own_taps = [taps_whole[0], taps_whole[1]]]
    ppermute x63, starting transfers between devices: 58.5 us -> 62.5 us  [swap(): return lax.ppermute(array, axis, [(i, i ^ bits) for i in range(size)])]
    pallas_call x5 -> x8, Pallas kernels: 33.8 us -> 34 us  [the longest x4 19.5 us: ffn_chunk(): pl.pallas_call(run, in_specs=[SMEM, VMEM, VMEM, VMEM] + [ANY] * nt, out_s...]
  transfers between devices with their start and end apart: 63 -> 63, of which waited for: 24 -> 19; matrix products, arithmetic and copies ran while one was open for 7% -> 2% of each run, Pallas kernels for 14% -> 14%
where the time goes in v1:
time: 233 us; the launch traced here: 230 us
  waiting for transfers between devices  121 us (52%)
  starting transfers between devices  62.5 us (27%)
  Pallas kernels  39.1 us (17%)
  local copies, waits for them, and re-layouts  3.44 us (1%)
  other arithmetic  2.92 us (1%)
    ppermute x63, waiting for transfers between devices, swap(): return lax.ppermute(array, axis, [(i, i ^ bits) for i in range(size)])  121 us
    ppermute x63, starting transfers between devices, swap(): return lax.ppermute(array, axis, [(i, i ^ bits) for i in range(size)])  62.5 us
    pallas_call x4, Pallas kernels, ffn_chunk(): pl.pallas_call(run, in_specs=[SMEM, VMEM, VMEM, VMEM] + [ANY] * nt, out_s...  19.5 us
  transfers between devices with their start and end apart: 63, of which 19 were waited for; matrix products, arithmetic and copies ran while one was open for 2% of the time, Pallas kernels for 14%

profile of v1, /device:TPU:0, one launch (start us, length us, event | category | flops | bytes accessed | tf_op | source)
XLA Modules:
  0.0 229.5 jit_solution(849527614460924626)
XLA Ops:
  0.6 2.5 %mix_shares.1 = (bf16[256,512]{1,0:T(8,128)(2,1)}, bf16[128,512]{1,0:T(8,128)(2,1)}) custom-call(s32[3]{0:T(128)} %pad_add_fusion.spot_ref, bf16[512,256]{1,0:T(8,128)(2,1)} %refs_4_.2, bf16[512,256]{1,0:T(8,128)(2,1)} %refs_5_.1, bf16[256,512]{1,0:T(8,128)(2,1)} %refs_4_.3), custom_call_target="tpu_custom_call" | custom-call | tf_op jit(solution)/shard_map/mix_shares/pallas_call | solution.py:267
  3.1 4.1 %collective-permute-start.4 = (bf16[256,512]{1,0:T(8,128)(2,1)}, bf16[256,512]{1,0:T(8,128)(2,1)S(1)}, u32[]{:S(2)}, u32[]{:S(2)}) collective-permute-start(bf16[256,512]{1,0:T(8,128)(2,1)} %get-tuple-element.41), channel_id=1, source_target_pairs={{0,8},{4,12},{8,0},{12,4},{1,9},{5,13},{9,1},{13,5},{2,10},{6,14},... | collective-permute-start | bytes 786440 | tf_op jit(solution)/shard_map/ppermute | solution.py:40
  13.0 10.0 %collective-permute-done.4.refs_7_ = bf16[256,512]{1,0:T(8,128)(2,1)S(1)} collective-permute-done((bf16[256,512]{1,0:T(8,128)(2,1)}, bf16[256,512]{1,0:T(8,128)(2,1)S(1)}, u32[]{:S(2)}, u32[]{:S(2)}) %collective-permute-start.4) | collective-permute-done | bytes 262176 | tf_op jit(solution)/shard_map/ppermute | solution.py:40
  23.2 1.8 collective-permute-done.13.refs_6_
  25.0 5.4 %collective-permute-done.12.refs_5_ = bf16[128,512]{1,0:T(8,128)(2,1)S(1)} collective-permute-done((bf16[128,512]{1,0:T(8,128)(2,1)}, bf16[128,512]{1,0:T(8,128)(2,1)S(1)}, u32[]{:S(2)}, u32[]{:S(2)}) %collective-permute-start.12) | collective-permute-done | bytes 131104 | tf_op jit(solution)/shard_map/ppermute | solution.py:40
  30.6 1.6 collective-permute-start.7
  32.2 4.7 %collective-permute-done.14.refs_7_ = bf16[128,512]{1,0:T(8,128)(2,1)S(1)} collective-permute-done((bf16[128,512]{1,0:T(8,128)(2,1)S(1)}, bf16[128,512]{1,0:T(8,128)(2,1)S(1)}, u32[]{:S(2)}, u32[]{:S(2)}) %collective-permute-start.14) | collective-permute-done | bytes 131104 | tf_op jit(solution)/shard_map/ppermute | solution.py:40
  42.0 4.1 %collective-permute-done.6.refs_9_ = bf16[256,512]{1,0:T(8,128)(2,1)S(1)} collective-permute-done((bf16[256,512]{1,0:T(8,128)(2,1)S(1)}, bf16[256,512]{1,0:T(8,128)(2,1)S(1)}, u32[]{:S(2)}, u32[]{:S(2)}) %collective-permute-start.6) | collective-permute-done | bytes 262176 | tf_op jit(solution)/shard_map/ppermute | solution.py:40
  47.7 4.0 %collective-permute-done.8.refs_11_ = bf16[256,512]{1,0:T(8,128)(2,1)S(1)} collective-permute-done((bf16[256,512]{1,0:T(8,128)(2,1)S(1)}, bf16[256,512]{1,0:T(8,128)(2,1)S(1)}, u32[]{:S(2)}, u32[]{:S(2)}) %collective-permute-start.8) | collective-permute-done | bytes 262176 | tf_op jit(solution)/shard_map/ppermute | solution.py:40
  51.7 4.5 %glu_conv.1 = (f32[320,256]{1,0:T(8,128)S(1)}, f32[16,320]{1,0:T(8,128)S(1)}) custom-call(s32[3]{0:T(128)S(1)} %copy-done.11, f32[31,256]{1,0:T(8,128)S(1)} %dynamic-slice_convert_fusion.taps_ref, bf16[80,2048]{1,0:T(8,128)(2,1)S(1)} %shard_map.136.refs_0_, bf16[80,2048]{1,0:T(8,128)(2,1)S(1)} %collective-permute-done.refs_1_, ...), custom_call_target="tpu_custom_call" | custom-call | flops 671088640 | bytes 2097152 | tf_op jit(solution)/shard_map/glu_conv/pallas_call | solution.py:163
  60.4 3.2 %out_product.1 = (bf16[80,2048]{1,0:T(8,128)(2,1)S(1)}, bf16[80,2048]{1,0:T(8,128)(2,1)}, bf16[80,2048]{1,0:T(8,128)(2,1)S(1)}, bf16[80,2048]{1,0:T(8,128)(2,1)S(1)}) custom-call(s32[3]{0:T(128)S(1)} %copy-done.11, f32[320,256]{1,0:T(8,128)S(1)} %get-tuple-element.42.conv_ref, f32[1,256]{1,0:T(1,128)S(1)} %bitcast.12, ...), custom_call_target="tpu_custom_call" | custom-call | flops 335544320 | bytes 1048576 | tf_op jit(solution)/shard_map/out_product/pallas_call | solution.py:225
  63.9 4.4 %ffn_shares.1 = (bf16[256,640]{1,0:T(8,128)(2,1)}, bf16[256,640]{1,0:T(8,128)(2,1)}, bf16[256,640]{1,0:T(8,128)(2,1)}, bf16[160,512]{1,0:T(8,128)(2,1)}, bf16[16...) custom-call(s32[3]{0:T(128)} %pad_add_fusion.spot_ref, ...), custom_call_target="tpu_custom_call" | custom-call | flops 327680 | bytes 2621440 | tf_op jit(solution)/shard_map/ffn_shares/pallas_call | solution.py:346
  70.4 4.5 %collective-permute-start.28 = (bf16[160,512]{1,0:T(8,128)(2,1)}, bf16[160,512]{1,0:T(8,128)(2,1)}, u32[]{:S(2)}, u32[]{:S(2)}) collective-permute-start(bf16[160,512]{1,0:T(8,128)(2,1)} %get-tuple-element.56), channel_id=1, source_target_pairs={{0,8},{4,12},{8,0},{12,4},{1,9},{5,13},{9,1},{13,5},{2,10},{6,14},... | collective-permute-start | bytes 491528 | tf_op jit(solution)/shard_map/ppermute | solution.py:40
  75.2 10.5 %collective-permute-done.27.refs_6_ = bf16[160,512]{1,0:T(8,128)(2,1)S(1)} collective-permute-done((bf16[160,512]{1,0:T(8,128)(2,1)}, bf16[160,512]{1,0:T(8,128)(2,1)S(1)}, u32[]{:S(2)}, u32[]{:S(2)}) %collective-permute-start.27) | collective-permute-done | bytes 163872 | tf_op jit(solution)/shard_map/ppermute | solution.py:40
  86.9 6.4 %collective-permute-start.22 = (bf16[256,640]{1,0:T(8,128)(2,1)}, bf16[256,640]{1,0:T(8,128)(2,1)S(1)}, u32[]{:S(2)}, u32[]{:S(2)}) collective-permute-start(bf16[256,640]{1,0:T(8,128)(2,1)} %get-tuple-element.53), channel_id=1, source_target_pairs={{0,8},{4,12},{8,0},{12,4},{1,9},{5,13},{9,1},{13,5},{2,10},{6,14},... | collective-permute-start | bytes 983048 | tf_op jit(solution)/shard_map/ppermute | solution.py:40
  93.3 1.9 collective-permute-start.23
  100.0 16.0 %collective-permute-done.22.refs_1_ = bf16[256,640]{1,0:T(8,128)(2,1)S(1)} collective-permute-done((bf16[256,640]{1,0:T(8,128)(2,1)}, bf16[256,640]{1,0:T(8,128)(2,1)S(1)}, u32[]{:S(2)}, u32[]{:S(2)}) %collective-permute-start.22) | collective-permute-done | bytes 327712 | tf_op jit(solution)/shard_map/ppermute | solution.py:40
  119.6 6.5 %collective-permute-start.47 = (bf16[80,2048]{1,0:T(8,128)(2,1)S(1)}, bf16[80,2048]{1,0:T(8,128)(2,1)S(1)}, u32[]{:S(2)}, u32[]{:S(2)}) collective-permute-start(bf16[80,2048]{1,0:T(8,128)(2,1)S(1)} %get-tuple-element.60.refs_0_), channel_id=1, source_target_pairs={{0,8},{4,12},{8,0},{12,4},{1,9},{5,13},{9,1},{13,5},{2,10},{6,14},... | collective-permute-start | bytes 983048 | tf_op jit(solution)/shard_map/ppermute | solution.py:40
  128.1 5.0 %collective-permute-done.25.refs_4_ = bf16[256,640]{1,0:T(8,128)(2,1)S(1)} collective-permute-done((bf16[256,640]{1,0:T(8,128)(2,1)S(1)}, bf16[256,640]{1,0:T(8,128)(2,1)S(1)}, u32[]{:S(2)}, u32[]{:S(2)}) %collective-permute-start.25) | collective-permute-done | bytes 327712 | tf_op jit(solution)/shard_map/ppermute | solution.py:40
  133.1 7.5 %collective-permute-done.47.refs_0_ = bf16[80,2048]{1,0:T(8,128)(2,1)S(1)} collective-permute-done((bf16[80,2048]{1,0:T(8,128)(2,1)S(1)}, bf16[80,2048]{1,0:T(8,128)(2,1)S(1)}, u32[]{:S(2)}, u32[]{:S(2)}) %collective-permute-start.47) | collective-permute-done | bytes 327712 | tf_op jit(solution)/shard_map/ppermute | solution.py:40
  141.7 3.0 %ffn_weights.1 = (bf16[2048,640]{1,0:T(8,128)(2,1)S(1)}, bf16[4,384,512]{2,1,0:T(8,128)(2,1)S(1)}) custom-call(s32[3]{0:T(128)S(1)} %copy-done.12, bf16[512,640]{1,0:T(8,128)(2,1)S(1)} %copy-done.5, bf16[320,512]{1,0:T(8,128)(2,1)S(1)} %copy-done.6, bf16[256,640]{1,0:T(8,128)(2,1)S(1)} %collective-permute-done.21.refs_0_, ...), custom_call_target="tpu_custom_call" | custom-call | flops 1310720 | bytes 5242880 | tf_op jit(solution)/shard_map/ffn_weights/pallas_call | solution.py:407
  146.3 4.0 %collective-permute-done.55.refs_0_ = bf16[80,2048]{1,0:T(8,128)(2,1)S(1)} collective-permute-done((bf16[80,2048]{1,0:T(8,128)(2,1)S(1)}, bf16[80,2048]{1,0:T(8,128)(2,1)S(1)}, u32[]{:S(2)}, u32[]{:S(2)}) %collective-permute-start.55) | collective-permute-done | bytes 327712 | tf_op jit(solution)/shard_map/ppermute | solution.py:40
  151.3 4.8 %ffn_chunk.4 = (bf16[80,2048]{1,0:T(8,128)(2,1)S(1)}, bf16[80,2048]{1,0:T(8,128)(2,1)S(1)}, bf16[80,2048]{1,0:T(8,128)(2,1)S(1)}, bf16[80,2048]{1,0:T(8,128)(2,1)S(1)}) custom-call(s32[3]{0:T(128)S(1)} %copy-done.12, f32[3,640]{1,0:T(4,128)S(1)} %maximum_convert_fusion.taps_ref, bf16[2048,640]{1,0:T(8,128)(2,1)S(1)} %get-tuple-element.58.up, ...), custom_call_target="tpu_custom_call" | custom-call | flops 1258291200 | bytes 2621440 | tf_op jit(solution)/shard_map/ffn_chunk/pallas_call | solution.py:481
  158.7 4.8 %ffn_chunk.6 = (bf16[80,2048]{1,0:T(8,128)(2,1)S(1)}, bf16[80,2048]{1,0:T(8,128)(2,1)S(1)}, bf16[80,2048]{1,0:T(8,128)(2,1)S(1)}, bf16[80,2048]{1,0:T(8,128)(2,1)S(1)}) custom-call(s32[3]{0:T(128)S(1)} %copy-done.12, f32[3,640]{1,0:T(4,128)S(1)} %maximum_convert_fusion.taps_ref, bf16[2048,640]{1,0:T(8,128)(2,1)S(1)} %get-tuple-element.58.up, ...), custom_call_target="tpu_custom_call" | custom-call | flops 1258291200 | bytes 2621440 | tf_op jit(solution)/shard_map/ffn_chunk/pallas_call | solution.py:481
  165.2 5.0 %ffn_chunk.5 = (bf16[80,2048]{1,0:T(8,128)(2,1)S(1)}, bf16[80,2048]{1,0:T(8,128)(2,1)S(1)}, bf16[80,2048]{1,0:T(8,128)(2,1)S(1)}, bf16[80,2048]{1,0:T(8,128)(2,1)S(1)}) custom-call(s32[3]{0:T(128)S(1)} %copy-done.12, f32[3,640]{1,0:T(4,128)S(1)} %maximum_convert_fusion.taps_ref, bf16[2048,640]{1,0:T(8,128)(2,1)S(1)} %get-tuple-element.58.up, ...), custom_call_target="tpu_custom_call" | custom-call | flops 1258291200 | bytes 2621440 | tf_op jit(solution)/shard_map/ffn_chunk/pallas_call | solution.py:481
  170.8 4.8 %ffn_chunk.7 = (bf16[80,2048]{1,0:T(8,128)(2,1)S(1)}, bf16[80,2048]{1,0:T(8,128)(2,1)S(1)}, bf16[80,2048]{1,0:T(8,128)(2,1)S(1)}, bf16[80,2048]{1,0:T(8,128)(2,1)S(1)}) custom-call(s32[3]{0:T(128)S(1)} %copy-done.12, f32[3,640]{1,0:T(4,128)S(1)} %maximum_convert_fusion.taps_ref, bf16[2048,640]{1,0:T(8,128)(2,1)S(1)} %get-tuple-element.58.up, ...), custom_call_target="tpu_custom_call" | custom-call | flops 1258291200 | bytes 2621440 | tf_op jit(solution)/shard_map/ffn_chunk/pallas_call | solution.py:481
  178.1 14.4 %collective-permute-done.53 = bf16[80,2048]{1,0:T(8,128)(2,1)S(1)} collective-permute-done((bf16[80,2048]{1,0:T(8,128)(2,1)S(1)}, bf16[80,2048]{1,0:T(8,128)(2,1)S(1)}, u32[]{:S(2)}, u32[]{:S(2)}) %collective-permute-start.53) | collective-permute-done | bytes 327712 | tf_op jit(solution)/shard_map/ppermute | solution.py:40
  194.8 8.4 %collective-permute-done.45 = bf16[80,2048]{1,0:T(8,128)(2,1)S(1)} collective-permute-done((bf16[80,2048]{1,0:T(8,128)(2,1)S(1)}, bf16[80,2048]{1,0:T(8,128)(2,1)S(1)}, u32[]{:S(2)}, u32[]{:S(2)}) %collective-permute-start.45) | collective-permute-done | bytes 327712 | tf_op jit(solution)/shard_map/ppermute | solution.py:40
  203.4 1.8 collective-permute-start.46
  205.2 4.6 %collective-permute-done.61 = bf16[80,2048]{1,0:T(8,128)(2,1)S(1)} collective-permute-done((bf16[80,2048]{1,0:T(8,128)(2,1)S(1)}, bf16[80,2048]{1,0:T(8,128)(2,1)S(1)}, u32[]{:S(2)}, u32[]{:S(2)}) %collective-permute-start.61) | collective-permute-done | bytes 327712 | tf_op jit(solution)/shard_map/ppermute | solution.py:40
  210.8 12.2 %collective-permute-done.54.refs_6_ = bf16[80,2048]{1,0:T(8,128)(2,1)S(1)} collective-permute-done((bf16[80,2048]{1,0:T(8,128)(2,1)S(1)}, bf16[80,2048]{1,0:T(8,128)(2,1)S(1)}, u32[]{:S(2)}, u32[]{:S(2)}) %collective-permute-start.54) | collective-permute-done | bytes 327712 | tf_op jit(solution)/shard_map/ppermute | solution.py:40
  223.0 5.3 %collective-permute-done.62.refs_7_ = bf16[80,2048]{1,0:T(8,128)(2,1)S(1)} collective-permute-done((bf16[80,2048]{1,0:T(8,128)(2,1)S(1)}, bf16[80,2048]{1,0:T(8,128)(2,1)S(1)}, u32[]{:S(2)}, u32[]{:S(2)}) %collective-permute-start.62) | collective-permute-done | bytes 327712 | tf_op jit(solution)/shard_map/ppermute | solution.py:40
  (158 shorter events, 47.0 us)
Async XLA Ops:
  3.1 19.9 %collective-permute-start.4 = (bf16[256,512]{1,0:T(8,128)(2,1)}, bf16[256,512]{1,0:T(8,128)(2,1)S(1)}, u32[]{:S(2)}, u32[]{:S(2)}) collective-permute-start(bf16[256,512]{1,0:T(8,128)(2,1)} %get-tuple-element.41), channel_id=1, source_target_pairs={{0,8},{4,12},{8,0},{12,4},{1,9},{5,13},{9,1},{13,5},{2,10},{6,14},... | collective-permute-start | bytes 786440 | tf_op jit(solution)/shard_map/ppermute | solution.py:40
  9.1 21.4 %collective-permute-start.1 = (bf16[80,2048]{1,0:T(8,128)(2,1)S(1)}, bf16[80,2048]{1,0:T(8,128)(2,1)S(1)}, u32[]{:S(2)}, u32[]{:S(2)}) collective-permute-start(bf16[80,2048]{1,0:T(8,128)(2,1)S(1)} %shard_map.136.refs_0_), channel_id=1, source_target_pairs={{0,2},{1,3},{2,0},{3,1},{4,6},{5,7},{6,4},{7,5},{8,10},{9,11},{10,... | collective-permute-start | bytes 983048 | tf_op jit(solution)/shard_map/ppermute | solution.py:40
  11.0 19.6 %collective-permute-start.3 = (bf16[256,512]{1,0:T(8,128)(2,1)}, bf16[256,512]{1,0:T(8,128)(2,1)S(1)}, u32[]{:S(2)}, u32[]{:S(2)}) collective-permute-start(bf16[256,512]{1,0:T(8,128)(2,1)} %get-tuple-element.41), channel_id=1, source_target_pairs={{0,4},{4,0},{8,12},{12,8},{1,5},{5,1},{9,13},{13,9},{2,6},{6,2},{1... | collective-permute-start | bytes 786440 | tf_op jit(solution)/shard_map/ppermute | solution.py:40
  12.6 17.9 %collective-permute-start.12 = (bf16[128,512]{1,0:T(8,128)(2,1)}, bf16[128,512]{1,0:T(8,128)(2,1)S(1)}, u32[]{:S(2)}, u32[]{:S(2)}) collective-permute-start(bf16[128,512]{1,0:T(8,128)(2,1)} %get-tuple-element.44), channel_id=1, source_target_pairs={{0,4},{4,0},{8,12},{12,8},{1,5},{5,1},{9,13},{13,9},{2,6},{6,2},{1... | collective-permute-start | bytes 393224 | tf_op jit(solution)/shard_map/ppermute | solution.py:40
  23.1 15.4 %collective-permute-start.5 = (bf16[256,512]{1,0:T(8,128)(2,1)S(1)}, bf16[256,512]{1,0:T(8,128)(2,1)S(1)}, u32[]{:S(2)}, u32[]{:S(2)}) collective-permute-start(bf16[256,512]{1,0:T(8,128)(2,1)S(1)} %collective-permute-done.4.refs_7_), channel_id=1, source_target_pairs={{0,4},{4,0},{8,12},{12,8},{1,5},{5,1},{9,13},{13,9},{2,6},{6,2},{1... | collective-permute-start | bytes 786440 | tf_op jit(solution)/shard_map/ppermute | solution.py:40
  30.5 17.2 %collective-permute-start.2 = (bf16[80,2048]{1,0:T(8,128)(2,1)S(1)}, bf16[80,2048]{1,0:T(8,128)(2,1)S(1)}, u32[]{:S(2)}, u32[]{:S(2)}) collective-permute-start(bf16[80,2048]{1,0:T(8,128)(2,1)S(1)} %collective-permute-done.1.refs_2_), channel_id=1, source_target_pairs={{0,1},{1,0},{2,3},{3,2},{4,5},{5,4},{6,7},{7,6},{8,9},{9,8},{10,11... | collective-permute-start | bytes 983048 | tf_op jit(solution)/shard_map/ppermute | solution.py:40
  39.2 17.7 %collective-permute-start.16 = (bf16[128,512]{1,0:T(8,128)(2,1)S(1)}, bf16[128,512]{1,0:T(8,128)(2,1)S(1)}, u32[]{:S(2)}, u32[]{:S(2)}) collective-permute-start(bf16[128,512]{1,0:T(8,128)(2,1)S(1)} %collective-permute-done.13.refs_6_), channel_id=1, source_target_pairs={{0,16},{16,0},{1,17},{17,1},{2,18},{18,2},{3,19},{19,3},{4,20},{20... | collective-permute-start | bytes 393224 | tf_op jit(solution)/shard_map/ppermute | solution.py:40
  41.4 17.9 %collective-permute-start.15 = (bf16[128,512]{1,0:T(8,128)(2,1)}, bf16[128,512]{1,0:T(8,128)(2,1)S(1)}, u32[]{:S(2)}, u32[]{:S(2)}) collective-permute-start(bf16[128,512]{1,0:T(8,128)(2,1)} %copy-done.7), channel_id=1, source_target_pairs={{0,16},{16,0},{1,17},{17,1},{2,18},{18,2},{3,19},{19,3},{4,20},{20... | collective-permute-start | bytes 393224 | tf_op jit(solution)/shard_map/ppermute | solution.py:40
  68.4 26.8 %collective-permute-start.21 = (bf16[256,640]{1,0:T(8,128)(2,1)}, bf16[256,640]{1,0:T(8,128)(2,1)S(1)}, u32[]{:S(2)}, u32[]{:S(2)}) collective-permute-start(bf16[256,640]{1,0:T(8,128)(2,1)} %get-tuple-element.52), channel_id=1, source_target_pairs={{0,4},{4,0},{8,12},{12,8},{1,5},{5,1},{9,13},{13,9},{2,6},{6,2},{1... | collective-permute-start | bytes 983048 | tf_op jit(solution)/shard_map/ppermute | solution.py:40
  69.5 16.2 %collective-permute-start.27 = (bf16[160,512]{1,0:T(8,128)(2,1)}, bf16[160,512]{1,0:T(8,128)(2,1)S(1)}, u32[]{:S(2)}, u32[]{:S(2)}) collective-permute-start(bf16[160,512]{1,0:T(8,128)(2,1)} %get-tuple-element.55), channel_id=1, source_target_pairs={{0,4},{4,0},{8,12},{12,8},{1,5},{5,1},{9,13},{13,9},{2,6},{6,2},{1... | collective-permute-start | bytes 491528 | tf_op jit(solution)/shard_map/ppermute | solution.py:40
  70.4 16.4 %collective-permute-start.28 = (bf16[160,512]{1,0:T(8,128)(2,1)}, bf16[160,512]{1,0:T(8,128)(2,1)}, u32[]{:S(2)}, u32[]{:S(2)}) collective-permute-start(bf16[160,512]{1,0:T(8,128)(2,1)} %get-tuple-element.56), channel_id=1, source_target_pairs={{0,8},{4,12},{8,0},{12,4},{1,9},{5,13},{9,1},{13,5},{2,10},{6,14},... | collective-permute-start | bytes 491528 | tf_op jit(solution)/shard_map/ppermute | solution.py:40
  74.9 18.3 %collective-permute-start.29 = (bf16[160,512]{1,0:T(8,128)(2,1)}, bf16[160,512]{1,0:T(8,128)(2,1)}, u32[]{:S(2)}, u32[]{:S(2)}) collective-permute-start(bf16[160,512]{1,0:T(8,128)(2,1)} %get-tuple-element.57), channel_id=1, source_target_pairs={{0,12},{4,8},{8,4},{12,0},{1,13},{5,9},{9,5},{13,1},{2,14},{6,10},... | collective-permute-start | bytes 491528 | tf_op jit(solution)/shard_map/ppermute | solution.py:40
  75.1 21.6 %collective-permute-start.18 = (bf16[80,2048]{1,0:T(8,128)(2,1)}, bf16[80,2048]{1,0:T(8,128)(2,1)S(1)}, u32[]{:S(2)}, u32[]{:S(2)}) collective-permute-start(bf16[80,2048]{1,0:T(8,128)(2,1)} %get-tuple-element.46), channel_id=1, source_target_pairs={{0,1},{1,0},{2,3},{3,2},{4,5},{5,4},{6,7},{7,6},{8,9},{9,8},{10,11... | collective-permute-start | bytes 983048 | tf_op jit(solution)/shard_map/ppermute | solution.py:40
  86.9 29.2 %collective-permute-start.22 = (bf16[256,640]{1,0:T(8,128)(2,1)}, bf16[256,640]{1,0:T(8,128)(2,1)S(1)}, u32[]{:S(2)}, u32[]{:S(2)}) collective-permute-start(bf16[256,640]{1,0:T(8,128)(2,1)} %get-tuple-element.53), channel_id=1, source_target_pairs={{0,8},{4,12},{8,0},{12,4},{1,9},{5,13},{9,1},{13,5},{2,10},{6,14},... | collective-permute-start | bytes 983048 | tf_op jit(solution)/shard_map/ppermute | solution.py:40
  93.3 24.3 %collective-permute-start.23 = (bf16[256,640]{1,0:T(8,128)(2,1)}, bf16[256,640]{1,0:T(8,128)(2,1)S(1)}, u32[]{:S(2)}, u32[]{:S(2)}) collective-permute-start(bf16[256,640]{1,0:T(8,128)(2,1)} %get-tuple-element.54), channel_id=1, source_target_pairs={{0,12},{4,8},{8,4},{12,0},{1,13},{5,9},{9,5},{13,1},{2,14},{6,10},... | collective-permute-start | bytes 983048 | tf_op jit(solution)/shard_map/ppermute | solution.py:40
  95.1 23.0 %collective-permute-start.30 = (bf16[160,512]{1,0:T(8,128)(2,1)S(1)}, bf16[160,512]{1,0:T(8,128)(2,1)}, u32[]{:S(2)}, u32[]{:S(2)}) collective-permute-start(bf16[160,512]{1,0:T(8,128)(2,1)S(1)} %collective-permute-done.27.refs_6_), channel_id=1, source_target_pairs={{0,16},{16,0},{1,17},{17,1},{2,18},{18,2},{3,19},{19,3},{4,20},{20... | collective-permute-start | bytes 491528 | tf_op jit(solution)/shard_map/ppermute | solution.py:40
  96.7 23.0 %collective-permute-start.31 = (bf16[160,512]{1,0:T(8,128)(2,1)}, bf16[160,512]{1,0:T(8,128)(2,1)}, u32[]{:S(2)}, u32[]{:S(2)}) collective-permute-start(bf16[160,512]{1,0:T(8,128)(2,1)} %collective-permute-done.28.refs_7_), channel_id=1, source_target_pairs={{0,16},{16,0},{1,17},{17,1},{2,18},{18,2},{3,19},{19,3},{4,20},{20... | collective-permute-start | bytes 491528 | tf_op jit(solution)/shard_map/ppermute | solution.py:40
  97.2 29.0 %collective-permute-start.32 = (bf16[160,512]{1,0:T(8,128)(2,1)}, bf16[160,512]{1,0:T(8,128)(2,1)}, u32[]{:S(2)}, u32[]{:S(2)}) collective-permute-start(bf16[160,512]{1,0:T(8,128)(2,1)} %collective-permute-done.29.refs_8_), channel_id=1, source_target_pairs={{0,16},{16,0},{1,17},{17,1},{2,18},{18,2},{3,19},{19,3},{4,20},{20... | collective-permute-start | bytes 491528 | tf_op jit(solution)/shard_map/ppermute | solution.py:40
  117.6 15.5 %collective-permute-start.25 = (bf16[256,640]{1,0:T(8,128)(2,1)S(1)}, bf16[256,640]{1,0:T(8,128)(2,1)S(1)}, u32[]{:S(2)}, u32[]{:S(2)}) collective-permute-start(bf16[256,640]{1,0:T(8,128)(2,1)S(1)} %collective-permute-done.22.refs_1_), channel_id=1, source_target_pairs={{0,16},{16,0},{1,17},{17,1},{2,18},{18,2},{3,19},{19,3},{4,20},{20... | collective-permute-start | bytes 983048 | tf_op jit(solution)/shard_map/ppermute | solution.py:40
  118.1 22.5 %collective-permute-start.26 = (bf16[256,640]{1,0:T(8,128)(2,1)S(1)}, bf16[256,640]{1,0:T(8,128)(2,1)S(1)}, u32[]{:S(2)}, u32[]{:S(2)}) collective-permute-start(bf16[256,640]{1,0:T(8,128)(2,1)S(1)} %collective-permute-done.23.refs_2_), channel_id=1, source_target_pairs={{0,16},{16,0},{1,17},{17,1},{2,18},{18,2},{3,19},{19,3},{4,20},{20... | collective-permute-start | bytes 983048 | tf_op jit(solution)/shard_map/ppermute | solution.py:40
  119.6 21.0 %collective-permute-start.47 = (bf16[80,2048]{1,0:T(8,128)(2,1)S(1)}, bf16[80,2048]{1,0:T(8,128)(2,1)S(1)}, u32[]{:S(2)}, u32[]{:S(2)}) collective-permute-start(bf16[80,2048]{1,0:T(8,128)(2,1)S(1)} %get-tuple-element.60.refs_0_), channel_id=1, source_target_pairs={{0,8},{4,12},{8,0},{12,4},{1,9},{5,13},{9,1},{13,5},{2,10},{6,14},... | collective-permute-start | bytes 983048 | tf_op jit(solution)/shard_map/ppermute | solution.py:40
  126.2 15.5 %collective-permute-start.34 = (bf16[80,2048]{1,0:T(8,128)(2,1)S(1)}, bf16[80,2048]{1,0:T(8,128)(2,1)S(1)}, u32[]{:S(2)}, u32[]{:S(2)}) collective-permute-start(bf16[80,2048]{1,0:T(8,128)(2,1)S(1)} %get-tuple-element.60.refs_0_), channel_id=1, source_target_pairs={{0,2},{1,3},{2,0},{3,1},{4,6},{5,7},{6,4},{7,5},{8,10},{9,11},{10,... | collective-permute-start | bytes 983048 | tf_op jit(solution)/shard_map/ppermute | solution.py:40
  128.0 16.7 %collective-permute-start.39 = (bf16[80,2048]{1,0:T(8,128)(2,1)S(1)}, bf16[80,2048]{1,0:T(8,128)(2,1)S(1)}, u32[]{:S(2)}, u32[]{:S(2)}) collective-permute-start(bf16[80,2048]{1,0:T(8,128)(2,1)S(1)} %get-tuple-element.60.refs_0_), channel_id=1, source_target_pairs={{0,4},{4,0},{8,12},{12,8},{1,5},{5,1},{9,13},{13,9},{2,6},{6,2},{1... | collective-permute-start | bytes 983048 | tf_op jit(solution)/shard_map/ppermute | solution.py:40
  164.6 46.1 %collective-permute-start.36 = (bf16[80,2048]{1,0:T(8,128)(2,1)S(1)}, bf16[80,2048]{1,0:T(8,128)(2,1)S(1)}, u32[]{:S(2)}, u32[]{:S(2)}) collective-permute-start(bf16[80,2048]{1,0:T(8,128)(2,1)S(1)} %get-tuple-element.62), channel_id=1, source_target_pairs={{0,1},{1,0},{2,3},{3,2},{4,5},{5,4},{6,7},{7,6},{8,9},{9,8},{10,11... | collective-permute-start | bytes 983048 | tf_op jit(solution)/shard_map/ppermute | solution.py:40
  170.4 23.4 %collective-permute-start.43 = (bf16[80,2048]{1,0:T(8,128)(2,1)S(1)}, bf16[80,2048]{1,0:T(8,128)(2,1)S(1)}, u32[]{:S(2)}, u32[]{:S(2)}) collective-permute-start(bf16[80,2048]{1,0:T(8,128)(2,1)S(1)} %get-tuple-element.66), channel_id=1, source_target_pairs={{0,1},{1,0},{2,3},{3,2},{4,5},{5,4},{6,7},{7,6},{8,9},{9,8},{10,11... | collective-permute-start | bytes 983048 | tf_op jit(solution)/shard_map/ppermute | solution.py:40
  175.6 35.1 %collective-permute-start.38 = (bf16[80,2048]{1,0:T(8,128)(2,1)S(1)}, bf16[80,2048]{1,0:T(8,128)(2,1)S(1)}, u32[]{:S(2)}, u32[]{:S(2)}) collective-permute-start(bf16[80,2048]{1,0:T(8,128)(2,1)S(1)} %add_convert_fusion.6), channel_id=1, source_target_pairs={{0,2},{1,3},{2,0},{3,1},{4,6},{5,7},{6,4},{7,5},{8,10},{9,11},{10,... | collective-permute-start | bytes 983048 | tf_op jit(solution)/shard_map/ppermute | solution.py:40
  176.8 15.6 %collective-permute-start.53 = (bf16[80,2048]{1,0:T(8,128)(2,1)S(1)}, bf16[80,2048]{1,0:T(8,128)(2,1)S(1)}, u32[]{:S(2)}, u32[]{:S(2)}) collective-permute-start(bf16[80,2048]{1,0:T(8,128)(2,1)S(1)} %add_convert_fusion.3), channel_id=1, source_target_pairs={{0,2},{1,3},{2,0},{3,1},{4,6},{5,7},{6,4},{7,5},{8,10},{9,11},{10,... | collective-permute-start | bytes 983048 | tf_op jit(solution)/shard_map/ppermute | solution.py:40
  178.0 14.6 %collective-permute-start.60 = (bf16[80,2048]{1,0:T(8,128)(2,1)S(1)}, bf16[80,2048]{1,0:T(8,128)(2,1)S(1)}, u32[]{:S(2)}, u32[]{:S(2)}) collective-permute-start(bf16[80,2048]{1,0:T(8,128)(2,1)S(1)} %get-tuple-element.76), channel_id=1, source_target_pairs={{0,1},{1,0},{2,3},{3,2},{4,5},{5,4},{6,7},{7,6},{8,9},{9,8},{10,11... | collective-permute-start | bytes 983048 | tf_op jit(solution)/shard_map/ppermute | solution.py:40
  193.7 16.1 %collective-permute-start.61 = (bf16[80,2048]{1,0:T(8,128)(2,1)S(1)}, bf16[80,2048]{1,0:T(8,128)(2,1)S(1)}, u32[]{:S(2)}, u32[]{:S(2)}) collective-permute-start(bf16[80,2048]{1,0:T(8,128)(2,1)S(1)} %add_convert_fusion.1), channel_id=1, source_target_pairs={{0,2},{1,3},{2,0},{3,1},{4,6},{5,7},{6,4},{7,5},{8,10},{9,11},{10,... | collective-permute-start | bytes 983048 | tf_op jit(solution)/shard_map/ppermute | solution.py:40
  203.2 19.7 %collective-permute-start.54 = (bf16[80,2048]{1,0:T(8,128)(2,1)S(1)}, bf16[80,2048]{1,0:T(8,128)(2,1)S(1)}, u32[]{:S(2)}, u32[]{:S(2)}) collective-permute-start(bf16[80,2048]{1,0:T(8,128)(2,1)S(1)} %add_convert_fusion.2), channel_id=1, source_target_pairs={{0,8},{4,12},{8,0},{12,4},{1,9},{5,13},{9,1},{13,5},{2,10},{6,14},... | collective-permute-start | bytes 983048 | tf_op jit(solution)/shard_map/ppermute | solution.py:40
  203.4 19.6 %collective-permute-start.46 = (bf16[80,2048]{1,0:T(8,128)(2,1)S(1)}, bf16[80,2048]{1,0:T(8,128)(2,1)S(1)}, u32[]{:S(2)}, u32[]{:S(2)}) collective-permute-start(bf16[80,2048]{1,0:T(8,128)(2,1)S(1)} %add_convert_fusion.4), channel_id=1, source_target_pairs={{0,4},{4,0},{8,12},{12,8},{1,5},{5,1},{9,13},{13,9},{2,6},{6,2},{1... | collective-permute-start | bytes 983048 | tf_op jit(solution)/shard_map/ppermute | solution.py:40
  209.9 18.4 %collective-permute-start.62 = (bf16[80,2048]{1,0:T(8,128)(2,1)S(1)}, bf16[80,2048]{1,0:T(8,128)(2,1)S(1)}, u32[]{:S(2)}, u32[]{:S(2)}) collective-permute-start(bf16[80,2048]{1,0:T(8,128)(2,1)S(1)} %add_convert_fusion), channel_id=1, source_target_pairs={{0,12},{4,8},{8,4},{12,0},{1,13},{5,9},{9,5},{13,1},{2,14},{6,10},... | collective-permute-start | bytes 983048 | tf_op jit(solution)/shard_map/ppermute | solution.py:40
  (47 other events, 864.5 us)

commit v2 on v1

--- a/solution.py
+++ b/solution.py
@@ -110,12 +110,11 @@
 
 
 def glu_conv(spot, sizes, blocks, val, gate, pieces, taps):
-    ng, nf, nt = sizes
+    _, nf, nt = sizes
     rows, width = blocks[0].shape
     total = nt * rows
     depth, channels = val.shape
     packed = 2 * channels
-    share = depth // ng
     count = taps.shape[0]
     lead = -(-(count - 1) // 8) * 8
     segments = total // LEN
@@ -132,8 +131,8 @@
             columns = pl.ds(i * channels, channels)
             pairs.append((ref, weight.at[aligned(slab, depth), columns]))
         for (d, e), ref in zip(keys, piece_refs):
-            place = (slab ^ d) * ng + (group ^ e)
-            pairs.append((ref, weight.at[aligned(place, share)]))
+            columns = pl.ds(pl.multiple_of((group ^ e) * channels, LANES), channels)
+            pairs.append((ref, weight.at[aligned(slab ^ d, depth), columns]))
         copies = start_copies(pairs, sems)
         padded[:, :lead, :] = jnp.zeros((segments, lead, channels), F32)
         for copy in copies:
@@ -216,10 +215,16 @@
         activated = (scaled * jax.nn.sigmoid(scaled)).astype(BF16)
         for copy in copies:
             copy.wait()
+        outward = []
         for s in range(nf):
-            mixed[:, s * cols : (s + 1) * cols] = product(activated, weight[s]).astype(BF16)
-        targets = [(mixed.at[aligned(member ^ d, rows)], out_refs[d]) for d in range(nt)]
-        for copy in start_copies(targets, sems):
+            columns = pl.ds(s * cols, cols)
+            mixed[:, columns] = product(activated, weight[s]).astype(BF16)
+            targets = [
+                (mixed.at[aligned(member ^ d, rows), columns], out_refs[d].at[:, columns])
+                for d in range(nt)
+            ]
+            outward += start_copies(targets, sems, 1 + len(keys) + len(outward))
+        for copy in outward:
             copy.wait()
 
     return pl.pallas_call(
@@ -230,7 +235,7 @@
         scratch_shapes=[
             pltpu.VMEM((nf, depth, cols), BF16),
             pltpu.VMEM((total, nf * cols), BF16),
-            pltpu.SemaphoreType.DMA((max(nt, 1 + len(keys)),)),
+            pltpu.SemaphoreType.DMA((1 + len(keys) + nf * nt,)),
         ],
         cost_estimate=pl.CostEstimate(
             flops=2 * total * channels * nf * cols,
@@ -240,46 +245,6 @@
         compiler_params=pltpu.CompilerParams(vmem_limit_bytes=24 * MEBI),
         name="out_product",
     )(spot, conv, gain, *sums, own, *pieces.values())
-
-
-def mix_shares(spot, sizes, val, gate, out):
-    ng = sizes[0]
-    depth, channels = val.shape
-    tall, cols = out.shape
-
-    def run(spot_ref, val_ref, gate_ref, out_ref, glu_share, out_share, glu_held, out_held, sems):
-        group = spot_ref[0]
-        rows = aligned(group, depth // ng)
-        pairs = [
-            (val_ref.at[rows], glu_held.at[:, pl.ds(0, channels)]),
-            (gate_ref.at[rows], glu_held.at[:, pl.ds(channels, channels)]),
-            (out_ref.at[aligned(group, tall // ng)], out_held),
-        ]
-        copies = start_copies(pairs, sems)
-        for copy in copies[:2]:
-            copy.wait()
-        outward = start_copies([(glu_held, glu_share)], sems, 3)
-        copies[2].wait()
-        outward += start_copies([(out_held, out_share)], sems, 4)
-        for copy in outward:
-            copy.wait()
-
-    return pl.pallas_call(
-        run,
-        in_specs=[SMEM, HBM, HBM, HBM],
-        out_specs=[ANY, ANY],
-        out_shape=[
-            jax.ShapeDtypeStruct((depth // ng, 2 * channels), BF16),
-            jax.ShapeDtypeStruct((tall // ng, cols), BF16),
-        ],
-        scratch_shapes=[
-            pltpu.VMEM((depth // ng, 2 * channels), BF16),
-            pltpu.VMEM((tall // ng, cols), BF16),
-            pltpu.SemaphoreType.DMA((5,)),
-        ],
-        compiler_params=pltpu.CompilerParams(vmem_limit_bytes=60 * MEBI),
-        name="mix_shares",
-    )(spot, val, gate, out)
 
 
 def ffn_shares(spot, sizes, gate, val, down):
@@ -296,8 +261,7 @@
 
     def run(spot_ref, *refs):
         sources, refs = refs[:3], refs[3:]
-        up_refs, refs = refs[:count], refs[count:]
-        down_refs, refs = refs[:count], refs[count:]
+        out_refs, refs = refs[:count], refs[count:]
         up_own_ref, down_own_ref, gate_ref, val_ref, down_ref, halves, sems = refs
         group, slab = spot_ref[0], spot_ref[1]
         rows = aligned(group, share)
@@ -315,16 +279,18 @@
         for d in range(1, nf):
             there = slab ^ d
             columns = pl.ds(pl.multiple_of(there * whole, LANES), whole)
+            out = out_refs[d - 1]
             for i, ref in enumerate((gate_ref, val_ref)):
-                pairs.append((ref.at[rows, columns], up_refs[d - 1].at[:, pl.ds(i * whole, whole)]))
+                target = out.at[pl.ds(0, share), pl.ds(i * whole, whole)]
+                pairs.append((ref.at[rows, columns], target))
             first = pl.multiple_of(there * whole + group * tall[0], 16)
-            pairs.append(
-                (down_ref.at[pl.ds(first, tall[0])], down_refs[d - 1].at[pl.ds(0, tall[0])])
-            )
-            if rest:
-                first = pl.multiple_of(nf * whole + there * rest + group * tall[1], 16)
-                part = down_refs[d - 1].at[pl.ds(tall[0], tall[1])]
-                pairs.append((down_ref.at[pl.ds(first, tall[1])], part))
+            target = out.at[pl.ds(share, tall[0]), pl.ds(0, cols)]
+            pairs.append((down_ref.at[pl.ds(first, tall[0])], target))
+            first = pl.multiple_of(nf * whole + there * rest + group * tall[1], 16)
+            for q in range(cols // LANES):
+                source = down_ref.at[pl.ds(first, tall[1]), pl.ds(q * LANES, LANES)]
+                target = out.at[pl.ds(share + q * tall[1], tall[1]), pl.ds(cols, LANES)]
+                pairs.append((source, target))
         copies = start_copies(pairs, sems, 3)
         if rest:
             lane = lax.broadcasted_iota(jnp.int32, (depth, LANES), 1)
@@ -335,7 +301,10 @@
                 pair[moved] = pltpu.roll(pair[moved], rest, 1)
                 halves[s] = jnp.where(lane < rest, pair[0], pair[1]).astype(BF16)
             pairs = [
-                (halves.at[slab ^ d, rows], up_refs[d - 1].at[:, pl.ds(2 * whole, LANES)])
+                (
+                    halves.at[slab ^ d, rows],
+                    out_refs[d - 1].at[pl.ds(0, share), pl.ds(2 * whole, LANES)],
+                )
                 for d in range(1, nf)
             ]
             pairs.append((halves.at[slab], up_own_ref.at[:, pl.ds(2 * whole, LANES)]))
@@ -346,9 +315,8 @@
     outs = pl.pallas_call(
         run,
         in_specs=[SMEM, HBM, HBM, HBM],
-        out_specs=[ANY] * (2 * count + 2),
-        out_shape=[jax.ShapeDtypeStruct((share, packed), BF16)] * count
-        + [jax.ShapeDtypeStruct((units // ng, cols), BF16)] * count
+        out_specs=[ANY] * (count + 2),
+        out_shape=[jax.ShapeDtypeStruct((share + tall[0], packed), BF16)] * count
         + [jax.ShapeDtypeStruct((depth, packed), BF16)]
         + [jax.ShapeDtypeStruct((units, cols), BF16)],
         scratch_shapes=[
@@ -356,7 +324,7 @@
             pltpu.VMEM(val.shape, BF16),
             pltpu.VMEM(down.shape, BF16),
             pltpu.VMEM((nf, depth, LANES), BF16),
-            pltpu.SemaphoreType.DMA((8 + 5 * count,)),
+            pltpu.SemaphoreType.DMA((8 + (4 + cols // LANES) * count,)),
         ],
         cost_estimate=pl.CostEstimate(
             flops=depth * packed, transcendentals=0, bytes_accessed=8 * depth * packed
@@ -364,12 +332,10 @@
         compiler_params=pltpu.CompilerParams(vmem_limit_bytes=60 * MEBI),
         name="ffn_shares",
     )(spot, gate, val, down)
-    ups = {d: outs[d - 1] for d in range(1, nf)}
-    downs = {d: outs[count + d - 1] for d in range(1, nf)}
-    return ups, downs, outs[-2], outs[-1]
-
-
-def ffn_weights(spot, sizes, up_own, up_pieces, down_own, down_pieces):
+    return {d: outs[d - 1] for d in range(1, nf)}, outs[-2], outs[-1]
+
+
+def ffn_weights(spot, sizes, up_own, down_own, pieces):
     ng, nf, _ = sizes
     depth, packed = up_own.shape
     units, cols = down_own.shape
@@ -378,26 +344,26 @@
     padded = -(-units // LANES) * LANES
     share = depth // ng
     tall = (whole // ng, rest // ng)
-    keys = list(up_pieces)
+    keys = list(pieces)
 
     def run(spot_ref, up_own_ref, down_own_ref, *refs):
-        up_refs, refs = refs[: len(keys)], refs[len(keys) :]
-        down_refs, refs = refs[: len(keys)], refs[len(keys) :]
+        piece_refs, refs = refs[: len(keys)], refs[len(keys) :]
         up, down, sems = refs
         group, slab = spot_ref[0], spot_ref[1]
         pairs = [
             (up_own_ref, up.at[aligned(slab, depth)]),
             (down_own_ref, down.at[slab, pl.ds(0, units)]),
         ]
-        for (d, e), up_ref, down_ref in zip(keys, up_refs, down_refs):
+        for (d, e), ref in zip(keys, piece_refs):
             place = (slab ^ d) * ng + (group ^ e)
-            pairs.append((up_ref, up.at[aligned(place, share)]))
-            target = down.at[slab ^ d, aligned(group ^ e, tall[0])]
-            pairs.append((down_ref.at[pl.ds(0, tall[0])], target))
-            if rest:
-                first = pl.multiple_of(whole + (group ^ e) * tall[1], 16)
-                target = down.at[slab ^ d, pl.ds(first, tall[1])]
-                pairs.append((down_ref.at[pl.ds(tall[0], tall[1])], target))
+            pairs.append((ref.at[pl.ds(0, share)], up.at[aligned(place, share)]))
+            source = ref.at[pl.ds(share, tall[0]), pl.ds(0, cols)]
+            pairs.append((source, down.at[slab ^ d, aligned(group ^ e, tall[0])]))
+            first = pl.multiple_of(whole + (group ^ e) * tall[1], 16)
+            for q in range(cols // LANES):
+                source = ref.at[pl.ds(share + q * tall[1], tall[1]), pl.ds(cols, LANES)]
+                target = down.at[slab ^ d, pl.ds(first, tall[1]), pl.ds(q * LANES, LANES)]
+                pairs.append((source, target))
         copies = start_copies(pairs, sems)
         if padded > units:
             down[:, units:, :] = jnp.zeros((nf, padded - units, cols), BF16)
@@ -406,19 +372,19 @@
 
     return pl.pallas_call(
         run,
-        in_specs=[SMEM] + [ANY] * (2 + 2 * len(keys)),
+        in_specs=[SMEM] + [ANY] * (2 + len(keys)),
         out_specs=[VMEM, VMEM],
         out_shape=[
             jax.ShapeDtypeStruct((nf * depth, packed), BF16),
             jax.ShapeDtypeStruct((nf, padded, cols), BF16),
         ],
-        scratch_shapes=[pltpu.SemaphoreType.DMA((2 + 3 * len(keys),))],
+        scratch_shapes=[pltpu.SemaphoreType.DMA((2 + (2 + cols // LANES) * len(keys),))],
         cost_estimate=pl.CostEstimate(
             flops=nf * depth * packed, transcendentals=0, bytes_accessed=4 * nf * depth * packed
         ),
         compiler_params=pltpu.CompilerParams(vmem_limit_bytes=12 * MEBI),
         name="ffn_weights",
-    )(spot, up_own, down_own, *up_pieces.values(), *down_pieces.values())
+    )(spot, up_own, down_own, *pieces.values())
 
 
 def ffn_chunk(spot, sizes, blocks, up, taps, down):
@@ -497,6 +463,10 @@
     )(spot, taps, up, down, *[blocks[d] for d in range(nt)])
 
 
+def middle_pair(nf, d):
+    return nf == 4 and d == nf - 1
+
+
 def exchange_shards(sizes):
     ng, nf, nt = sizes
 
@@ -526,15 +496,25 @@
                     pieces[d, e] = swap(blocks[d], "grp", ng, e)
             return pieces
 
-        def fetch(shares):
-            sent = {d: swap(shares[d], "fs", nf, d) for d in shares}
+        def fetch(shares, inner):
+            sent = {}
+            for d in shares:
+                pairs = [(i, i ^ d) for i in range(nf)]
+                early = [p for p in pairs if middle_pair(nf, d) and abs(p[0] - p[1]) == 1]
+                late = [p for p in pairs if p not in early]
+                sent[d] = lax.ppermute(shares[d], "fs", late)
+                if early:
+                    first = lax.ppermute(shares[d], "fs", early)
+                    sent[d] = jnp.where(inner, first, sent[d])
             return share_out(sent)
 
         def fetch_all(mine):
             return share_out(gather_blocks(mine, "fs", nf))
 
         local_ch = val_weight.shape[1]
-        glu_share, out_share = mix_shares(spot, sizes, val_weight, gate_weight, out_weight)
+        glu_share = jnp.where(group == 0, val_weight, gate_weight)
+        out_rows = out_weight.shape[0] // ng
+        out_share = lax.dynamic_slice_in_dim(out_weight, group * out_rows, out_rows, 0)
         glu_pieces = fetch_all(glu_share)
         out_pieces = fetch_all(out_share)
 
@@ -542,11 +522,6 @@
         units = local_ff // nf
         whole = units // LANES * LANES
         rest = units - whole
-        up_shares, down_shares, up_own, down_own = ffn_shares(
-            spot, sizes, up_gate_weight, up_val_weight, down_weight
-        )
-        up_pieces, down_pieces = fetch(up_shares), fetch(down_shares)
-        up_full, down_full = ffn_weights(spot, sizes, up_own, up_pieces, down_own, down_pieces)
         begin = member * local_ff
         taps_whole = lax.dynamic_slice_in_dim(ffn_taps, begin + slab * whole, whole, 2)
         own_taps = [taps_whole[0], taps_whole[1]]
@@ -556,16 +531,30 @@
             own_taps += [taps_rest[0], taps_rest[1]]
         own_taps = jnp.concatenate(own_taps, axis=1).astype(F32)
 
+        mix_taps = lax.dynamic_slice_in_dim(conv_taps, member * local_ch, local_ch, 1)
+        own_gain = lax.dynamic_slice_in_dim(chan_gain[None], member * local_ch, local_ch, 1)
+        mix_taps, own_gain = mix_taps.astype(F32), own_gain.astype(F32)
+        post_gain, next_gain, last_gain = (
+            gain[None] for gain in (mix_post_gain, ffn_gain, ffn_post_gain)
+        )
+        inner = (slab > 0) & (slab < nf - 1)
+        small = (own_taps, mix_taps, own_gain, post_gain, next_gain, last_gain, inner)
+        spot, small = lax.optimization_barrier((spot, small))
+        own_taps, mix_taps, own_gain, post_gain, next_gain, last_gain, inner = small
+        ffn_parts, up_own, down_own = ffn_shares(
+            spot, sizes, up_gate_weight, up_val_weight, down_weight
+        )
+        ffn_pieces = fetch(ffn_parts, inner)
+        up_full, down_full = ffn_weights(spot, sizes, up_own, down_own, ffn_pieces)
+
         def scaled(values, gain):
             mean = jnp.mean(values * values, axis=-1, keepdims=True)
             return values * lax.rsqrt(mean + norm_epsilon) * gain
 
-        mix_taps = lax.dynamic_slice_in_dim(conv_taps, member * local_ch, local_ch, 1)
-        own_gain = lax.dynamic_slice_in_dim(chan_gain[None], member * local_ch, local_ch, 1)
         (normed,) = row_kernel(lambda t, g: (scaled(t, g),), [tokens, mix_gain[None]], 1)
         row_blocks = gather_blocks(normed, "tp", nt)
         conv, sums = glu_conv(
-            spot, sizes, row_blocks, val_weight, gate_weight, glu_pieces, mix_taps.astype(F32)
+            spot, sizes, row_blocks, val_weight, gate_weight, glu_pieces, mix_taps
         )
         all_sums = [sums] + [swap(sums, "tp", nt, d) for d in range(1, nt)]
         mixed = out_product(
@@ -573,7 +562,7 @@
             sizes,
             conv,
             all_sums,
-            own_gain.astype(F32),
+            own_gain,
             chan_gain.shape[0],
             out_weight,
             out_pieces,
@@ -584,9 +573,7 @@
             result = (t + scaled(sum(parts), post)).astype(BF16).astype(F32)
             return result, scaled(result, gain)
 
-        residual, acted = row_kernel(
-            residual_rows, [tokens, mix_post_gain[None], ffn_gain[None], *terms], 2
-        )
+        residual, acted = row_kernel(residual_rows, [tokens, post_gain, next_gain, *terms], 2)
 
         last = []
         acts = gather_blocks(acted, "fs", nf)
@@ -598,9 +585,7 @@
                 terms = [swap(add_terms(terms), "fs", nf, d)]
             last += terms
         (result,) = row_kernel(
-            lambda r, gain, *parts: (r + scaled(sum(parts), gain),),
-            [residual, ffn_post_gain[None], *last],
-            1,
+            lambda r, gain, *parts: (r + scaled(sum(parts), gain),), [residual, last_gain, *last], 1
         )
         return result
 
@@ -684,11 +669,14 @@
         P(),
     )
     powers = all(size & (size - 1) == 0 for size in sizes)
-    exchange = powers and sizes[1] * sizes[2] <= 16
+    exchange = powers and sizes[0] == 2 and sizes[1] * sizes[2] <= 16
 
     def run(*args):
         units = args[9].shape[1] // (sizes[1] * sizes[2])
-        cuts = units % LANES in (0, LANES // 2) and units % (32 * sizes[0]) == 0
+        cols = args[12].shape[1] // sizes[1]
+        whole = units // LANES * LANES
+        cuts = units - whole == LANES // 2 and cols + LANES == 2 * units
+        cuts = cuts and cols // LANES * (units - whole) == whole and whole % (32 * sizes[0]) == 0
         shards = exchange_shards(sizes) if exchange and cuts else gather_shards
         return jax.shard_map(
             shards,

time: 233 us -> 222 us (0.953)
  starting transfers between devices: 62.5 us -> 51.7 us
  Pallas kernels: 39.1 us -> 35.9 us
    ppermute x0 -> x4, waiting for transfers between devices: none -> 36.4 us  [the longest x3 36.4 us: fetch(): sent[d] = lax.ppermute(shares[d], 'fs', late)]
    ppermute x63 -> x54, waiting for transfers between devices: 121 us -> 85.1 us  [swap(): return lax.ppermute(array, axis, [(i, i ^ bits) for i in range(size)])]
    ppermute x63 -> x54, starting transfers between devices: 62.5 us -> 44.5 us  [swap(): return lax.ppermute(array, axis, [(i, i ^ bits) for i in range(size)])]
    ppermute x0 -> x4, starting transfers between devices: none -> 7.18 us  [the longest x3 6.35 us: fetch(): sent[d] = lax.ppermute(shares[d], 'fs', late)]
    pallas_call x3 -> x2, Pallas kernels: 9.93 us -> 6.79 us  [the longest x1 4.49 us: ffn_shares(): pl.pallas_call(run, in_specs=[SMEM, HBM, HBM, HBM], out_specs=[ANY] * (co...]
  transfers between devices with their start and end apart: 63 -> 58, of which waited for: 19 -> 21; matrix products, arithmetic and copies ran while one was open for 2% -> 3% of each run, Pallas kernels for 14% -> 14%
where the time goes in v2:
time: 222 us; the launch traced here: 219 us
  waiting for transfers between devices  121 us (55%)
  starting transfers between devices  51.7 us (23%)
  Pallas kernels  35.9 us (16%)
  local copies, waits for them, and re-layouts  5.71 us (3%)
  other arithmetic  3.49 us (2%)
    ppermute x54, waiting for transfers between devices, swap(): return lax.ppermute(array, axis, [(i, i ^ bits) for i in range(size)])  85.1 us
    ppermute x54, starting transfers between devices, swap(): return lax.ppermute(array, axis, [(i, i ^ bits) for i in range(size)])  44.5 us
    ppermute x3, waiting for transfers between devices, fetch(): sent[d] = lax.ppermute(shares[d], 'fs', late)  36.4 us
    pallas_call x4, Pallas kernels, ffn_chunk(): pl.pallas_call(run, in_specs=[SMEM, VMEM, VMEM, VMEM] + [ANY] * nt, out_s...  19.3 us
    ppermute x3, starting transfers between devices, fetch(): sent[d] = lax.ppermute(shares[d], 'fs', late)  6.35 us
    pallas_call x1, Pallas kernels, glu_conv(): pl.pallas_call(run, in_specs=[SMEM, VMEM] + [ANY] * nt + [HBM] * 2 + [ANY...  4.54 us
    pallas_call x1, Pallas kernels, ffn_shares(): pl.pallas_call(run, in_specs=[SMEM, HBM, HBM, HBM], out_specs=[ANY] * (co...  4.49 us
  transfers between devices with their start and end apart: 58, of which 21 were waited for; matrix products, arithmetic and copies ran while one was open for 3% of the time, Pallas kernels for 14%

profile of v2, /device:TPU:0, one launch (start us, length us, event | category | flops | bytes accessed | tf_op | source)
XLA Modules:
  0.0 218.7 jit_solution(10585367885744180704)
XLA Ops:
  1.1 4.1 %collective-permute-start.4 = (bf16[512,256]{1,0:T(8,128)(2,1)S(1)}, bf16[512,256]{1,0:T(8,128)(2,1)S(1)}, u32[]{:S(2)}, u32[]{:S(2)}) collective-permute-start(bf16[512,256]{1,0:T(8,128)(2,1)S(1)} %broadcast_select_fusion.1), channel_id=1, source_target_pairs={{0,8},{4,12},{8,0},{12,4},{1,9},{5,13},{9,1},{13,5},{2,10},{6,14},... | collective-permute-start | bytes 786440 | tf_op jit(solution)/shard_map/ppermute | solution.py:40
  5.2 1.6 collective-permute-start.3
  10.1 1.8 collective-permute-start.1
  13.6 9.3 %collective-permute-done.13.refs_6_ = bf16[128,512]{1,0:T(8,128)(2,1)S(1)} collective-permute-done((bf16[128,512]{1,0:T(8,128)(2,1)S(1)}, bf16[128,512]{1,0:T(8,128)(2,1)S(1)}, u32[]{:S(2)}, u32[]{:S(2)}) %collective-permute-start.13) | collective-permute-done | bytes 131104 | tf_op jit(solution)/shard_map/ppermute | solution.py:40
  24.9 1.6 collective-permute-start.7
  26.6 2.7 %collective-permute-done.14.refs_7_ = bf16[128,512]{1,0:T(8,128)(2,1)S(1)} collective-permute-done((bf16[128,512]{1,0:T(8,128)(2,1)S(1)}, bf16[128,512]{1,0:T(8,128)(2,1)S(1)}, u32[]{:S(2)}, u32[]{:S(2)}) %collective-permute-start.14) | collective-permute-done | bytes 131104 | tf_op jit(solution)/shard_map/ppermute | solution.py:40
  30.9 1.9 collective-permute-done.5.refs_8_
  37.9 1.9 collective-permute-done.6.refs_9_
  42.9 2.5 %collective-permute-done.8.refs_11_ = bf16[512,256]{1,0:T(8,128)(2,1)S(1)} collective-permute-done((bf16[512,256]{1,0:T(8,128)(2,1)S(1)}, bf16[512,256]{1,0:T(8,128)(2,1)S(1)}, u32[]{:S(2)}, u32[]{:S(2)}) %collective-permute-start.8) | collective-permute-done | bytes 262176 | tf_op jit(solution)/shard_map/ppermute | solution.py:40
  45.4 4.5 %glu_conv.1 = (f32[320,256]{1,0:T(8,128)S(1)}, f32[16,320]{1,0:T(8,128)S(1)}) custom-call(s32[3]{0:T(128)S(1)} %pad_add_fusion.spot_ref, f32[31,256]{1,0:T(8,128)S(1)} %dynamic-slice_convert_fusion.taps_ref, bf16[80,2048]{1,0:T(8,128)(2,1)S(1)} %shard_map.136.refs_0_, bf16[80,2048]{1,0:T(8,128)(2,1)S(1)} %collective-permute-done.refs_1_, ...), custom_call_target="tpu_custom_call" | custom-call | flops 671088640 | bytes 2097152 | tf_op jit(solution)/shard_map/glu_conv/pallas_call | solution.py:162
  50.0 1.6 collective-permute-start.10
  54.9 3.4 %out_product.1 = (bf16[80,2048]{1,0:T(8,128)(2,1)S(1)}, bf16[80,2048]{1,0:T(8,128)(2,1)S(1)}, bf16[80,2048]{1,0:T(8,128)(2,1)S(1)}, bf16[80,2048]{1,0:T(8,128)(2,1)S(1)}) custom-call(s32[3]{0:T(128)S(1)} %pad_add_fusion.spot_ref, f32[320,256]{1,0:T(8,128)S(1)} %get-tuple-element.48.conv_ref, f32[1,256]{1,0:T(1,128)S(1)} %bitcast.12, ...), custom_call_target="tpu_custom_call" | custom-call | flops 335544320 | bytes 1048576 | tf_op jit(solution)/shard_map/out_product/pallas_call | solution.py:230
  58.4 4.5 %ffn_shares.1 = (bf16[384,640]{1,0:T(8,128)(2,1)}, bf16[384,640]{1,0:T(8,128)(2,1)}, bf16[384,640]{1,0:T(8,128)(2,1)}, bf16[512,640]{1,0:T(8,128)(2,1)}, bf16[320,512]{1,0:T(8,128)(2,1)}) custom-call(s32[3]{0:T(128)} %copy-done.11, bf16[512,1280]{1,0:T(8,128)(2,1)} %refs_0_.5, bf16[512,1280]{1,0:T(8,128)(2,1)} %refs_1_.1, bf16[1280,512]{1,0:T(8,128)(2,1)} %refs_2_.1), custom_call_target="tpu_custom_call" | custom-call | flops 327680 | bytes 2621440 | tf_op jit(solution)/shard_map/ffn_shares/pallas_call | solution.py:315
  63.7 5.3 %collective-permute-start.24 = (bf16[384,640]{1,0:T(8,128)(2,1)}, bf16[384,640]{1,0:T(8,128)(2,1)S(1)}, u32[]{:S(2)}, u32[]{:S(2)}) collective-permute-start(bf16[384,640]{1,0:T(8,128)(2,1)} %get-tuple-element.63), channel_id=1, source_target_pairs={{0,12},{12,0},{1,13},{13,1},{2,14},{14,2},{3,15},{15,3},{16,28},{2... | collective-permute-start | bytes 1474568 | tf_op jit(solution)/shard_map/ppermute | solution.py:505
  71.1 10.7 %collective-permute-done.24 = bf16[384,640]{1,0:T(8,128)(2,1)S(1)} collective-permute-done((bf16[384,640]{1,0:T(8,128)(2,1)}, bf16[384,640]{1,0:T(8,128)(2,1)S(1)}, u32[]{:S(2)}, u32[]{:S(2)}) %collective-permute-start.24) | collective-permute-done | bytes 491552 | tf_op jit(solution)/shard_map/ppermute | solution.py:505
  81.8 1.6 collective-permute-start.27
  83.4 10.7 %collective-permute-done.21.refs_0_ = bf16[384,640]{1,0:T(8,128)(2,1)S(1)} collective-permute-done((bf16[384,640]{1,0:T(8,128)(2,1)}, bf16[384,640]{1,0:T(8,128)(2,1)S(1)}, u32[]{:S(2)}, u32[]{:S(2)}) %collective-permute-start.21) | collective-permute-done | bytes 491552 | tf_op jit(solution)/shard_map/ppermute | solution.py:505
  95.7 15.0 %collective-permute-done.22.refs_1_ = bf16[384,640]{1,0:T(8,128)(2,1)S(1)} collective-permute-done((bf16[384,640]{1,0:T(8,128)(2,1)}, bf16[384,640]{1,0:T(8,128)(2,1)S(1)}, u32[]{:S(2)}, u32[]{:S(2)}) %collective-permute-start.22) | collective-permute-done | bytes 491552 | tf_op jit(solution)/shard_map/ppermute | solution.py:505
  113.6 3.1 %collective-permute-start.34 = (bf16[80,2048]{1,0:T(8,128)(2,1)S(1)}, bf16[80,2048]{1,0:T(8,128)(2,1)S(1)}, u32[]{:S(2)}, u32[]{:S(2)}) collective-permute-start(bf16[80,2048]{1,0:T(8,128)(2,1)S(1)} %get-tuple-element.66.refs_0_), channel_id=1, source_target_pairs={{0,4},{4,0},{8,12},{12,8},{1,5},{5,1},{9,13},{13,9},{2,6},{6,2},{1... | collective-permute-start | bytes 983048 | tf_op jit(solution)/shard_map/ppermute | solution.py:40
  116.7 13.0 %collective-permute-done.42.refs_0_ = bf16[80,2048]{1,0:T(8,128)(2,1)S(1)} collective-permute-done((bf16[80,2048]{1,0:T(8,128)(2,1)S(1)}, bf16[80,2048]{1,0:T(8,128)(2,1)S(1)}, u32[]{:S(2)}, u32[]{:S(2)}) %collective-permute-start.42) | collective-permute-done | bytes 327712 | tf_op jit(solution)/shard_map/ppermute | solution.py:40
  130.5 2.3 %ffn_weights.1 = (bf16[2048,640]{1,0:T(8,128)(2,1)S(1)}, bf16[4,384,512]{2,1,0:T(8,128)(2,1)S(1)}) custom-call(s32[3]{0:T(128)S(1)} %copy-done.12, bf16[512,640]{1,0:T(8,128)(2,1)S(1)} %copy-done.4, bf16[320,512]{1,0:T(8,128)(2,1)S(1)} %copy-done.6, bf16[384,640]{1,0:T(8,128)(2,1)S(1)} %collective-permute-done.21.refs_0_, ...), custom_call_target="tpu_custom_call" | custom-call | flops 1310720 | bytes 5242880 | tf_op jit(solution)/shard_map/ffn_weights/pallas_call | solution.py:373
  134.7 4.6 %collective-permute-done.50.refs_0_ = bf16[80,2048]{1,0:T(8,128)(2,1)S(1)} collective-permute-done((bf16[80,2048]{1,0:T(8,128)(2,1)S(1)}, bf16[80,2048]{1,0:T(8,128)(2,1)S(1)}, u32[]{:S(2)}, u32[]{:S(2)}) %collective-permute-start.50) | collective-permute-done | bytes 327712 | tf_op jit(solution)/shard_map/ppermute | solution.py:40
  140.3 4.8 %ffn_chunk.4 = (bf16[80,2048]{1,0:T(8,128)(2,1)S(1)}, bf16[80,2048]{1,0:T(8,128)(2,1)S(1)}, bf16[80,2048]{1,0:T(8,128)(2,1)S(1)}, bf16[80,2048]{1,0:T(8,128)(2,1)S(1)}) custom-call(s32[3]{0:T(128)S(1)} %copy-done.12, f32[3,640]{1,0:T(4,128)S(1)} %maximum_convert_fusion.taps_ref, bf16[2048,640]{1,0:T(8,128)(2,1)S(1)} %get-tuple-element.64.up, ...), custom_call_target="tpu_custom_call" | custom-call | flops 1258291200 | bytes 2621440 | tf_op jit(solution)/shard_map/ffn_chunk/pallas_call | solution.py:447
  147.9 4.8 %ffn_chunk.6 = (bf16[80,2048]{1,0:T(8,128)(2,1)S(1)}, bf16[80,2048]{1,0:T(8,128)(2,1)S(1)}, bf16[80,2048]{1,0:T(8,128)(2,1)S(1)}, bf16[80,2048]{1,0:T(8,128)(2,1)S(1)}) custom-call(s32[3]{0:T(128)S(1)} %copy-done.12, f32[3,640]{1,0:T(4,128)S(1)} %maximum_convert_fusion.taps_ref, bf16[2048,640]{1,0:T(8,128)(2,1)S(1)} %get-tuple-element.64.up, ...), custom_call_target="tpu_custom_call" | custom-call | flops 1258291200 | bytes 2621440 | tf_op jit(solution)/shard_map/ffn_chunk/pallas_call | solution.py:447
  154.6 4.8 %ffn_chunk.5 = (bf16[80,2048]{1,0:T(8,128)(2,1)S(1)}, bf16[80,2048]{1,0:T(8,128)(2,1)S(1)}, bf16[80,2048]{1,0:T(8,128)(2,1)S(1)}, bf16[80,2048]{1,0:T(8,128)(2,1)S(1)}) custom-call(s32[3]{0:T(128)S(1)} %copy-done.12, f32[3,640]{1,0:T(4,128)S(1)} %maximum_convert_fusion.taps_ref, bf16[2048,640]{1,0:T(8,128)(2,1)S(1)} %get-tuple-element.64.up, ...), custom_call_target="tpu_custom_call" | custom-call | flops 1258291200 | bytes 2621440 | tf_op jit(solution)/shard_map/ffn_chunk/pallas_call | solution.py:447
  160.0 4.8 %ffn_chunk.7 = (bf16[80,2048]{1,0:T(8,128)(2,1)S(1)}, bf16[80,2048]{1,0:T(8,128)(2,1)S(1)}, bf16[80,2048]{1,0:T(8,128)(2,1)S(1)}, bf16[80,2048]{1,0:T(8,128)(2,1)S(1)}) custom-call(s32[3]{0:T(128)S(1)} %copy-done.12, f32[3,640]{1,0:T(4,128)S(1)} %maximum_convert_fusion.taps_ref, bf16[2048,640]{1,0:T(8,128)(2,1)S(1)} %get-tuple-element.64.up, ...), custom_call_target="tpu_custom_call" | custom-call | flops 1258291200 | bytes 2621440 | tf_op jit(solution)/shard_map/ffn_chunk/pallas_call | solution.py:447
  167.2 14.4 %collective-permute-done.48 = bf16[80,2048]{1,0:T(8,128)(2,1)S(1)} collective-permute-done((bf16[80,2048]{1,0:T(8,128)(2,1)S(1)}, bf16[80,2048]{1,0:T(8,128)(2,1)S(1)}, u32[]{:S(2)}, u32[]{:S(2)}) %collective-permute-start.48) | collective-permute-done | bytes 327712 | tf_op jit(solution)/shard_map/ppermute | solution.py:40
  184.0 8.4 %collective-permute-done.40 = bf16[80,2048]{1,0:T(8,128)(2,1)S(1)} collective-permute-done((bf16[80,2048]{1,0:T(8,128)(2,1)S(1)}, bf16[80,2048]{1,0:T(8,128)(2,1)S(1)}, u32[]{:S(2)}, u32[]{:S(2)}) %collective-permute-start.40) | collective-permute-done | bytes 327712 | tf_op jit(solution)/shard_map/ppermute | solution.py:40
  192.4 1.7 collective-permute-start.49
  194.6 4.3 %collective-permute-done.56 = bf16[80,2048]{1,0:T(8,128)(2,1)S(1)} collective-permute-done((bf16[80,2048]{1,0:T(8,128)(2,1)S(1)}, bf16[80,2048]{1,0:T(8,128)(2,1)S(1)}, u32[]{:S(2)}, u32[]{:S(2)}) %collective-permute-start.56) | collective-permute-done | bytes 327712 | tf_op jit(solution)/shard_map/ppermute | solution.py:40
  200.6 11.5 %collective-permute-done.49.refs_6_ = bf16[80,2048]{1,0:T(8,128)(2,1)S(1)} collective-permute-done((bf16[80,2048]{1,0:T(8,128)(2,1)S(1)}, bf16[80,2048]{1,0:T(8,128)(2,1)S(1)}, u32[]{:S(2)}, u32[]{:S(2)}) %collective-permute-start.49) | collective-permute-done | bytes 327712 | tf_op jit(solution)/shard_map/ppermute | solution.py:40
  212.1 5.3 %collective-permute-done.57.refs_7_ = bf16[80,2048]{1,0:T(8,128)(2,1)S(1)} collective-permute-done((bf16[80,2048]{1,0:T(8,128)(2,1)S(1)}, bf16[80,2048]{1,0:T(8,128)(2,1)S(1)}, u32[]{:S(2)}, u32[]{:S(2)}) %collective-permute-start.57) | collective-permute-done | bytes 327712 | tf_op jit(solution)/shard_map/ppermute | solution.py:40
  (146 shorter events, 45.4 us)
Async XLA Ops:
  1.1 22.4 %collective-permute-start.4 = (bf16[512,256]{1,0:T(8,128)(2,1)S(1)}, bf16[512,256]{1,0:T(8,128)(2,1)S(1)}, u32[]{:S(2)}, u32[]{:S(2)}) collective-permute-start(bf16[512,256]{1,0:T(8,128)(2,1)S(1)} %broadcast_select_fusion.1), channel_id=1, source_target_pairs={{0,8},{4,12},{8,0},{12,4},{1,9},{5,13},{9,1},{13,5},{2,10},{6,14},... | collective-permute-start | bytes 786440 | tf_op jit(solution)/shard_map/ppermute | solution.py:40
  5.2 19.7 %collective-permute-start.3 = (bf16[512,256]{1,0:T(8,128)(2,1)S(1)}, bf16[512,256]{1,0:T(8,128)(2,1)S(1)}, u32[]{:S(2)}, u32[]{:S(2)}) collective-permute-start(bf16[512,256]{1,0:T(8,128)(2,1)S(1)} %broadcast_select_fusion.1), channel_id=1, source_target_pairs={{0,4},{4,0},{8,12},{12,8},{1,5},{5,1},{9,13},{13,9},{2,6},{6,2},{1... | collective-permute-start | bytes 786440 | tf_op jit(solution)/shard_map/ppermute | solution.py:40
  7.7 15.2 %collective-permute-start.13 = (bf16[128,512]{1,0:T(8,128)(2,1)S(1)}, bf16[128,512]{1,0:T(8,128)(2,1)S(1)}, u32[]{:S(2)}, u32[]{:S(2)}) collective-permute-start(bf16[128,512]{1,0:T(8,128)(2,1)S(1)} %constant_dynamic-slice_fusion.2), channel_id=1, source_target_pairs={{0,8},{4,12},{8,0},{12,4},{1,9},{5,13},{9,1},{13,5},{2,10},{6,14},... | collective-permute-start | bytes 393224 | tf_op jit(solution)/shard_map/ppermute | solution.py:40
  8.1 16.8 %collective-permute-start.12 = (bf16[128,512]{1,0:T(8,128)(2,1)S(1)}, bf16[128,512]{1,0:T(8,128)(2,1)}, u32[]{:S(2)}, u32[]{:S(2)}) collective-permute-start(bf16[128,512]{1,0:T(8,128)(2,1)S(1)} %constant_dynamic-slice_fusion.2), channel_id=1, source_target_pairs={{0,4},{4,0},{8,12},{12,8},{1,5},{5,1},{9,13},{13,9},{2,6},{6,2},{1... | collective-permute-start | bytes 393224 | tf_op jit(solution)/shard_map/ppermute | solution.py:40
  10.1 20.8 %collective-permute-start.1 = (bf16[80,2048]{1,0:T(8,128)(2,1)S(1)}, bf16[80,2048]{1,0:T(8,128)(2,1)S(1)}, u32[]{:S(2)}, u32[]{:S(2)}) collective-permute-start(bf16[80,2048]{1,0:T(8,128)(2,1)S(1)} %shard_map.136.refs_0_), channel_id=1, source_target_pairs={{0,2},{1,3},{2,0},{3,1},{4,6},{5,7},{6,4},{7,5},{8,10},{9,11},{10,... | collective-permute-start | bytes 983048 | tf_op jit(solution)/shard_map/ppermute | solution.py:40
  35.9 15.7 %collective-permute-start.16 = (bf16[128,512]{1,0:T(8,128)(2,1)}, bf16[128,512]{1,0:T(8,128)(2,1)}, u32[]{:S(2)}, u32[]{:S(2)}) collective-permute-start(bf16[128,512]{1,0:T(8,128)(2,1)} %copy-done.7), channel_id=1, source_target_pairs={{0,16},{16,0},{1,17},{17,1},{2,18},{18,2},{3,19},{19,3},{4,20},{20... | collective-permute-start | bytes 393224 | tf_op jit(solution)/shard_map/ppermute | solution.py:40
  36.4 15.8 %collective-permute-start.15 = (bf16[128,512]{1,0:T(8,128)(2,1)}, bf16[128,512]{1,0:T(8,128)(2,1)}, u32[]{:S(2)}, u32[]{:S(2)}) collective-permute-start(bf16[128,512]{1,0:T(8,128)(2,1)} %collective-permute-done.12.refs_5_), channel_id=1, source_target_pairs={{0,16},{16,0},{1,17},{17,1},{2,18},{18,2},{3,19},{19,3},{4,20},{20... | collective-permute-start | bytes 393224 | tf_op jit(solution)/shard_map/ppermute | solution.py:40
  39.8 13.6 %collective-permute-start.17 = (bf16[128,512]{1,0:T(8,128)(2,1)}, bf16[128,512]{1,0:T(8,128)(2,1)}, u32[]{:S(2)}, u32[]{:S(2)}) collective-permute-start(bf16[128,512]{1,0:T(8,128)(2,1)} %copy-done.9), channel_id=1, source_target_pairs={{0,16},{16,0},{1,17},{17,1},{2,18},{18,2},{3,19},{19,3},{4,20},{20... | collective-permute-start | bytes 393224 | tf_op jit(solution)/shard_map/ppermute | solution.py:40
  63.7 18.1 %collective-permute-start.24 = (bf16[384,640]{1,0:T(8,128)(2,1)}, bf16[384,640]{1,0:T(8,128)(2,1)S(1)}, u32[]{:S(2)}, u32[]{:S(2)}) collective-permute-start(bf16[384,640]{1,0:T(8,128)(2,1)} %get-tuple-element.63), channel_id=1, source_target_pairs={{0,12},{12,0},{1,13},{13,1},{2,14},{14,2},{3,15},{15,3},{16,28},{2... | collective-permute-start | bytes 1474568 | tf_op jit(solution)/shard_map/ppermute | solution.py:505
  69.0 25.2 %collective-permute-start.21 = (bf16[384,640]{1,0:T(8,128)(2,1)}, bf16[384,640]{1,0:T(8,128)(2,1)S(1)}, u32[]{:S(2)}, u32[]{:S(2)}) collective-permute-start(bf16[384,640]{1,0:T(8,128)(2,1)} %get-tuple-element.60), channel_id=1, source_target_pairs={{0,4},{4,0},{8,12},{12,8},{1,5},{5,1},{9,13},{13,9},{2,6},{6,2},{1... | collective-permute-start | bytes 1474568 | tf_op jit(solution)/shard_map/ppermute | solution.py:505
  69.1 41.6 %collective-permute-start.22 = (bf16[384,640]{1,0:T(8,128)(2,1)}, bf16[384,640]{1,0:T(8,128)(2,1)S(1)}, u32[]{:S(2)}, u32[]{:S(2)}) collective-permute-start(bf16[384,640]{1,0:T(8,128)(2,1)} %get-tuple-element.61), channel_id=1, source_target_pairs={{0,8},{4,12},{8,0},{12,4},{1,9},{5,13},{9,1},{13,5},{2,10},{6,14},... | collective-permute-start | bytes 1474568 | tf_op jit(solution)/shard_map/ppermute | solution.py:505
  70.1 42.1 %collective-permute-start.18 = (bf16[80,2048]{1,0:T(8,128)(2,1)S(1)}, bf16[80,2048]{1,0:T(8,128)(2,1)S(1)}, u32[]{:S(2)}, u32[]{:S(2)}) collective-permute-start(bf16[80,2048]{1,0:T(8,128)(2,1)S(1)} %get-tuple-element.52), channel_id=1, source_target_pairs={{0,1},{1,0},{2,3},{3,2},{4,5},{5,4},{6,7},{7,6},{8,9},{9,8},{10,11... | collective-permute-start | bytes 983048 | tf_op jit(solution)/shard_map/ppermute | solution.py:40
  70.2 42.0 %collective-permute-start.20 = (bf16[80,2048]{1,0:T(8,128)(2,1)S(1)}, bf16[80,2048]{1,0:T(8,128)(2,1)S(1)}, u32[]{:S(2)}, u32[]{:S(2)}) collective-permute-start(bf16[80,2048]{1,0:T(8,128)(2,1)S(1)} %add_convert_fusion.7), channel_id=1, source_target_pairs={{0,2},{1,3},{2,0},{3,1},{4,6},{5,7},{6,4},{7,5},{8,10},{9,11},{10,... | collective-permute-start | bytes 983048 | tf_op jit(solution)/shard_map/ppermute | solution.py:40
  81.8 31.8 %collective-permute-start.27 = (bf16[384,640]{1,0:T(8,128)(2,1)S(1)}, bf16[384,640]{1,0:T(8,128)(2,1)S(1)}, u32[]{:S(2)}, u32[]{:S(2)}) collective-permute-start(bf16[384,640]{1,0:T(8,128)(2,1)S(1)} %broadcast_select_fusion.refs_2_), channel_id=1, source_target_pairs={{0,16},{16,0},{1,17},{17,1},{2,18},{18,2},{3,19},{19,3},{4,20},{20... | collective-permute-start | bytes 1474568 | tf_op jit(solution)/shard_map/ppermute | solution.py:40
  94.2 22.6 %collective-permute-start.25 = (bf16[384,640]{1,0:T(8,128)(2,1)S(1)}, bf16[384,640]{1,0:T(8,128)(2,1)S(1)}, u32[]{:S(2)}, u32[]{:S(2)}) collective-permute-start(bf16[384,640]{1,0:T(8,128)(2,1)S(1)} %collective-permute-done.21.refs_0_), channel_id=1, source_target_pairs={{0,16},{16,0},{1,17},{17,1},{2,18},{18,2},{3,19},{19,3},{4,20},{20... | collective-permute-start | bytes 1474568 | tf_op jit(solution)/shard_map/ppermute | solution.py:40
  110.7 19.1 %collective-permute-start.26 = (bf16[384,640]{1,0:T(8,128)(2,1)S(1)}, bf16[384,640]{1,0:T(8,128)(2,1)S(1)}, u32[]{:S(2)}, u32[]{:S(2)}) collective-permute-start(bf16[384,640]{1,0:T(8,128)(2,1)S(1)} %collective-permute-done.22.refs_1_), channel_id=1, source_target_pairs={{0,16},{16,0},{1,17},{17,1},{2,18},{18,2},{3,19},{19,3},{4,20},{20... | collective-permute-start | bytes 1474568 | tf_op jit(solution)/shard_map/ppermute | solution.py:40
  112.7 17.1 %collective-permute-start.42 = (bf16[80,2048]{1,0:T(8,128)(2,1)S(1)}, bf16[80,2048]{1,0:T(8,128)(2,1)S(1)}, u32[]{:S(2)}, u32[]{:S(2)}) collective-permute-start(bf16[80,2048]{1,0:T(8,128)(2,1)S(1)} %get-tuple-element.66.refs_0_), channel_id=1, source_target_pairs={{0,8},{4,12},{8,0},{12,4},{1,9},{5,13},{9,1},{13,5},{2,10},{6,14},... | collective-permute-start | bytes 983048 | tf_op jit(solution)/shard_map/ppermute | solution.py:40
  112.8 17.7 %collective-permute-start.29 = (bf16[80,2048]{1,0:T(8,128)(2,1)S(1)}, bf16[80,2048]{1,0:T(8,128)(2,1)S(1)}, u32[]{:S(2)}, u32[]{:S(2)}) collective-permute-start(bf16[80,2048]{1,0:T(8,128)(2,1)S(1)} %get-tuple-element.66.refs_0_), channel_id=1, source_target_pairs={{0,2},{1,3},{2,0},{3,1},{4,6},{5,7},{6,4},{7,5},{8,10},{9,11},{10,... | collective-permute-start | bytes 983048 | tf_op jit(solution)/shard_map/ppermute | solution.py:40
  113.6 19.2 %collective-permute-start.34 = (bf16[80,2048]{1,0:T(8,128)(2,1)S(1)}, bf16[80,2048]{1,0:T(8,128)(2,1)S(1)}, u32[]{:S(2)}, u32[]{:S(2)}) collective-permute-start(bf16[80,2048]{1,0:T(8,128)(2,1)S(1)} %get-tuple-element.66.refs_0_), channel_id=1, source_target_pairs={{0,4},{4,0},{8,12},{12,8},{1,5},{5,1},{9,13},{13,9},{2,6},{6,2},{1... | collective-permute-start | bytes 983048 | tf_op jit(solution)/shard_map/ppermute | solution.py:40
  116.7 16.6 %collective-permute-start.28 = (bf16[80,2048]{1,0:T(8,128)(2,1)S(1)}, bf16[80,2048]{1,0:T(8,128)(2,1)S(1)}, u32[]{:S(2)}, u32[]{:S(2)}) collective-permute-start(bf16[80,2048]{1,0:T(8,128)(2,1)S(1)} %get-tuple-element.66.refs_0_), channel_id=1, source_target_pairs={{0,1},{1,0},{2,3},{3,2},{4,5},{5,4},{6,7},{7,6},{8,9},{9,8},{10,11... | collective-permute-start | bytes 983048 | tf_op jit(solution)/shard_map/ppermute | solution.py:40
  133.4 14.0 %collective-permute-start.36 = (bf16[80,2048]{1,0:T(8,128)(2,1)S(1)}, bf16[80,2048]{1,0:T(8,128)(2,1)S(1)}, u32[]{:S(2)}, u32[]{:S(2)}) collective-permute-start(bf16[80,2048]{1,0:T(8,128)(2,1)S(1)} %collective-permute-done.34.refs_0_), channel_id=1, source_target_pairs={{0,2},{1,3},{2,0},{3,1},{4,6},{5,7},{6,4},{7,5},{8,10},{9,11},{10,... | collective-permute-start | bytes 983048 | tf_op jit(solution)/shard_map/ppermute | solution.py:40
  139.3 14.1 %collective-permute-start.52 = (bf16[80,2048]{1,0:T(8,128)(2,1)S(1)}, bf16[80,2048]{1,0:T(8,128)(2,1)S(1)}, u32[]{:S(2)}, u32[]{:S(2)}) collective-permute-start(bf16[80,2048]{1,0:T(8,128)(2,1)S(1)} %collective-permute-done.50.refs_0_), channel_id=1, source_target_pairs={{0,2},{1,3},{2,0},{3,1},{4,6},{5,7},{6,4},{7,5},{8,10},{9,11},{10,... | collective-permute-start | bytes 983048 | tf_op jit(solution)/shard_map/ppermute | solution.py:40
  154.0 46.6 %collective-permute-start.31 = (bf16[80,2048]{1,0:T(8,128)(2,1)S(1)}, bf16[80,2048]{1,0:T(8,128)(2,1)S(1)}, u32[]{:S(2)}, u32[]{:S(2)}) collective-permute-start(bf16[80,2048]{1,0:T(8,128)(2,1)S(1)} %get-tuple-element.68), channel_id=1, source_target_pairs={{0,1},{1,0},{2,3},{3,2},{4,5},{5,4},{6,7},{7,6},{8,9},{9,8},{10,11... | collective-permute-start | bytes 983048 | tf_op jit(solution)/shard_map/ppermute | solution.py:40
  154.1 13.1 %collective-permute-start.46 = (bf16[80,2048]{1,0:T(8,128)(2,1)S(1)}, bf16[80,2048]{1,0:T(8,128)(2,1)S(1)}, u32[]{:S(2)}, u32[]{:S(2)}) collective-permute-start(bf16[80,2048]{1,0:T(8,128)(2,1)S(1)} %get-tuple-element.76), channel_id=1, source_target_pairs={{0,1},{1,0},{2,3},{3,2},{4,5},{5,4},{6,7},{7,6},{8,9},{9,8},{10,11... | collective-permute-start | bytes 983048 | tf_op jit(solution)/shard_map/ppermute | solution.py:40
  159.5 23.1 %collective-permute-start.38 = (bf16[80,2048]{1,0:T(8,128)(2,1)S(1)}, bf16[80,2048]{1,0:T(8,128)(2,1)S(1)}, u32[]{:S(2)}, u32[]{:S(2)}) collective-permute-start(bf16[80,2048]{1,0:T(8,128)(2,1)S(1)} %get-tuple-element.72), channel_id=1, source_target_pairs={{0,1},{1,0},{2,3},{3,2},{4,5},{5,4},{6,7},{7,6},{8,9},{9,8},{10,11... | collective-permute-start | bytes 983048 | tf_op jit(solution)/shard_map/ppermute | solution.py:40
  164.8 35.8 %collective-permute-start.33 = (bf16[80,2048]{1,0:T(8,128)(2,1)S(1)}, bf16[80,2048]{1,0:T(8,128)(2,1)S(1)}, u32[]{:S(2)}, u32[]{:S(2)}) collective-permute-start(bf16[80,2048]{1,0:T(8,128)(2,1)S(1)} %add_convert_fusion.6), channel_id=1, source_target_pairs={{0,2},{1,3},{2,0},{3,1},{4,6},{5,7},{6,4},{7,5},{8,10},{9,11},{10,... | collective-permute-start | bytes 983048 | tf_op jit(solution)/shard_map/ppermute | solution.py:40
  165.7 15.9 %collective-permute-start.48 = (bf16[80,2048]{1,0:T(8,128)(2,1)S(1)}, bf16[80,2048]{1,0:T(8,128)(2,1)S(1)}, u32[]{:S(2)}, u32[]{:S(2)}) collective-permute-start(bf16[80,2048]{1,0:T(8,128)(2,1)S(1)} %add_convert_fusion.3), channel_id=1, source_target_pairs={{0,2},{1,3},{2,0},{3,1},{4,6},{5,7},{6,4},{7,5},{8,10},{9,11},{10,... | collective-permute-start | bytes 983048 | tf_op jit(solution)/shard_map/ppermute | solution.py:40
  167.2 14.6 %collective-permute-start.55 = (bf16[80,2048]{1,0:T(8,128)(2,1)S(1)}, bf16[80,2048]{1,0:T(8,128)(2,1)S(1)}, u32[]{:S(2)}, u32[]{:S(2)}) collective-permute-start(bf16[80,2048]{1,0:T(8,128)(2,1)S(1)} %get-tuple-element.82), channel_id=1, source_target_pairs={{0,1},{1,0},{2,3},{3,2},{4,5},{5,4},{6,7},{7,6},{8,9},{9,8},{10,11... | collective-permute-start | bytes 983048 | tf_op jit(solution)/shard_map/ppermute | solution.py:40
  182.6 16.3 %collective-permute-start.56 = (bf16[80,2048]{1,0:T(8,128)(2,1)S(1)}, bf16[80,2048]{1,0:T(8,128)(2,1)S(1)}, u32[]{:S(2)}, u32[]{:S(2)}) collective-permute-start(bf16[80,2048]{1,0:T(8,128)(2,1)S(1)} %add_convert_fusion.1), channel_id=1, source_target_pairs={{0,2},{1,3},{2,0},{3,1},{4,6},{5,7},{6,4},{7,5},{8,10},{9,11},{10,... | collective-permute-start | bytes 983048 | tf_op jit(solution)/shard_map/ppermute | solution.py:40
  192.4 19.7 %collective-permute-start.49 = (bf16[80,2048]{1,0:T(8,128)(2,1)S(1)}, bf16[80,2048]{1,0:T(8,128)(2,1)S(1)}, u32[]{:S(2)}, u32[]{:S(2)}) collective-permute-start(bf16[80,2048]{1,0:T(8,128)(2,1)S(1)} %add_convert_fusion.2), channel_id=1, source_target_pairs={{0,8},{4,12},{8,0},{12,4},{1,9},{5,13},{9,1},{13,5},{2,10},{6,14},... | collective-permute-start | bytes 983048 | tf_op jit(solution)/shard_map/ppermute | solution.py:40
  194.3 17.9 %collective-permute-start.41 = (bf16[80,2048]{1,0:T(8,128)(2,1)S(1)}, bf16[80,2048]{1,0:T(8,128)(2,1)S(1)}, u32[]{:S(2)}, u32[]{:S(2)}) collective-permute-start(bf16[80,2048]{1,0:T(8,128)(2,1)S(1)} %add_convert_fusion.4), channel_id=1, source_target_pairs={{0,4},{4,0},{8,12},{12,8},{1,5},{5,1},{9,13},{13,9},{2,6},{6,2},{1... | collective-permute-start | bytes 983048 | tf_op jit(solution)/shard_map/ppermute | solution.py:40
  199.1 18.4 %collective-permute-start.57 = (bf16[80,2048]{1,0:T(8,128)(2,1)S(1)}, bf16[80,2048]{1,0:T(8,128)(2,1)S(1)}, u32[]{:S(2)}, u32[]{:S(2)}) collective-permute-start(bf16[80,2048]{1,0:T(8,128)(2,1)S(1)} %add_convert_fusion), channel_id=1, source_target_pairs={{0,12},{4,8},{8,4},{12,0},{1,13},{5,9},{9,5},{13,1},{2,14},{6,10},... | collective-permute-start | bytes 983048 | tf_op jit(solution)/shard_map/ppermute | solution.py:40
  (40 other events, 653.2 us)

commit v3 on v2

--- a/solution.py
+++ b/solution.py
@@ -215,16 +215,10 @@
         activated = (scaled * jax.nn.sigmoid(scaled)).astype(BF16)
         for copy in copies:
             copy.wait()
-        outward = []
         for s in range(nf):
-            columns = pl.ds(s * cols, cols)
-            mixed[:, columns] = product(activated, weight[s]).astype(BF16)
-            targets = [
-                (mixed.at[aligned(member ^ d, rows), columns], out_refs[d].at[:, columns])
-                for d in range(nt)
-            ]
-            outward += start_copies(targets, sems, 1 + len(keys) + len(outward))
-        for copy in outward:
+            mixed[:, s * cols : (s + 1) * cols] = product(activated, weight[s]).astype(BF16)
+        targets = [(mixed.at[aligned(member ^ d, rows)], out_refs[d]) for d in range(nt)]
+        for copy in start_copies(targets, sems):
             copy.wait()
 
     return pl.pallas_call(
@@ -401,11 +395,10 @@
     def run(spot_ref, taps_ref, up, down, *refs):
         block_refs, refs = refs[:nt], refs[nt:]
         out_refs, refs = refs[:nt], refs[nt:]
-        gathered, hidden, mixed, sems = refs
+        gathered, hidden, mixed = refs
         member = spot_ref[2]
-        pairs = [(block_refs[d], gathered.at[aligned(member ^ d, rows)]) for d in range(nt)]
-        for copy in start_copies(pairs, sems):
-            copy.wait()
+        for d in range(nt):
+            gathered[aligned(member ^ d, rows), :] = block_refs[d][...]
 
         def conv(column, size):
             raw = product(gathered[...], up[:, column : column + size])
@@ -431,29 +424,21 @@
             lane = lax.broadcasted_iota(jnp.int32, both.shape, 1)
             gated = gelu(both) * pltpu.roll(both, LANES - rest, 1)
             hidden[:, whole:] = jnp.where(lane < rest, gated, 0.0).astype(BF16)
-        outward = []
         for s in range(parts):
-            columns = pl.ds(s * cols, cols)
-            mixed[:, columns] = product(hidden[...], down[s]).astype(BF16)
-            targets = [
-                (mixed.at[aligned(member ^ d, rows), columns], out_refs[d].at[:, columns])
-                for d in range(nt)
-            ]
-            outward += start_copies(targets, sems, nt + len(outward))
-        for copy in outward:
-            copy.wait()
+            mixed[:, s * cols : (s + 1) * cols] = product(hidden[...], down[s]).astype(BF16)
+        for d in range(nt):
+            out_refs[d][...] = mixed[aligned(member ^ d, rows), :]
 
     flops = 2 * total * width * packed + 2 * total * units * parts * cols
     return pl.pallas_call(
         run,
-        in_specs=[SMEM, VMEM, VMEM, VMEM] + [ANY] * nt,
-        out_specs=[ANY] * nt,
+        in_specs=[SMEM, VMEM, VMEM, VMEM] + [VMEM] * nt,
+        out_specs=[VMEM] * nt,
         out_shape=[jax.ShapeDtypeStruct((rows, parts * cols), BF16)] * nt,
         scratch_shapes=[
             pltpu.VMEM((total, width), BF16),
             pltpu.VMEM((total, padded), BF16),
             pltpu.VMEM((total, parts * cols), BF16),
-            pltpu.SemaphoreType.DMA((nt + nt * parts,)),
         ],
         cost_estimate=pl.CostEstimate(
             flops=flops, transcendentals=total * units, bytes_accessed=2 * width * packed

time: 222 us -> 220 us (level)
  Pallas kernels: 35.9 us -> 31.1 us
  waiting for transfers between devices: 121 us -> 124 us
    pallas_call x4, Pallas kernels: 19.3 us -> 14.8 us  [ffn_chunk(): pl.pallas_call(run, in_specs=[SMEM, VMEM, VMEM, VMEM] + [VMEM] * nt, out_...]
    ppermute x54, waiting for transfers between devices: 85.1 us -> 87.3 us  [swap(): return lax.ppermute(array, axis, [(i, i ^ bits) for i in range(size)])]
  transfers between devices with their start and end apart: 58 -> 58, of which waited for: 21 -> 21; matrix products, arithmetic and copies ran while one was open for 3% -> 3% of each run, Pallas kernels for 14% -> 12%
where the time goes in v3:
time: 220 us; the launch traced here: 216 us
  waiting for transfers between devices  124 us (56%)
  starting transfers between devices  51.7 us (24%)
  Pallas kernels  31.1 us (14%)
  local copies, waits for them, and re-layouts  5.71 us (3%)
  other arithmetic  3.49 us (2%)
    ppermute x54, waiting for transfers between devices, swap(): return lax.ppermute(array, axis, [(i, i ^ bits) for i in range(size)])  87.3 us
    ppermute x54, starting transfers between devices, swap(): return lax.ppermute(array, axis, [(i, i ^ bits) for i in range(size)])  44.5 us
    ppermute x3, waiting for transfers between devices, fetch(): sent[d] = lax.ppermute(shares[d], 'fs', late)  36.4 us
    pallas_call x4, Pallas kernels, ffn_chunk(): pl.pallas_call(run, in_specs=[SMEM, VMEM, VMEM, VMEM] + [VMEM] * nt, out_...  14.8 us
    ppermute x3, starting transfers between devices, fetch(): sent[d] = lax.ppermute(shares[d], 'fs', late)  6.35 us
    pallas_call x1, Pallas kernels, glu_conv(): pl.pallas_call(run, in_specs=[SMEM, VMEM] + [ANY] * nt + [HBM] * 2 + [ANY...  4.54 us
    pallas_call x1, Pallas kernels, ffn_shares(): pl.pallas_call(run, in_specs=[SMEM, HBM, HBM, HBM], out_specs=[ANY] * (co...  4.49 us
  transfers between devices with their start and end apart: 58, of which 21 were waited for; matrix products, arithmetic and copies ran while one was open for 3% of the time, Pallas kernels for 12%

profile of v3, /device:TPU:0, one launch (start us, length us, event | category | flops | bytes accessed | tf_op | source)
XLA Modules:
  0.0 216.2 jit_solution(1619495958430234528)
XLA Ops:
  1.1 4.1 %collective-permute-start.4 = (bf16[512,256]{1,0:T(8,128)(2,1)S(1)}, bf16[512,256]{1,0:T(8,128)(2,1)S(1)}, u32[]{:S(2)}, u32[]{:S(2)}) collective-permute-start(bf16[512,256]{1,0:T(8,128)(2,1)S(1)} %broadcast_select_fusion.1), channel_id=1, source_target_pairs={{0,8},{4,12},{8,0},{12,4},{1,9},{5,13},{9,1},{13,5},{2,10},{6,14},... | collective-permute-start | bytes 786440 | tf_op jit(solution)/shard_map/ppermute | solution.py:40
  10.1 1.8 collective-permute-start.1
  13.6 9.3 %collective-permute-done.13.refs_6_ = bf16[128,512]{1,0:T(8,128)(2,1)S(1)} collective-permute-done((bf16[128,512]{1,0:T(8,128)(2,1)S(1)}, bf16[128,512]{1,0:T(8,128)(2,1)S(1)}, u32[]{:S(2)}, u32[]{:S(2)}) %collective-permute-start.13) | collective-permute-done | bytes 131104 | tf_op jit(solution)/shard_map/ppermute | solution.py:40
  24.9 1.6 collective-permute-start.7
  26.6 2.7 %collective-permute-done.14.refs_7_ = bf16[128,512]{1,0:T(8,128)(2,1)S(1)} collective-permute-done((bf16[128,512]{1,0:T(8,128)(2,1)S(1)}, bf16[128,512]{1,0:T(8,128)(2,1)S(1)}, u32[]{:S(2)}, u32[]{:S(2)}) %collective-permute-start.14) | collective-permute-done | bytes 131104 | tf_op jit(solution)/shard_map/ppermute | solution.py:40
  30.9 1.9 collective-permute-done.5.refs_8_
  37.9 1.9 collective-permute-done.6.refs_9_
  42.9 2.5 %collective-permute-done.8.refs_11_ = bf16[512,256]{1,0:T(8,128)(2,1)S(1)} collective-permute-done((bf16[512,256]{1,0:T(8,128)(2,1)S(1)}, bf16[512,256]{1,0:T(8,128)(2,1)S(1)}, u32[]{:S(2)}, u32[]{:S(2)}) %collective-permute-start.8) | collective-permute-done | bytes 262176 | tf_op jit(solution)/shard_map/ppermute | solution.py:40
  45.4 4.5 %glu_conv.1 = (f32[320,256]{1,0:T(8,128)S(1)}, f32[16,320]{1,0:T(8,128)S(1)}) custom-call(s32[3]{0:T(128)S(1)} %pad_add_fusion.spot_ref, f32[31,256]{1,0:T(8,128)S(1)} %dynamic-slice_convert_fusion.taps_ref, bf16[80,2048]{1,0:T(8,128)(2,1)S(1)} %shard_map.136.refs_0_, bf16[80,2048]{1,0:T(8,128)(2,1)S(1)} %collective-permute-done.refs_1_, ...), custom_call_target="tpu_custom_call" | custom-call | flops 671088640 | bytes 2097152 | tf_op jit(solution)/shard_map/glu_conv/pallas_call | solution.py:162
  50.0 1.6 collective-permute-start.10
  54.9 3.2 %out_product.1 = (bf16[80,2048]{1,0:T(8,128)(2,1)S(1)}, bf16[80,2048]{1,0:T(8,128)(2,1)S(1)}, bf16[80,2048]{1,0:T(8,128)(2,1)S(1)}, bf16[80,2048]{1,0:T(8,128)(2,1)S(1)}) custom-call(s32[3]{0:T(128)S(1)} %pad_add_fusion.spot_ref, f32[320,256]{1,0:T(8,128)S(1)} %get-tuple-element.48.conv_ref, f32[1,256]{1,0:T(1,128)S(1)} %bitcast.12, ...), custom_call_target="tpu_custom_call" | custom-call | flops 335544320 | bytes 1048576 | tf_op jit(solution)/shard_map/out_product/pallas_call | solution.py:224
  58.1 4.5 %ffn_shares.1 = (bf16[384,640]{1,0:T(8,128)(2,1)}, bf16[384,640]{1,0:T(8,128)(2,1)}, bf16[384,640]{1,0:T(8,128)(2,1)}, bf16[512,640]{1,0:T(8,128)(2,1)}, bf16[320,512]{1,0:T(8,128)(2,1)}) custom-call(s32[3]{0:T(128)} %copy-done.11, bf16[512,1280]{1,0:T(8,128)(2,1)} %refs_0_.5, bf16[512,1280]{1,0:T(8,128)(2,1)} %refs_1_.1, bf16[1280,512]{1,0:T(8,128)(2,1)} %refs_2_.1), custom_call_target="tpu_custom_call" | custom-call | flops 327680 | bytes 2621440 | tf_op jit(solution)/shard_map/ffn_shares/pallas_call | solution.py:309
  63.4 5.3 %collective-permute-start.24 = (bf16[384,640]{1,0:T(8,128)(2,1)}, bf16[384,640]{1,0:T(8,128)(2,1)S(1)}, u32[]{:S(2)}, u32[]{:S(2)}) collective-permute-start(bf16[384,640]{1,0:T(8,128)(2,1)} %get-tuple-element.63), channel_id=1, source_target_pairs={{0,12},{12,0},{1,13},{13,1},{2,14},{14,2},{3,15},{15,3},{16,28},{2... | collective-permute-start | bytes 1474568 | tf_op jit(solution)/shard_map/ppermute | solution.py:490
  70.9 10.7 %collective-permute-done.24 = bf16[384,640]{1,0:T(8,128)(2,1)S(1)} collective-permute-done((bf16[384,640]{1,0:T(8,128)(2,1)}, bf16[384,640]{1,0:T(8,128)(2,1)S(1)}, u32[]{:S(2)}, u32[]{:S(2)}) %collective-permute-start.24) | collective-permute-done | bytes 491552 | tf_op jit(solution)/shard_map/ppermute | solution.py:490
  83.2 10.8 %collective-permute-done.21.refs_0_ = bf16[384,640]{1,0:T(8,128)(2,1)S(1)} collective-permute-done((bf16[384,640]{1,0:T(8,128)(2,1)}, bf16[384,640]{1,0:T(8,128)(2,1)S(1)}, u32[]{:S(2)}, u32[]{:S(2)}) %collective-permute-start.21) | collective-permute-done | bytes 491552 | tf_op jit(solution)/shard_map/ppermute | solution.py:490
  95.5 15.0 %collective-permute-done.22.refs_1_ = bf16[384,640]{1,0:T(8,128)(2,1)S(1)} collective-permute-done((bf16[384,640]{1,0:T(8,128)(2,1)}, bf16[384,640]{1,0:T(8,128)(2,1)S(1)}, u32[]{:S(2)}, u32[]{:S(2)}) %collective-permute-start.22) | collective-permute-done | bytes 491552 | tf_op jit(solution)/shard_map/ppermute | solution.py:490
  113.4 3.1 %collective-permute-start.34 = (bf16[80,2048]{1,0:T(8,128)(2,1)S(1)}, bf16[80,2048]{1,0:T(8,128)(2,1)S(1)}, u32[]{:S(2)}, u32[]{:S(2)}) collective-permute-start(bf16[80,2048]{1,0:T(8,128)(2,1)S(1)} %get-tuple-element.66.refs_0_), channel_id=1, source_target_pairs={{0,4},{4,0},{8,12},{12,8},{1,5},{5,1},{9,13},{13,9},{2,6},{6,2},{1... | collective-permute-start | bytes 983048 | tf_op jit(solution)/shard_map/ppermute | solution.py:40
  116.5 13.0 %collective-permute-done.42.refs_0_ = bf16[80,2048]{1,0:T(8,128)(2,1)S(1)} collective-permute-done((bf16[80,2048]{1,0:T(8,128)(2,1)S(1)}, bf16[80,2048]{1,0:T(8,128)(2,1)S(1)}, u32[]{:S(2)}, u32[]{:S(2)}) %collective-permute-start.42) | collective-permute-done | bytes 327712 | tf_op jit(solution)/shard_map/ppermute | solution.py:40
  130.2 2.3 %ffn_weights.1 = (bf16[2048,640]{1,0:T(8,128)(2,1)S(1)}, bf16[4,384,512]{2,1,0:T(8,128)(2,1)S(1)}) custom-call(s32[3]{0:T(128)S(1)} %copy-done.12, bf16[512,640]{1,0:T(8,128)(2,1)S(1)} %copy-done.4, bf16[320,512]{1,0:T(8,128)(2,1)S(1)} %copy-done.6, bf16[384,640]{1,0:T(8,128)(2,1)S(1)} %collective-permute-done.21.refs_0_, ...), custom_call_target="tpu_custom_call" | custom-call | flops 1310720 | bytes 5242880 | tf_op jit(solution)/shard_map/ffn_weights/pallas_call | solution.py:367
  134.4 4.6 %collective-permute-done.50.refs_0_ = bf16[80,2048]{1,0:T(8,128)(2,1)S(1)} collective-permute-done((bf16[80,2048]{1,0:T(8,128)(2,1)S(1)}, bf16[80,2048]{1,0:T(8,128)(2,1)S(1)}, u32[]{:S(2)}, u32[]{:S(2)}) %collective-permute-start.50) | collective-permute-done | bytes 327712 | tf_op jit(solution)/shard_map/ppermute | solution.py:40
  140.1 3.7 %ffn_chunk.4 = (bf16[80,2048]{1,0:T(8,128)(2,1)S(1)}, bf16[80,2048]{1,0:T(8,128)(2,1)S(1)}, bf16[80,2048]{1,0:T(8,128)(2,1)S(1)}, bf16[80,2048]{1,0:T(8,128)(2,1)S(1)}) custom-call(s32[3]{0:T(128)S(1)} %copy-done.12, f32[3,640]{1,0:T(4,128)S(1)} %maximum_convert_fusion.taps_ref, bf16[2048,640]{1,0:T(8,128)(2,1)S(1)} %get-tuple-element.64.up, ...), custom_call_target="tpu_custom_call" | custom-call | flops 1258291200 | bytes 2621440 | tf_op jit(solution)/shard_map/ffn_chunk/pallas_call | solution.py:433
  144.4 2.7 %collective-permute-done.36.refs_2_ = bf16[80,2048]{1,0:T(8,128)(2,1)S(1)} collective-permute-done((bf16[80,2048]{1,0:T(8,128)(2,1)S(1)}, bf16[80,2048]{1,0:T(8,128)(2,1)S(1)}, u32[]{:S(2)}, u32[]{:S(2)}) %collective-permute-start.36) | collective-permute-done | bytes 327712 | tf_op jit(solution)/shard_map/ppermute | solution.py:40
  147.6 3.7 %ffn_chunk.6 = (bf16[80,2048]{1,0:T(8,128)(2,1)S(1)}, bf16[80,2048]{1,0:T(8,128)(2,1)S(1)}, bf16[80,2048]{1,0:T(8,128)(2,1)S(1)}, bf16[80,2048]{1,0:T(8,128)(2,1)S(1)}) custom-call(s32[3]{0:T(128)S(1)} %copy-done.12, f32[3,640]{1,0:T(4,128)S(1)} %maximum_convert_fusion.taps_ref, bf16[2048,640]{1,0:T(8,128)(2,1)S(1)} %get-tuple-element.64.up, ...), custom_call_target="tpu_custom_call" | custom-call | flops 1258291200 | bytes 2621440 | tf_op jit(solution)/shard_map/ffn_chunk/pallas_call | solution.py:433
  151.3 1.8 collective-permute-done.52.refs_2_
  154.3 3.7 %ffn_chunk.5 = (bf16[80,2048]{1,0:T(8,128)(2,1)S(1)}, bf16[80,2048]{1,0:T(8,128)(2,1)S(1)}, bf16[80,2048]{1,0:T(8,128)(2,1)S(1)}, bf16[80,2048]{1,0:T(8,128)(2,1)S(1)}) custom-call(s32[3]{0:T(128)S(1)} %copy-done.12, f32[3,640]{1,0:T(4,128)S(1)} %maximum_convert_fusion.taps_ref, bf16[2048,640]{1,0:T(8,128)(2,1)S(1)} %get-tuple-element.64.up, ...), custom_call_target="tpu_custom_call" | custom-call | flops 1258291200 | bytes 2621440 | tf_op jit(solution)/shard_map/ffn_chunk/pallas_call | solution.py:433
  158.6 3.7 %ffn_chunk.7 = (bf16[80,2048]{1,0:T(8,128)(2,1)S(1)}, bf16[80,2048]{1,0:T(8,128)(2,1)S(1)}, bf16[80,2048]{1,0:T(8,128)(2,1)S(1)}, bf16[80,2048]{1,0:T(8,128)(2,1)S(1)}) custom-call(s32[3]{0:T(128)S(1)} %copy-done.12, f32[3,640]{1,0:T(4,128)S(1)} %maximum_convert_fusion.taps_ref, bf16[2048,640]{1,0:T(8,128)(2,1)S(1)} %get-tuple-element.64.up, ...), custom_call_target="tpu_custom_call" | custom-call | flops 1258291200 | bytes 2621440 | tf_op jit(solution)/shard_map/ffn_chunk/pallas_call | solution.py:433
  164.7 14.4 %collective-permute-done.48 = bf16[80,2048]{1,0:T(8,128)(2,1)S(1)} collective-permute-done((bf16[80,2048]{1,0:T(8,128)(2,1)S(1)}, bf16[80,2048]{1,0:T(8,128)(2,1)S(1)}, u32[]{:S(2)}, u32[]{:S(2)}) %collective-permute-start.48) | collective-permute-done | bytes 327712 | tf_op jit(solution)/shard_map/ppermute | solution.py:40
  181.5 8.4 %collective-permute-done.40 = bf16[80,2048]{1,0:T(8,128)(2,1)S(1)} collective-permute-done((bf16[80,2048]{1,0:T(8,128)(2,1)S(1)}, bf16[80,2048]{1,0:T(8,128)(2,1)S(1)}, u32[]{:S(2)}, u32[]{:S(2)}) %collective-permute-start.40) | collective-permute-done | bytes 327712 | tf_op jit(solution)/shard_map/ppermute | solution.py:40
  189.9 1.7 collective-permute-start.49
  192.1 4.3 %collective-permute-done.56 = bf16[80,2048]{1,0:T(8,128)(2,1)S(1)} collective-permute-done((bf16[80,2048]{1,0:T(8,128)(2,1)S(1)}, bf16[80,2048]{1,0:T(8,128)(2,1)S(1)}, u32[]{:S(2)}, u32[]{:S(2)}) %collective-permute-start.56) | collective-permute-done | bytes 327712 | tf_op jit(solution)/shard_map/ppermute | solution.py:40
  198.1 11.5 %collective-permute-done.49.refs_6_ = bf16[80,2048]{1,0:T(8,128)(2,1)S(1)} collective-permute-done((bf16[80,2048]{1,0:T(8,128)(2,1)S(1)}, bf16[80,2048]{1,0:T(8,128)(2,1)S(1)}, u32[]{:S(2)}, u32[]{:S(2)}) %collective-permute-start.49) | collective-permute-done | bytes 327712 | tf_op jit(solution)/shard_map/ppermute | solution.py:40
  209.6 5.3 %collective-permute-done.57.refs_7_ = bf16[80,2048]{1,0:T(8,128)(2,1)S(1)} collective-permute-done((bf16[80,2048]{1,0:T(8,128)(2,1)S(1)}, bf16[80,2048]{1,0:T(8,128)(2,1)S(1)}, u32[]{:S(2)}, u32[]{:S(2)}) %collective-permute-start.57) | collective-permute-done | bytes 327712 | tf_op jit(solution)/shard_map/ppermute | solution.py:40
  (146 shorter events, 46.4 us)
Async XLA Ops:
  1.1 22.4 %collective-permute-start.4 = (bf16[512,256]{1,0:T(8,128)(2,1)S(1)}, bf16[512,256]{1,0:T(8,128)(2,1)S(1)}, u32[]{:S(2)}, u32[]{:S(2)}) collective-permute-start(bf16[512,256]{1,0:T(8,128)(2,1)S(1)} %broadcast_select_fusion.1), channel_id=1, source_target_pairs={{0,8},{4,12},{8,0},{12,4},{1,9},{5,13},{9,1},{13,5},{2,10},{6,14},... | collective-permute-start | bytes 786440 | tf_op jit(solution)/shard_map/ppermute | solution.py:40
  5.2 19.7 %collective-permute-start.3 = (bf16[512,256]{1,0:T(8,128)(2,1)S(1)}, bf16[512,256]{1,0:T(8,128)(2,1)S(1)}, u32[]{:S(2)}, u32[]{:S(2)}) collective-permute-start(bf16[512,256]{1,0:T(8,128)(2,1)S(1)} %broadcast_select_fusion.1), channel_id=1, source_target_pairs={{0,4},{4,0},{8,12},{12,8},{1,5},{5,1},{9,13},{13,9},{2,6},{6,2},{1... | collective-permute-start | bytes 786440 | tf_op jit(solution)/shard_map/ppermute | solution.py:40
  7.7 15.2 %collective-permute-start.13 = (bf16[128,512]{1,0:T(8,128)(2,1)S(1)}, bf16[128,512]{1,0:T(8,128)(2,1)S(1)}, u32[]{:S(2)}, u32[]{:S(2)}) collective-permute-start(bf16[128,512]{1,0:T(8,128)(2,1)S(1)} %constant_dynamic-slice_fusion.2), channel_id=1, source_target_pairs={{0,8},{4,12},{8,0},{12,4},{1,9},{5,13},{9,1},{13,5},{2,10},{6,14},... | collective-permute-start | bytes 393224 | tf_op jit(solution)/shard_map/ppermute | solution.py:40
  8.1 16.8 %collective-permute-start.12 = (bf16[128,512]{1,0:T(8,128)(2,1)S(1)}, bf16[128,512]{1,0:T(8,128)(2,1)}, u32[]{:S(2)}, u32[]{:S(2)}) collective-permute-start(bf16[128,512]{1,0:T(8,128)(2,1)S(1)} %constant_dynamic-slice_fusion.2), channel_id=1, source_target_pairs={{0,4},{4,0},{8,12},{12,8},{1,5},{5,1},{9,13},{13,9},{2,6},{6,2},{1... | collective-permute-start | bytes 393224 | tf_op jit(solution)/shard_map/ppermute | solution.py:40
  10.1 20.8 %collective-permute-start.1 = (bf16[80,2048]{1,0:T(8,128)(2,1)S(1)}, bf16[80,2048]{1,0:T(8,128)(2,1)S(1)}, u32[]{:S(2)}, u32[]{:S(2)}) collective-permute-start(bf16[80,2048]{1,0:T(8,128)(2,1)S(1)} %shard_map.136.refs_0_), channel_id=1, source_target_pairs={{0,2},{1,3},{2,0},{3,1},{4,6},{5,7},{6,4},{7,5},{8,10},{9,11},{10,... | collective-permute-start | bytes 983048 | tf_op jit(solution)/shard_map/ppermute | solution.py:40
  35.9 15.7 %collective-permute-start.16 = (bf16[128,512]{1,0:T(8,128)(2,1)}, bf16[128,512]{1,0:T(8,128)(2,1)}, u32[]{:S(2)}, u32[]{:S(2)}) collective-permute-start(bf16[128,512]{1,0:T(8,128)(2,1)} %copy-done.7), channel_id=1, source_target_pairs={{0,16},{16,0},{1,17},{17,1},{2,18},{18,2},{3,19},{19,3},{4,20},{20... | collective-permute-start | bytes 393224 | tf_op jit(solution)/shard_map/ppermute | solution.py:40
  36.4 15.8 %collective-permute-start.15 = (bf16[128,512]{1,0:T(8,128)(2,1)}, bf16[128,512]{1,0:T(8,128)(2,1)}, u32[]{:S(2)}, u32[]{:S(2)}) collective-permute-start(bf16[128,512]{1,0:T(8,128)(2,1)} %collective-permute-done.12.refs_5_), channel_id=1, source_target_pairs={{0,16},{16,0},{1,17},{17,1},{2,18},{18,2},{3,19},{19,3},{4,20},{20... | collective-permute-start | bytes 393224 | tf_op jit(solution)/shard_map/ppermute | solution.py:40
  39.8 13.6 %collective-permute-start.17 = (bf16[128,512]{1,0:T(8,128)(2,1)}, bf16[128,512]{1,0:T(8,128)(2,1)}, u32[]{:S(2)}, u32[]{:S(2)}) collective-permute-start(bf16[128,512]{1,0:T(8,128)(2,1)} %copy-done.9), channel_id=1, source_target_pairs={{0,16},{16,0},{1,17},{17,1},{2,18},{18,2},{3,19},{19,3},{4,20},{20... | collective-permute-start | bytes 393224 | tf_op jit(solution)/shard_map/ppermute | solution.py:40
  63.4 18.1 %collective-permute-start.24 = (bf16[384,640]{1,0:T(8,128)(2,1)}, bf16[384,640]{1,0:T(8,128)(2,1)S(1)}, u32[]{:S(2)}, u32[]{:S(2)}) collective-permute-start(bf16[384,640]{1,0:T(8,128)(2,1)} %get-tuple-element.63), channel_id=1, source_target_pairs={{0,12},{12,0},{1,13},{13,1},{2,14},{14,2},{3,15},{15,3},{16,28},{2... | collective-permute-start | bytes 1474568 | tf_op jit(solution)/shard_map/ppermute | solution.py:490
  68.8 25.2 %collective-permute-start.21 = (bf16[384,640]{1,0:T(8,128)(2,1)}, bf16[384,640]{1,0:T(8,128)(2,1)S(1)}, u32[]{:S(2)}, u32[]{:S(2)}) collective-permute-start(bf16[384,640]{1,0:T(8,128)(2,1)} %get-tuple-element.60), channel_id=1, source_target_pairs={{0,4},{4,0},{8,12},{12,8},{1,5},{5,1},{9,13},{13,9},{2,6},{6,2},{1... | collective-permute-start | bytes 1474568 | tf_op jit(solution)/shard_map/ppermute | solution.py:490
  68.8 41.6 %collective-permute-start.22 = (bf16[384,640]{1,0:T(8,128)(2,1)}, bf16[384,640]{1,0:T(8,128)(2,1)S(1)}, u32[]{:S(2)}, u32[]{:S(2)}) collective-permute-start(bf16[384,640]{1,0:T(8,128)(2,1)} %get-tuple-element.61), channel_id=1, source_target_pairs={{0,8},{4,12},{8,0},{12,4},{1,9},{5,13},{9,1},{13,5},{2,10},{6,14},... | collective-permute-start | bytes 1474568 | tf_op jit(solution)/shard_map/ppermute | solution.py:490
  69.8 42.1 %collective-permute-start.18 = (bf16[80,2048]{1,0:T(8,128)(2,1)S(1)}, bf16[80,2048]{1,0:T(8,128)(2,1)S(1)}, u32[]{:S(2)}, u32[]{:S(2)}) collective-permute-start(bf16[80,2048]{1,0:T(8,128)(2,1)S(1)} %get-tuple-element.52), channel_id=1, source_target_pairs={{0,1},{1,0},{2,3},{3,2},{4,5},{5,4},{6,7},{7,6},{8,9},{9,8},{10,11... | collective-permute-start | bytes 983048 | tf_op jit(solution)/shard_map/ppermute | solution.py:40
  70.0 42.0 %collective-permute-start.20 = (bf16[80,2048]{1,0:T(8,128)(2,1)S(1)}, bf16[80,2048]{1,0:T(8,128)(2,1)S(1)}, u32[]{:S(2)}, u32[]{:S(2)}) collective-permute-start(bf16[80,2048]{1,0:T(8,128)(2,1)S(1)} %add_convert_fusion.7), channel_id=1, source_target_pairs={{0,2},{1,3},{2,0},{3,1},{4,6},{5,7},{6,4},{7,5},{8,10},{9,11},{10,... | collective-permute-start | bytes 983048 | tf_op jit(solution)/shard_map/ppermute | solution.py:40
  81.6 31.8 %collective-permute-start.27 = (bf16[384,640]{1,0:T(8,128)(2,1)S(1)}, bf16[384,640]{1,0:T(8,128)(2,1)S(1)}, u32[]{:S(2)}, u32[]{:S(2)}) collective-permute-start(bf16[384,640]{1,0:T(8,128)(2,1)S(1)} %broadcast_select_fusion.refs_2_), channel_id=1, source_target_pairs={{0,16},{16,0},{1,17},{17,1},{2,18},{18,2},{3,19},{19,3},{4,20},{20... | collective-permute-start | bytes 1474568 | tf_op jit(solution)/shard_map/ppermute | solution.py:40
  93.9 22.6 %collective-permute-start.25 = (bf16[384,640]{1,0:T(8,128)(2,1)S(1)}, bf16[384,640]{1,0:T(8,128)(2,1)S(1)}, u32[]{:S(2)}, u32[]{:S(2)}) collective-permute-start(bf16[384,640]{1,0:T(8,128)(2,1)S(1)} %collective-permute-done.21.refs_0_), channel_id=1, source_target_pairs={{0,16},{16,0},{1,17},{17,1},{2,18},{18,2},{3,19},{19,3},{4,20},{20... | collective-permute-start | bytes 1474568 | tf_op jit(solution)/shard_map/ppermute | solution.py:40
  110.4 19.1 %collective-permute-start.26 = (bf16[384,640]{1,0:T(8,128)(2,1)S(1)}, bf16[384,640]{1,0:T(8,128)(2,1)S(1)}, u32[]{:S(2)}, u32[]{:S(2)}) collective-permute-start(bf16[384,640]{1,0:T(8,128)(2,1)S(1)} %collective-permute-done.22.refs_1_), channel_id=1, source_target_pairs={{0,16},{16,0},{1,17},{17,1},{2,18},{18,2},{3,19},{19,3},{4,20},{20... | collective-permute-start | bytes 1474568 | tf_op jit(solution)/shard_map/ppermute | solution.py:40
  112.4 17.1 %collective-permute-start.42 = (bf16[80,2048]{1,0:T(8,128)(2,1)S(1)}, bf16[80,2048]{1,0:T(8,128)(2,1)S(1)}, u32[]{:S(2)}, u32[]{:S(2)}) collective-permute-start(bf16[80,2048]{1,0:T(8,128)(2,1)S(1)} %get-tuple-element.66.refs_0_), channel_id=1, source_target_pairs={{0,8},{4,12},{8,0},{12,4},{1,9},{5,13},{9,1},{13,5},{2,10},{6,14},... | collective-permute-start | bytes 983048 | tf_op jit(solution)/shard_map/ppermute | solution.py:40
  112.5 17.7 %collective-permute-start.29 = (bf16[80,2048]{1,0:T(8,128)(2,1)S(1)}, bf16[80,2048]{1,0:T(8,128)(2,1)S(1)}, u32[]{:S(2)}, u32[]{:S(2)}) collective-permute-start(bf16[80,2048]{1,0:T(8,128)(2,1)S(1)} %get-tuple-element.66.refs_0_), channel_id=1, source_target_pairs={{0,2},{1,3},{2,0},{3,1},{4,6},{5,7},{6,4},{7,5},{8,10},{9,11},{10,... | collective-permute-start | bytes 983048 | tf_op jit(solution)/shard_map/ppermute | solution.py:40
  113.4 19.2 %collective-permute-start.34 = (bf16[80,2048]{1,0:T(8,128)(2,1)S(1)}, bf16[80,2048]{1,0:T(8,128)(2,1)S(1)}, u32[]{:S(2)}, u32[]{:S(2)}) collective-permute-start(bf16[80,2048]{1,0:T(8,128)(2,1)S(1)} %get-tuple-element.66.refs_0_), channel_id=1, source_target_pairs={{0,4},{4,0},{8,12},{12,8},{1,5},{5,1},{9,13},{13,9},{2,6},{6,2},{1... | collective-permute-start | bytes 983048 | tf_op jit(solution)/shard_map/ppermute | solution.py:40
  116.5 16.6 %collective-permute-start.28 = (bf16[80,2048]{1,0:T(8,128)(2,1)S(1)}, bf16[80,2048]{1,0:T(8,128)(2,1)S(1)}, u32[]{:S(2)}, u32[]{:S(2)}) collective-permute-start(bf16[80,2048]{1,0:T(8,128)(2,1)S(1)} %get-tuple-element.66.refs_0_), channel_id=1, source_target_pairs={{0,1},{1,0},{2,3},{3,2},{4,5},{5,4},{6,7},{7,6},{8,9},{9,8},{10,11... | collective-permute-start | bytes 983048 | tf_op jit(solution)/shard_map/ppermute | solution.py:40
  133.1 14.0 %collective-permute-start.36 = (bf16[80,2048]{1,0:T(8,128)(2,1)S(1)}, bf16[80,2048]{1,0:T(8,128)(2,1)S(1)}, u32[]{:S(2)}, u32[]{:S(2)}) collective-permute-start(bf16[80,2048]{1,0:T(8,128)(2,1)S(1)} %collective-permute-done.34.refs_0_), channel_id=1, source_target_pairs={{0,2},{1,3},{2,0},{3,1},{4,6},{5,7},{6,4},{7,5},{8,10},{9,11},{10,... | collective-permute-start | bytes 983048 | tf_op jit(solution)/shard_map/ppermute | solution.py:40
  139.1 14.1 %collective-permute-start.52 = (bf16[80,2048]{1,0:T(8,128)(2,1)S(1)}, bf16[80,2048]{1,0:T(8,128)(2,1)S(1)}, u32[]{:S(2)}, u32[]{:S(2)}) collective-permute-start(bf16[80,2048]{1,0:T(8,128)(2,1)S(1)} %collective-permute-done.50.refs_0_), channel_id=1, source_target_pairs={{0,2},{1,3},{2,0},{3,1},{4,6},{5,7},{6,4},{7,5},{8,10},{9,11},{10,... | collective-permute-start | bytes 983048 | tf_op jit(solution)/shard_map/ppermute | solution.py:40
  153.7 44.4 %collective-permute-start.31 = (bf16[80,2048]{1,0:T(8,128)(2,1)S(1)}, bf16[80,2048]{1,0:T(8,128)(2,1)S(1)}, u32[]{:S(2)}, u32[]{:S(2)}) collective-permute-start(bf16[80,2048]{1,0:T(8,128)(2,1)S(1)} %get-tuple-element.68), channel_id=1, source_target_pairs={{0,1},{1,0},{2,3},{3,2},{4,5},{5,4},{6,7},{7,6},{8,9},{9,8},{10,11... | collective-permute-start | bytes 983048 | tf_op jit(solution)/shard_map/ppermute | solution.py:40
  158.2 21.9 %collective-permute-start.38 = (bf16[80,2048]{1,0:T(8,128)(2,1)S(1)}, bf16[80,2048]{1,0:T(8,128)(2,1)S(1)}, u32[]{:S(2)}, u32[]{:S(2)}) collective-permute-start(bf16[80,2048]{1,0:T(8,128)(2,1)S(1)} %get-tuple-element.72), channel_id=1, source_target_pairs={{0,1},{1,0},{2,3},{3,2},{4,5},{5,4},{6,7},{7,6},{8,9},{9,8},{10,11... | collective-permute-start | bytes 983048 | tf_op jit(solution)/shard_map/ppermute | solution.py:40
  162.3 35.8 %collective-permute-start.33 = (bf16[80,2048]{1,0:T(8,128)(2,1)S(1)}, bf16[80,2048]{1,0:T(8,128)(2,1)S(1)}, u32[]{:S(2)}, u32[]{:S(2)}) collective-permute-start(bf16[80,2048]{1,0:T(8,128)(2,1)S(1)} %add_convert_fusion.6), channel_id=1, source_target_pairs={{0,2},{1,3},{2,0},{3,1},{4,6},{5,7},{6,4},{7,5},{8,10},{9,11},{10,... | collective-permute-start | bytes 983048 | tf_op jit(solution)/shard_map/ppermute | solution.py:40
  163.2 15.9 %collective-permute-start.48 = (bf16[80,2048]{1,0:T(8,128)(2,1)S(1)}, bf16[80,2048]{1,0:T(8,128)(2,1)S(1)}, u32[]{:S(2)}, u32[]{:S(2)}) collective-permute-start(bf16[80,2048]{1,0:T(8,128)(2,1)S(1)} %add_convert_fusion.3), channel_id=1, source_target_pairs={{0,2},{1,3},{2,0},{3,1},{4,6},{5,7},{6,4},{7,5},{8,10},{9,11},{10,... | collective-permute-start | bytes 983048 | tf_op jit(solution)/shard_map/ppermute | solution.py:40
  164.6 14.6 %collective-permute-start.55 = (bf16[80,2048]{1,0:T(8,128)(2,1)S(1)}, bf16[80,2048]{1,0:T(8,128)(2,1)S(1)}, u32[]{:S(2)}, u32[]{:S(2)}) collective-permute-start(bf16[80,2048]{1,0:T(8,128)(2,1)S(1)} %get-tuple-element.82), channel_id=1, source_target_pairs={{0,1},{1,0},{2,3},{3,2},{4,5},{5,4},{6,7},{7,6},{8,9},{9,8},{10,11... | collective-permute-start | bytes 983048 | tf_op jit(solution)/shard_map/ppermute | solution.py:40
  179.1 12.7 %collective-permute-start.54 = (bf16[80,2048]{1,0:T(8,128)(2,1)S(1)}, bf16[80,2048]{1,0:T(8,128)(2,1)S(1)}, u32[]{:S(2)}, u32[]{:S(2)}) collective-permute-start(bf16[80,2048]{1,0:T(8,128)(2,1)S(1)} %get-tuple-element.80), channel_id=1, source_target_pairs={{0,1},{1,0},{2,3},{3,2},{4,5},{5,4},{6,7},{7,6},{8,9},{9,8},{10,11... | collective-permute-start | bytes 983048 | tf_op jit(solution)/shard_map/ppermute | solution.py:40
  180.1 16.3 %collective-permute-start.56 = (bf16[80,2048]{1,0:T(8,128)(2,1)S(1)}, bf16[80,2048]{1,0:T(8,128)(2,1)S(1)}, u32[]{:S(2)}, u32[]{:S(2)}) collective-permute-start(bf16[80,2048]{1,0:T(8,128)(2,1)S(1)} %add_convert_fusion.1), channel_id=1, source_target_pairs={{0,2},{1,3},{2,0},{3,1},{4,6},{5,7},{6,4},{7,5},{8,10},{9,11},{10,... | collective-permute-start | bytes 983048 | tf_op jit(solution)/shard_map/ppermute | solution.py:40
  189.9 19.7 %collective-permute-start.49 = (bf16[80,2048]{1,0:T(8,128)(2,1)S(1)}, bf16[80,2048]{1,0:T(8,128)(2,1)S(1)}, u32[]{:S(2)}, u32[]{:S(2)}) collective-permute-start(bf16[80,2048]{1,0:T(8,128)(2,1)S(1)} %add_convert_fusion.2), channel_id=1, source_target_pairs={{0,8},{4,12},{8,0},{12,4},{1,9},{5,13},{9,1},{13,5},{2,10},{6,14},... | collective-permute-start | bytes 983048 | tf_op jit(solution)/shard_map/ppermute | solution.py:40
  191.8 17.9 %collective-permute-start.41 = (bf16[80,2048]{1,0:T(8,128)(2,1)S(1)}, bf16[80,2048]{1,0:T(8,128)(2,1)S(1)}, u32[]{:S(2)}, u32[]{:S(2)}) collective-permute-start(bf16[80,2048]{1,0:T(8,128)(2,1)S(1)} %add_convert_fusion.4), channel_id=1, source_target_pairs={{0,4},{4,0},{8,12},{12,8},{1,5},{5,1},{9,13},{13,9},{2,6},{6,2},{1... | collective-permute-start | bytes 983048 | tf_op jit(solution)/shard_map/ppermute | solution.py:40
  196.6 18.4 %collective-permute-start.57 = (bf16[80,2048]{1,0:T(8,128)(2,1)S(1)}, bf16[80,2048]{1,0:T(8,128)(2,1)S(1)}, u32[]{:S(2)}, u32[]{:S(2)}) collective-permute-start(bf16[80,2048]{1,0:T(8,128)(2,1)S(1)} %add_convert_fusion), channel_id=1, source_target_pairs={{0,12},{4,8},{8,4},{12,0},{1,13},{5,9},{9,5},{13,1},{2,14},{6,10},... | collective-permute-start | bytes 983048 | tf_op jit(solution)/shard_map/ppermute | solution.py:40
  (40 other events, 646.9 us)
